TPU v7x, 768 devices: a whole 4x8x12 slice. The times are simulated.
768 devices in a mesh: fs: 24 (over z, core), tp: 32 (over y, x).
Axes of the slice: x: 4, y: 8, z: 12, core: 2. Of those that a mesh axis runs over, the one named last changes fastest.
Arguments:
- grad_gate: float32 [2112, 5632], P('fs', 'tp'), may hold values from -45 to 45
- grad_up: float32 [2112, 5632], P('fs', 'tp'), may hold values from -45 to 45
- moment_gate: float32 [2112, 5632], P('fs', 'tp'), may hold values from -6 to 6
- moment_up: float32 [2112, 5632], P('fs', 'tp'), may hold values from -6 to 6
Outputs:
- moment_gate_next: float32 [2112, 5632], P('fs', 'tp')
- moment_up_next: float32 [2112, 5632], P('fs', 'tp')
- update_gate: float32 [2112, 5632], P('fs', 'tp')
- update_up: float32 [2112, 5632], P('fs', 'tp')
All inputs are finite; a program needn't handle non-finite values.
Results may differ from a plain program's by a relative error of at most 0.0019.
The roundings to bfloat16 on the way count: a program that leaves them out, or rounds other values in their place, can miss the bound.
Values may be sent and summed in bfloat16 or wider, within the bound.
No kernel may reach another device: no remote copies, remote signals or barrier semaphores. Data moves between devices by JAX's collectives and lax.ppermute only.
A program may use at most 32 MiB of HBM per device.

v0:
```python
import jax
import jax.numpy as jnp
from jax import lax
from jax.sharding import Mesh
from jax.sharding import PartitionSpec as P

FF = 5632
ITERS = 3
FS = ("fs_0", "fs_1")
TP = ("tp_0", "tp_1")
FS_TP = ("fs_0", "fs_1", "tp_0", "tp_1")


BETA = 0.95
EPS = 1e-06


def laid_out(blocks, dim):
    shape = list(blocks.shape[1:])
    shape[dim] *= blocks.shape[0]
    return jnp.moveaxis(blocks, 0, dim).reshape(shape)


def stacked_from(array, axes, order):
    blocks = array
    for k in order:
        blocks = lax.all_gather(blocks, axes[k])
    done = order[::-1]
    back = [done.index(k) for k in range(len(axes))]
    blocks = blocks.transpose(*back, *range(len(axes), blocks.ndim))
    return blocks.reshape(-1, *array.shape)


def whole_of(array, axes, order, dim):
    return laid_out(stacked_from(array, axes, order), dim)


def copy_for_each(array, axis):
    copies = jnp.broadcast_to(array, (lax.axis_size(axis), *array.shape))
    return lax.all_to_all(copies, axis, split_axis=0, concat_axis=0, tiled=True)


def gather_directly(array, axis, dim):
    return laid_out(copy_for_each(array, axis), dim)


def turned_gather(arrays, axis, dims):
    turned = [jnp.moveaxis(a, dim, 0) for a, dim in zip(arrays, dims)]
    both = jnp.concatenate([t.reshape(len(t), -1) for t in turned], axis=1)
    result, at, outs = (lax.all_gather(both, axis, axis=0, tiled=True), 0, [])
    for t, dim in zip(turned, dims):
        slab = result[:, at : at + t[0].size].reshape(-1, *t.shape[1:])
        outs.append(jnp.moveaxis(slab, 0, dim))
        at += t[0].size
    return tuple(outs)


def over_axes(array, axes):
    for axis in axes:
        array = lax.psum(array, axis)
    return array


def in_one_piece(arrays, axis, dim, along):
    both = jnp.concatenate(arrays, axis=along)
    result, at, outs = (lax.all_gather(both, axis, axis=dim, tiled=True), 0, [])
    for a in arrays:
        outs.append(lax.slice_in_dim(result, at, at + a.shape[along], axis=along))
        at += a.shape[along]
    return tuple(outs)


def cut_along(array, dim, devices):
    shape = array.shape
    blocks = array.reshape(*shape[:dim], devices, shape[dim] // devices, *shape[dim + 1 :])
    return jnp.moveaxis(blocks, dim, 0)


def sum_at_owner(array, axis, dim):
    blocks = cut_along(array, dim, lax.axis_size(axis))
    arrived = lax.all_to_all(blocks, axis, split_axis=0, concat_axis=0, tiled=True)
    return arrived.sum(axis=0)


def multiply(left_low, right_low):
    left_rows = whole_of(left_low, FS, (0, 1), 1)

    def accumulate(running, segment, offset):
        return jnp.dot(left_rows, segment, preferred_element_type=jnp.float32)

    empty = jnp.zeros(left_low.shape, jnp.float32)
    return accumulate(empty, gather_directly(right_low, TP, 0), jnp.int32(0))


def multiply_pair(first_low, second_low, right_low):
    first_rows, second_rows = turned_gather((first_low, second_low), FS, (1, 1))

    def accumulate(running, segment, offset):
        return (
            jnp.dot(first_rows, segment, preferred_element_type=jnp.float32),
            jnp.dot(second_rows, segment, preferred_element_type=jnp.float32),
        )

    empty = jnp.zeros(first_low.shape, jnp.float32)
    return accumulate((empty, empty), gather_directly(right_low, TP, 0), jnp.int32(0))


def local(grad_gate, grad_up, moment_gate, moment_up):
    moment_gate_next = BETA * moment_gate + grad_gate
    moment_up_next = BETA * moment_up + grad_up
    low_gate = moment_gate_next.astype(jnp.bfloat16)
    low_up = moment_up_next.astype(jnp.bfloat16)
    trace_local = jnp.sum(jnp.square(low_gate.astype(jnp.float32))) + jnp.sum(
        jnp.square(low_up.astype(jnp.float32))
    )
    trace_total = over_axes(trace_local, FS_TP)
    columns_gate, columns_up = in_one_piece((low_gate, low_up), FS, 0, 1)
    rows_dev = low_gate.shape[0]
    width = columns_gate.shape[0]
    own_rows = width // lax.axis_size(TP)
    block_gate = columns_gate
    block_up = columns_up
    gram = sum_at_owner(
        jnp.einsum("ik,jk->ij", block_gate, low_gate, preferred_element_type=jnp.float32)
        + jnp.einsum("ik,jk->ij", block_up, low_up, preferred_element_type=jnp.float32),
        TP,
        0,
    )
    square_local = jnp.sum(gram * gram)
    square_total = over_axes(square_local, FS_TP)
    spectral = 2.0 * square_total / (trace_total + EPS)
    current = gram / spectral
    row_index = lax.axis_index(TP) * own_rows + lax.broadcasted_iota(
        jnp.int32, (own_rows, rows_dev), 0
    )
    col_index = lax.axis_index(FS) * rows_dev + lax.broadcasted_iota(
        jnp.int32, (own_rows, rows_dev), 1
    )
    identity = (row_index == col_index).astype(jnp.float32)
    product_low = None
    for iteration in range(ITERS):
        poly_low = (1.5 * identity - 0.5 * current).astype(jnp.bfloat16)
        final_turn = iteration == ITERS - 1
        square_low = None
        if iteration == 0:
            product_low = poly_low
            square_low = multiply(poly_low, poly_low).astype(jnp.bfloat16)
        elif final_turn:
            product_low = multiply(product_low, poly_low).astype(jnp.bfloat16)
        else:
            product_full, square_full = multiply_pair(product_low, poly_low, poly_low)
            product_low = product_full.astype(jnp.bfloat16)
            square_low = square_full.astype(jnp.bfloat16)
        if not final_turn:
            current = multiply(current.astype(jnp.bfloat16), square_low)
    factor = jnp.sqrt(2.0 * FF / spectral)
    segment = gather_directly(product_low, TP, 0)
    block_gate = columns_gate
    block_up = columns_up
    ortho_gate = jnp.einsum("jr,jc->rc", segment, block_gate, preferred_element_type=jnp.float32)
    ortho_up = jnp.einsum("jr,jc->rc", segment, block_up, preferred_element_type=jnp.float32)
    return (moment_gate_next, moment_up_next, ortho_gate * factor, ortho_up * factor)


def solution(mesh):
    split = Mesh(mesh.devices.reshape(12, 2, 8, 4), ("fs_0", "fs_1", "tp_0", "tp_1"))
    in_specs = (P(FS, TP), P(FS, TP), P(FS, TP), P(FS, TP))
    out_specs = (P(FS, TP), P(FS, TP), P(FS, TP), P(FS, TP))
    return jax.shard_map(local, mesh=split, in_specs=in_specs, out_specs=out_specs, check_vma=False)
```

profile of v0, /device:TPU:8, one launch (start us, length us, event | category | flops | bytes accessed | tf_op | source)
XLA Modules:
  0.0 398.2 jit_solution(16128045076685427762)
XLA Ops:
  7.2 2.4 multiply_reduce_fusion
  9.6 0.7 pad_maximum_fusion
  10.3 67.1 %all-gather.13.cloned.1.call-done = bf16[2112,352]{1,0:T(8,128)(2,1)} async-done(((bf16[88,352]{1,0:T(8,128)(2,1)}), bf16[2112,352]{1,0:T(8,128)(2,1)}) %all-gather.13.cloned.1.call-update) | async-done | bytes 1486864 | tf_op jit(solution)/shard_map/all_gather | solution.py:66
  77.4 1.8 fusion.6
  79.2 1.4 convolution_add_fusion
  80.6 3.3 reshape.123
  84.0 1.9 copy.19
  85.9 9.8 %all-to-all-start = ((f32[32,66,88]{2,1,0:T(8,128)}), f32[32,66,88]{2,1,0:T(8,128)S(1)}, u32[]{:S(2)}, u32[]{:S(2)}) async-start(f32[32,66,88]{2,1,0:T(8,128)} %copy.19), calls=%async_computation | async-start | bytes 2359296 | tf_op jit(solution)/shard_map/all_to_all | solution.py:81
  97.1 29.0 %all-to-all-done = f32[32,66,88]{2,1,0:T(8,128)S(1)} async-done(((f32[32,66,88]{2,1,0:T(8,128)}), f32[32,66,88]{2,1,0:T(8,128)S(1)}, u32[]{:S(2)}, u32[]{:S(2)}) %all-to-all-start) | async-done | bytes 743456 | tf_op jit(solution)/shard_map/all_to_all | solution.py:81
  126.1 0.1 reduce_sum.36
  126.2 0.1 copy.39
  126.3 0.6 multiply_reduce_fusion.2
  126.9 21.9 %all-reduce = (f32[]{:T(128)}, f32[]{:T(128)}) all-reduce(f32[]{:T(128)} %multiply_reduce_fusion.2, f32[]{:T(128)S(6)} %add.60), channel_id=1, replica_groups=mesh['fs_0'=12,'fs_1'=2,'tp_0'=8,'tp_1'=4] {'fs_0'}, use_global_device_ids=true, to_apply=%region_2.0 | all-reduce | flops 2 | bytes 16 | tf_op jit(solution)/shard_map/psum | solution.py:60
  148.8 3.1 all-reduce.3
  151.9 15.9 %all-reduce.1 = (f32[]{:T(128)}, f32[]{:T(128)}) all-reduce(f32[]{:T(128)} %get-tuple-element.10, f32[]{:T(128)} %get-tuple-element.11), channel_id=1, replica_groups=mesh['fs_0'=12,'fs_1'=2,'tp_0'=8,'tp_1'=4] {'tp_0'}, use_global_device_ids=true, to_apply=%region_4.0 | all-reduce | flops 2 | bytes 16 | tf_op jit(solution)/shard_map/psum | solution.py:60
  167.8 11.4 %all-reduce.2 = (f32[]{:T(128)}, f32[]{:T(128)}) all-reduce(f32[]{:T(128)} %get-tuple-element.6, f32[]{:T(128)} %get-tuple-element.7), channel_id=1, replica_groups=mesh['fs_0'=12,'fs_1'=2,'tp_0'=8,'tp_1'=4] {'tp_1'}, use_global_device_ids=true, to_apply=%region_5.0 | all-reduce | flops 2 | bytes 16 | tf_op jit(solution)/shard_map/psum | solution.py:60
  180.5 0.1 fusion.12
  180.6 0.9 broadcast_in_dim.18
  181.5 5.0 %all-to-all-start.1 = ((bf16[32,66,88]{2,1,0:T(8,128)(2,1)}), bf16[32,66,88]{2,1,0:T(8,128)(2,1)S(1)}, u32[]{:S(2)}, u32[]{:S(2)}) async-start(bf16[32,66,88]{2,1,0:T(8,128)(2,1)} %broadcast_in_dim.18), calls=%async_computation.1 | async-start | bytes 1179648 | tf_op jit(solution)/shard_map/all_to_all | solution.py:40
  186.4 0.1 fusion.14
  186.5 22.2 %all_gather.54 = bf16[12,66,88]{2,1,0:T(8,128)(2,1)S(1)} all-gather(bf16[1,66,88]{2,1,0:T(8,128)(2,1)S(1)} %fusion.14), channel_id=1, replica_groups=mesh['fs_0'=12,'fs_1'=2,'tp_0'=8,'tp_1'=4] {'fs_0'}, dimensions={0}, use_global_device_ids=true | all-gather | bytes 151008 | tf_op jit(solution)/shard_map/all_gather | solution.py:27
  208.7 2.1 all-gather.2
  210.8 0.3 copy.23
  211.1 0.4 reshape.127
  211.5 0.2 reshape.156
  211.7 0.3 convolution_convert_fusion.3
  212.0 0.9 broadcast_in_dim.19
  212.9 9.7 %all-to-all-start.2 = ((bf16[32,66,88]{2,1,0:T(8,128)(2,1)}), bf16[32,66,88]{2,1,0:T(8,128)(2,1)S(1)}, u32[]{:S(2)}, u32[]{:S(2)}) async-start(bf16[32,66,88]{2,1,0:T(8,128)(2,1)} %broadcast_in_dim.19), calls=%async_computation.2 | async-start | bytes 1179648 | tf_op jit(solution)/shard_map/all_to_all | solution.py:40
  222.6 21.5 %all-gather.7 = bf16[12,66,88]{2,1,0:T(8,128)(2,1)S(1)} all-gather(bf16[1,66,88]{2,1,0:T(8,128)(2,1)S(1)} %get-tuple-element.21), channel_id=2, replica_groups=mesh['fs_0'=12,'fs_1'=2,'tp_0'=8,'tp_1'=4] {'fs_0'}, dimensions={0}, use_global_device_ids=true | all-gather | bytes 151008 | tf_op jit(solution)/shard_map/all_gather | solution.py:27
  244.1 2.1 all-gather.1
  246.2 0.3 copy.22
  246.5 0.4 reshape.125
  246.9 0.2 reshape.157
  247.1 0.2 fusion.10
  247.4 0.9 broadcast_in_dim.20
  248.4 9.8 %all-to-all-start.3 = ((bf16[32,66,88]{2,1,0:T(8,128)(2,1)}), bf16[32,66,88]{2,1,0:T(8,128)(2,1)S(1)}, u32[]{:S(2)}, u32[]{:S(2)}) async-start(bf16[32,66,88]{2,1,0:T(8,128)(2,1)} %broadcast_in_dim.20), calls=%async_computation.3 | async-start | bytes 1179648 | tf_op jit(solution)/shard_map/all_to_all | solution.py:40
  258.2 24.1 %all-gather.8 = bf16[24,88,132]{1,2,0:T(8,128)(2,1)S(1)} all-gather(bf16[1,88,132]{1,2,0:T(8,128)(2,1)S(1)} %maximum_bitcast_fusion), channel_id=1, replica_groups=mesh['fs_0'=12,'fs_1'=2,'tp_0'=8,'tp_1'=4] {'fs_0','fs_1'}, dimensions={0}, use_global_device_ids=true | all-gather | bytes 580800 | tf_op jit(solution)/shard_map/all_gather | solution.py:50
  282.3 0.1 copy.26
  282.4 1.5 reshape.148
  283.9 0.2 reshape.158
  284.1 1.4 convolution_convert_fusion.1
  285.5 0.9 broadcast_in_dim.21
  286.4 9.8 %all-to-all-start.4 = ((bf16[32,66,88]{2,1,0:T(8,128)(2,1)}), bf16[32,66,88]{2,1,0:T(8,128)(2,1)S(1)}, u32[]{:S(2)}, u32[]{:S(2)}) async-start(bf16[32,66,88]{2,1,0:T(8,128)(2,1)} %broadcast_in_dim.21), calls=%async_computation.4 | async-start | bytes 1179648 | tf_op jit(solution)/shard_map/all_to_all | solution.py:40
  296.2 21.4 %all-gather.10 = bf16[12,66,88]{2,1,0:T(8,128)(2,1)S(1)} all-gather(bf16[1,66,88]{2,1,0:T(8,128)(2,1)S(1)} %get-tuple-element.18), channel_id=7, replica_groups=mesh['fs_0'=12,'fs_1'=2,'tp_0'=8,'tp_1'=4] {'fs_0'}, dimensions={0}, use_global_device_ids=true | all-gather | bytes 151008 | tf_op jit(solution)/shard_map/all_gather | solution.py:27
  317.6 2.3 all-gather.6
  319.9 0.3 copy.29
  320.2 1.1 reshape.134
  321.4 0.2 reshape.159
  321.6 1.3 fusion.1
  322.9 0.9 broadcast_in_dim.22
  323.8 9.8 %all-to-all-start.5 = ((bf16[32,66,88]{2,1,0:T(8,128)(2,1)}), bf16[32,66,88]{2,1,0:T(8,128)(2,1)S(1)}, u32[]{:S(2)}, u32[]{:S(2)}) async-start(bf16[32,66,88]{2,1,0:T(8,128)(2,1)} %broadcast_in_dim.22), calls=%async_computation.5 | async-start | bytes 1179648 | tf_op jit(solution)/shard_map/all_to_all | solution.py:40
  333.6 0.3 fusion.2
  333.8 22.3 %all-gather.9 = bf16[12,66,88]{2,1,0:T(8,128)(2,1)S(1)} all-gather(bf16[1,66,88]{2,1,0:T(8,128)(2,1)S(1)} %fusion.2), channel_id=5, replica_groups=mesh['fs_0'=12,'fs_1'=2,'tp_0'=8,'tp_1'=4] {'fs_0'}, dimensions={0}, use_global_device_ids=true | all-gather | bytes 151008 | tf_op jit(solution)/shard_map/all_gather | solution.py:27
  356.1 2.1 all-gather.4
  358.2 0.3 copy.28
  358.5 0.4 reshape.132
  358.9 0.2 reshape.160
  359.1 0.3 convolution_convert_fusion
  359.4 0.9 broadcast_in_dim.23
  360.3 9.8 %all-to-all-start.6 = ((bf16[32,66,88]{2,1,0:T(8,128)(2,1)}), bf16[32,66,88]{2,1,0:T(8,128)(2,1)S(1)}, u32[]{:S(2)}, u32[]{:S(2)}) async-start(bf16[32,66,88]{2,1,0:T(8,128)(2,1)} %broadcast_in_dim.23), calls=%async_computation.6 | async-start | bytes 1179648 | tf_op jit(solution)/shard_map/all_to_all | solution.py:40
  370.2 18.7 %all-to-all-done.6 = bf16[32,66,88]{2,1,0:T(8,128)(2,1)S(1)} async-done(((bf16[32,66,88]{2,1,0:T(8,128)(2,1)}), bf16[32,66,88]{2,1,0:T(8,128)(2,1)S(1)}, u32[]{:S(2)}, u32[]{:S(2)}) %all-to-all-start.6) | async-done | bytes 371744 | tf_op jit(solution)/shard_map/all_to_all | solution.py:40
  388.9 0.2 reshape.161
  389.1 1.3 convolution_multiply_fusion
  390.3 1.0 convolution_multiply_fusion.1
  (19 shorter events, 0.2 us)
Async XLA Ops:
  7.2 70.2 %all-gather.13.cloned.1.call-start = ((), (), s32[]{:S(2)}) async-start(), calls=%async_computation.7 | async-start | bytes 1689600 | tf_op jit(solution)/shard_map/all_gather | solution.py:66
  77.4 1.8 copy-start
  85.9 40.2 %all-to-all-start = ((f32[32,66,88]{2,1,0:T(8,128)}), f32[32,66,88]{2,1,0:T(8,128)S(1)}, u32[]{:S(2)}, u32[]{:S(2)}) async-start(f32[32,66,88]{2,1,0:T(8,128)} %copy.19), calls=%async_computation | async-start | bytes 2359296 | tf_op jit(solution)/shard_map/all_to_all | solution.py:81
  181.5 30.1 %all-to-all-start.1 = ((bf16[32,66,88]{2,1,0:T(8,128)(2,1)}), bf16[32,66,88]{2,1,0:T(8,128)(2,1)S(1)}, u32[]{:S(2)}, u32[]{:S(2)}) async-start(bf16[32,66,88]{2,1,0:T(8,128)(2,1)} %broadcast_in_dim.18), calls=%async_computation.1 | async-start | bytes 1179648 | tf_op jit(solution)/shard_map/all_to_all | solution.py:40
  212.9 34.0 %all-to-all-start.2 = ((bf16[32,66,88]{2,1,0:T(8,128)(2,1)}), bf16[32,66,88]{2,1,0:T(8,128)(2,1)S(1)}, u32[]{:S(2)}, u32[]{:S(2)}) async-start(bf16[32,66,88]{2,1,0:T(8,128)(2,1)} %broadcast_in_dim.19), calls=%async_computation.2 | async-start | bytes 1179648 | tf_op jit(solution)/shard_map/all_to_all | solution.py:40
  248.4 35.5 %all-to-all-start.3 = ((bf16[32,66,88]{2,1,0:T(8,128)(2,1)}), bf16[32,66,88]{2,1,0:T(8,128)(2,1)S(1)}, u32[]{:S(2)}, u32[]{:S(2)}) async-start(bf16[32,66,88]{2,1,0:T(8,128)(2,1)} %broadcast_in_dim.20), calls=%async_computation.3 | async-start | bytes 1179648 | tf_op jit(solution)/shard_map/all_to_all | solution.py:40
  284.1 2.3 copy-start.1
  286.4 34.9 %all-to-all-start.4 = ((bf16[32,66,88]{2,1,0:T(8,128)(2,1)}), bf16[32,66,88]{2,1,0:T(8,128)(2,1)S(1)}, u32[]{:S(2)}, u32[]{:S(2)}) async-start(bf16[32,66,88]{2,1,0:T(8,128)(2,1)} %broadcast_in_dim.21), calls=%async_computation.4 | async-start | bytes 1179648 | tf_op jit(solution)/shard_map/all_to_all | solution.py:40
  321.6 12.0 %copy-start.2 = (bf16[2112,88]{1,0:T(8,128)(2,1)S(1)}, bf16[2112,88]{1,0:T(8,128)(2,1)}, u32[]{:S(2)}) copy-start(bf16[2112,88]{1,0:T(8,128)(2,1)} %copy-done.1) | copy-start | bytes 1115140
  322.8 10.7 %copy-start.3 = (bf16[2112,132]{0,1:T(8,128)(2,1)S(1)}, bf16[2112,132]{0,1:T(8,128)(2,1)}, u32[]{:S(2)}) copy-start(bf16[2112,132]{0,1:T(8,128)(2,1)} %reshape.148) | copy-start | bytes 1672708
  323.8 35.1 %all-to-all-start.5 = ((bf16[32,66,88]{2,1,0:T(8,128)(2,1)}), bf16[32,66,88]{2,1,0:T(8,128)(2,1)S(1)}, u32[]{:S(2)}, u32[]{:S(2)}) async-start(bf16[32,66,88]{2,1,0:T(8,128)(2,1)} %broadcast_in_dim.22), calls=%async_computation.5 | async-start | bytes 1179648 | tf_op jit(solution)/shard_map/all_to_all | solution.py:40
  360.3 28.6 %all-to-all-start.6 = ((bf16[32,66,88]{2,1,0:T(8,128)(2,1)}), bf16[32,66,88]{2,1,0:T(8,128)(2,1)S(1)}, u32[]{:S(2)}, u32[]{:S(2)}) async-start(bf16[32,66,88]{2,1,0:T(8,128)(2,1)} %broadcast_in_dim.23), calls=%async_computation.6 | async-start | bytes 1179648 | tf_op jit(solution)/shard_map/all_to_all | solution.py:40
Sparse Core Ops, SparseCore 0:
  11.0 66.3 all-gather.12
where the time goes:
time: 399 us; the launch traced here: 398 us
  blocking collectives  172 us (43%)
  waiting for transfers between devices  115 us (29%)
  starting transfers between devices  63.6 us (16%)
  between operations  17.1 us (4%)
  local copies, waits for them, and re-layouts  17 us (4%)
  matrix products  9.17 us (2%)
  other arithmetic  4.08 us (1%)
    all_gather x8, blocking collectives, stacked_from(): blocks = lax.all_gather(blocks, axes[k])  96 us
    all_gather x1, waiting for transfers between devices, in_one_piece(): result, at, outs = (lax.all_gather(both, axis, axis=dim, tiled=True), 0, [])  67.1 us
    all_to_all x6, starting transfers between devices, copy_for_each(): return lax.all_to_all(copies, axis, split_axis=0, concat_axis=0, tiled=True)  53.7 us
    psum x4, blocking collectives, over_axes(): array = lax.psum(array, axis)  52.2 us
    all_to_all x1, waiting for transfers between devices, sum_at_owner(): lax.all_to_all(blocks, axis, split_axis=0, concat_axis=0, tiled=True)  29 us
    all_gather x1, blocking collectives, turned_gather(): result, at, outs = (lax.all_gather(both, axis, axis=0, tiled=True), 0, [])  24.1 us
    all_to_all x6, waiting for transfers between devices, copy_for_each(): return lax.all_to_all(copies, axis, split_axis=0, concat_axis=0, tiled=True)  18.7 us
    all_to_all x1, starting transfers between devices, sum_at_owner(): lax.all_to_all(blocks, axis, split_axis=0, concat_axis=0, tiled=True)  9.85 us
  transfers between devices with their start and end apart: 8, of which 3 were waited for; matrix products, arithmetic and copies ran while one was open for 1% of the time, Pallas kernels for 0%

commit v1 on v0

v1 whole, which is shorter than its diff:
```python
import jax
import jax.numpy as jnp
from jax import lax
from jax.sharding import Mesh
from jax.sharding import PartitionSpec as P

FF = 5632
FS = ("z", "core")
TP = ("y", "x")
BETA = 0.95
EPS = 1e-06


def dot(left, right):
    return jnp.dot(left, right, preferred_element_type=jnp.float32)


def to_all(block, axes):
    copies = jnp.broadcast_to(block, (lax.axis_size(axes), *block.shape))
    return lax.all_to_all(copies, axes, split_axis=0, concat_axis=0, tiled=True)


def rows_of(blocks):
    return jnp.moveaxis(blocks, 0, 1).reshape(blocks.shape[1], -1)


def gather_rows(block):
    by_z = lax.all_gather(block, "z")
    both = lax.all_gather(by_z, "core")
    return jnp.swapaxes(both, 0, 1).reshape(-1, *block.shape)


def local(grad_gate, grad_up, moment_gate, moment_up):
    gate_next = BETA * moment_gate + grad_gate
    up_next = BETA * moment_up + grad_up
    low = jnp.concatenate([gate_next.astype(jnp.bfloat16), up_next.astype(jnp.bfloat16)], axis=1)
    rows_dev, half = gate_next.shape
    by_z = lax.all_gather(low, "z")
    gate_all = gather_core(by_z[..., :half])
    up_all = gather_core(by_z[..., half:])
    width = gate_all.shape[0]
    own_rows = width // lax.axis_size(TP)
    share = lax.dot_general(
        gate_all, low[:, :half], (((1,), (1,)), ((), ())), preferred_element_type=jnp.float32
    ) + lax.dot_general(
        up_all, low[:, half:], (((1,), (1,)), ((), ())), preferred_element_type=jnp.float32
    )
    blocks = share.reshape(-1, own_rows, rows_dev)
    arrived = lax.all_to_all(blocks, TP, split_axis=0, concat_axis=0, tiled=True)
    gram = arrived.sum(axis=0)

    rows_at = lax.axis_index(TP) * own_rows
    cols_at = lax.axis_index(FS) * rows_dev

    def eye_of(shape, row, col):
        i = row + lax.broadcasted_iota(jnp.int32, shape, 0)
        j = col + lax.broadcasted_iota(jnp.int32, shape, 1)
        return i == j

    own_eye = eye_of((own_rows, rows_dev), rows_at, cols_at)
    rows_eye = eye_of((own_rows, width), rows_at, 0)
    cols_eye = eye_of((width, rows_dev), 0, cols_at)

    gram_rows = rows_of(gather_rows(gram))
    square = jnp.sum(gram_rows * gram_rows)
    trace = jnp.sum(jnp.where(rows_eye, gram_rows, 0.0))
    tail = jnp.zeros((own_rows, 2), jnp.float32) + jnp.stack([square, trace])[None, :]
    sent = jnp.concatenate([gram, tail], axis=1)
    arrived = to_all(sent, TP)
    gram_cols = arrived[..., :rows_dev].reshape(width, rows_dev)
    totals = arrived[:, 0, rows_dev:].sum(axis=0)
    spectral = 2.0 * totals[0] / (totals[1] + EPS)

    def poly(eye, current):
        return jnp.where(eye, 1.5 - 0.5 * current, -0.5 * current).astype(jnp.bfloat16)

    current_rows = gram_rows / spectral
    poly_rows = poly(rows_eye, current_rows)
    current_rows = current_rows.astype(jnp.bfloat16)
    poly_cols = poly(cols_eye, gram_cols / spectral)

    square_low = dot(poly_rows, poly_cols).astype(jnp.bfloat16)
    square_cols = to_all(square_low, TP).reshape(width, rows_dev)
    current = dot(current_rows, square_cols)
    poly_low = poly(own_eye, current)
    diag = jnp.sum(jnp.where(own_eye, current, 0.0), axis=1, keepdims=True).astype(jnp.bfloat16)

    poly_cols = to_all(poly_low, TP).reshape(width, rows_dev)
    blocks = gather_rows(jnp.concatenate([poly_low, diag], axis=1))
    first_rows = rows_of(blocks[..., :rows_dev])
    diag = blocks[..., rows_dev].astype(jnp.float32).sum(axis=0)
    current_rows = jnp.where(
        rows_eye, diag[:, None], -2.0 * first_rows.astype(jnp.float32)
    ).astype(jnp.bfloat16)

    product_low = dot(poly_rows, poly_cols).astype(jnp.bfloat16)
    square_low = dot(first_rows, poly_cols).astype(jnp.bfloat16)
    square_cols = to_all(square_low, TP).reshape(width, rows_dev)
    product_rows = rows_of(gather_rows(product_low))
    current = dot(current_rows, square_cols)
    poly_low = poly(own_eye, current)
    poly_cols = to_all(poly_low, TP).reshape(width, rows_dev)
    product_low = dot(product_rows, poly_cols).astype(jnp.bfloat16)
    product_cols = to_all(product_low, TP).reshape(width, rows_dev)

    factor = jnp.sqrt(2.0 * FF / spectral)
    over_rows = (((0,), (0,)), ((), ()))
    ortho_gate = lax.dot_general(product_cols, gate_all, over_rows, preferred_element_type=jnp.float32)
    ortho_up = lax.dot_general(product_cols, up_all, over_rows, preferred_element_type=jnp.float32)
    return gate_next, up_next, ortho_gate * factor, ortho_up * factor


def gather_core(by_z):
    both = lax.all_gather(by_z, "core")
    return jnp.swapaxes(both, 0, 1).reshape(-1, by_z.shape[-1])


def solution(mesh):
    split = Mesh(mesh.devices.reshape(12, 2, 8, 4), ("z", "core", "y", "x"))
    spec = P(FS, TP)
    return jax.shard_map(
        local, mesh=split, in_specs=(spec,) * 4, out_specs=(spec,) * 4, check_vma=False
    )
```

time: 399 us -> 334 us (0.84)
  blocking collectives: 172 us -> 115 us
  local copies, waits for them, and re-layouts: 17 us -> 32 us
  between operations: 17.1 us -> 2.42 us
  starting transfers between devices: 63.6 us -> 53 us
  other arithmetic: 4.08 us -> 10.2 us
  waiting for transfers between devices: 115 us -> 111 us
    all_gather x1 -> x0, waiting for transfers between devices: 67.1 us -> none  [in_one_piece(): result, at, outs = (lax.all_gather(both, axis, axis=dim, tiled=True), 0, [])]
    all_to_all x7, waiting for transfers between devices: 47.7 us -> 111 us  [the longest x6 81 us: to_all(): return lax.all_to_all(copies, axes, split_axis=0, concat_axis=0, tiled=True)]
    psum x4 -> x0, blocking collectives: 52.2 us -> none  [over_axes(): array = lax.psum(array, axis)]
    all_to_all x7, starting transfers between devices: 63.6 us -> 53 us  [the longest x6 42.8 us: to_all(): return lax.all_to_all(copies, axes, split_axis=0, concat_axis=0, tiled=True)]
    convert_element_type x0 -> x6, local copies, waits for them, and re-layouts: none -> 8.57 us  [the longest x3 6.65 us: poly(): jnp.where(eye, 1.5 - 0.5 * current, -0.5 * current).astype(jnp.bfloat16)]
    convert_element_type x2 -> x4, other arithmetic: 0.16 us -> 5.91 us  [the longest x1 2.12 us: poly(): jnp.where(eye, 1.5 - 0.5 * current, -0.5 * current).astype(jnp.bfloat16)]
    all_gather x9, blocking collectives: 120 us -> 115 us  [the longest x3 66.1 us: gather_rows(): by_z = lax.all_gather(block, 'z')]
    transpose x0 -> x4, local copies, waits for them, and re-layouts: none -> 4.37 us  [the longest x2 3.7 us: gather_core(): return jnp.swapaxes(both, 0, 1).reshape(-1, by_z.shape[-1])]
  transfers between devices with their start and end apart: 8 -> 7, of which waited for: 3 -> 5; matrix products, arithmetic and copies ran while one was open for 1% -> 2% of each run, Pallas kernels for 0% -> 0%
where the time goes in v1:
time: 334 us; the launch traced here: 332 us
  blocking collectives  115 us (34%)
  waiting for transfers between devices  111 us (33%)
  starting transfers between devices  53 us (16%)
  local copies, waits for them, and re-layouts  32 us (10%)
  other arithmetic  10.2 us (3%)
  matrix products  8.2 us (2%)
    all_to_all x6, waiting for transfers between devices, to_all(): return lax.all_to_all(copies, axes, split_axis=0, concat_axis=0, tiled=True)  81 us
    all_gather x3, blocking collectives, gather_rows(): by_z = lax.all_gather(block, 'z')  66.1 us
    all_to_all x6, starting transfers between devices, to_all(): return lax.all_to_all(copies, axes, split_axis=0, concat_axis=0, tiled=True)  42.8 us
    all_gather x1, blocking collectives, local(): by_z = lax.all_gather(low, 'z')  37.4 us
    all_to_all x1, waiting for transfers between devices, local(): lax.all_to_all(blocks, TP, split_axis=0, concat_axis=0, tiled=True)  30.3 us
    all_to_all x1, starting transfers between devices, local(): lax.all_to_all(blocks, TP, split_axis=0, concat_axis=0, tiled=True)  10.2 us
  transfers between devices with their start and end apart: 7, of which 5 were waited for; matrix products, arithmetic and copies ran while one was open for 2% of the time, Pallas kernels for 0%

profile of v1, /device:TPU:8, one launch (start us, length us, event | category | flops | bytes accessed | tf_op | source)
XLA Modules:
  0.0 332.4 jit_solution(11447079531061005362)
XLA Ops:
  0.6 1.7 fusion.8
  2.4 37.4 %all-gather = bf16[1056,352]{1,0:T(8,128)(2,1)S(1)} all-gather(bf16[88,352]{1,0:T(8,128)(2,1)S(1)} %pad_maximum_fusion), channel_id=2, replica_groups=mesh['z'=12,'core'=2,'y'=8,'x'=4] {'z'}, dimensions={0}, use_global_device_ids=true | all-gather | bytes 805376 | tf_op jit(solution)/shard_map/all_gather | solution.py:38
  39.8 1.1 fusion.10
  40.8 2.6 all-gather.1
  43.4 1.0 copy.46
  44.5 0.8 reshape.122
  45.3 0.3 fusion.12
  45.6 0.8 copy-done.1
  46.4 2.7 all-gather.2
  49.0 2.7 copy.47
  51.7 0.8 reshape.123
  52.5 1.2 convolution_add_fusion
  53.7 3.3 %reshape.124 = f32[32,66,88]{1,0,2:T(8,128)S(1)} reshape(f32[2112,88]{0,1:T(8,128)} %convolution_add_fusion) | data formatting | bytes 1486848 | tf_op jit(solution)/shard_map/reshape | solution.py:48
  57.0 1.9 copy.48
  58.9 10.2 %all-to-all-start = ((f32[32,66,88]{2,1,0:T(8,128)}), f32[32,66,88]{2,1,0:T(8,128)S(1)}, u32[]{:S(2)}, u32[]{:S(2)}) async-start(f32[32,66,88]{2,1,0:T(8,128)} %copy.48), calls=%async_computation | async-start | bytes 2359296 | tf_op jit(solution)/shard_map/all_to_all | solution.py:49
  69.1 30.3 %all-to-all-done = f32[32,66,88]{2,1,0:T(8,128)S(1)} async-done(((f32[32,66,88]{2,1,0:T(8,128)}), f32[32,66,88]{2,1,0:T(8,128)S(1)}, u32[]{:S(2)}, u32[]{:S(2)}) %all-to-all-start) | async-done | bytes 743456 | tf_op jit(solution)/shard_map/all_to_all | solution.py:49
  99.7 22.5 %all-gather.9 = f32[12,66,88]{2,1,0:T(8,128)S(1)} all-gather(f32[1,66,88]{2,1,0:T(8,128)S(1)} %copy.50), channel_id=5, replica_groups=mesh['z'=12,'core'=2,'y'=8,'x'=4] {'z'}, dimensions={0}, use_global_device_ids=true | all-gather | bytes 302016 | tf_op jit(solution)/shard_map/all_gather | solution.py:28
  122.2 2.4 all-gather.4
  124.6 0.6 copy.51
  125.3 0.9 multiply_reduce_fusion
  126.2 1.4 pad_maximum_fusion.2
  127.7 1.1 broadcast_in_dim.38
  128.8 6.1 %all-to-all-start.1 = ((f32[32,66,90]{2,1,0:T(8,128)}), f32[32,66,90]{2,1,0:T(8,128)S(1)}, u32[]{:S(2)}, u32[]{:S(2)}) async-start(f32[32,66,90]{2,1,0:T(8,128)} %broadcast_in_dim.38), calls=%async_computation.1 | async-start | bytes 2359296 | tf_op jit(solution)/shard_map/all_to_all | solution.py:20
  135.0 0.6 multiply_add_fusion.2
  135.6 29.6 %all-to-all-done.1 = f32[32,66,90]{2,1,0:T(8,128)S(1)} async-done(((f32[32,66,90]{2,1,0:T(8,128)}), f32[32,66,90]{2,1,0:T(8,128)S(1)}, u32[]{:S(2)}, u32[]{:S(2)}) %all-to-all-start.1) | async-done | bytes 760352 | tf_op jit(solution)/shard_map/all_to_all | solution.py:20
  165.4 0.6 fusion.11
  167.3 1.1 fusion.4
  168.5 2.1 convert_element_type.74
  170.6 2.1 select_convert_fusion
  172.7 2.4 copy.54
  175.1 2.1 convert_element_type.78
  177.2 1.3 convolution_convert_fusion.3
  178.6 0.9 broadcast_in_dim.39
  179.4 6.5 %all-to-all-start.2 = ((bf16[32,66,88]{2,1,0:T(8,128)(2,1)}), bf16[32,66,88]{2,1,0:T(8,128)(2,1)S(1)}, u32[]{:S(2)}, u32[]{:S(2)}) async-start(bf16[32,66,88]{2,1,0:T(8,128)(2,1)} %broadcast_in_dim.39), calls=%async_computation.2 | async-start | bytes 1179648 | tf_op jit(solution)/shard_map/all_to_all | solution.py:20
  185.9 0.4 convert_element_type.76
  186.3 17.1 %all-to-all-done.2 = bf16[32,66,88]{2,1,0:T(8,128)(2,1)S(1)} async-done(((bf16[32,66,88]{2,1,0:T(8,128)(2,1)}), bf16[32,66,88]{2,1,0:T(8,128)(2,1)S(1)}, u32[]{:S(2)}, u32[]{:S(2)}) %all-to-all-start.2) | async-done | bytes 371744 | tf_op jit(solution)/shard_map/all_to_all | solution.py:20
  203.6 0.3 fusion.6
  204.0 0.9 broadcast_in_dim.40
  204.9 5.2 %all-to-all-start.3 = ((bf16[32,66,88]{2,1,0:T(8,128)(2,1)}), bf16[32,66,88]{2,1,0:T(8,128)(2,1)S(1)}, u32[]{:S(2)}, u32[]{:S(2)}) async-start(bf16[32,66,88]{2,1,0:T(8,128)(2,1)} %broadcast_in_dim.40), calls=%async_computation.3 | async-start | bytes 1179648 | tf_op jit(solution)/shard_map/all_to_all | solution.py:20
  210.4 22.6 %all-gather.11 = bf16[12,66,89]{2,1,0:T(8,128)(2,1)S(1)} all-gather(bf16[1,66,89]{2,1,0:T(8,128)(2,1)S(1)} %maximum_bitcast_fusion), channel_id=9, replica_groups=mesh['z'=12,'core'=2,'y'=8,'x'=4] {'z'}, dimensions={0}, use_global_device_ids=true | all-gather | bytes 152724 | tf_op jit(solution)/shard_map/all_gather | solution.py:28
  232.9 2.1 all-gather.8
  235.0 0.3 copy.59
  235.4 1.1 reshape.131
  236.7 1.2 convolution_convert_fusion.1
  238.0 0.9 broadcast_in_dim.43
  238.9 9.8 %all-to-all-start.4 = ((bf16[32,66,88]{2,1,0:T(8,128)(2,1)}), bf16[32,66,88]{2,1,0:T(8,128)(2,1)S(1)}, u32[]{:S(2)}, u32[]{:S(2)}) async-start(bf16[32,66,88]{2,1,0:T(8,128)(2,1)} %broadcast_in_dim.43), calls=%async_computation.4 | async-start | bytes 1179648 | tf_op jit(solution)/shard_map/all_to_all | solution.py:20
  248.7 0.9 convert_reduce_fusion
  249.5 1.0 fusion.3
  250.5 1.4 convert_element_type.87
  251.9 15.6 %all-to-all-done.4 = bf16[32,66,88]{2,1,0:T(8,128)(2,1)S(1)} async-done(((bf16[32,66,88]{2,1,0:T(8,128)(2,1)}), bf16[32,66,88]{2,1,0:T(8,128)(2,1)S(1)}, u32[]{:S(2)}, u32[]{:S(2)}) %all-to-all-start.4) | async-done | bytes 371744 | tf_op jit(solution)/shard_map/all_to_all | solution.py:20
  267.5 1.0 reshape.155
  268.5 1.3 fusion.7
  269.8 0.9 broadcast_in_dim.44
  270.7 5.3 %all-to-all-start.5 = ((bf16[32,66,88]{2,1,0:T(8,128)(2,1)}), bf16[32,66,88]{2,1,0:T(8,128)(2,1)S(1)}, u32[]{:S(2)}, u32[]{:S(2)}) async-start(bf16[32,66,88]{2,1,0:T(8,128)(2,1)} %broadcast_in_dim.44), calls=%async_computation.5 | async-start | bytes 1179648 | tf_op jit(solution)/shard_map/all_to_all | solution.py:20
  276.0 0.3 fusion
  276.3 21.0 %all-gather.10 = bf16[12,66,88]{2,1,0:T(8,128)(2,1)S(1)} all-gather(bf16[1,66,88]{2,1,0:T(8,128)(2,1)S(1)} %fusion), channel_id=7, replica_groups=mesh['z'=12,'core'=2,'y'=8,'x'=4] {'z'}, dimensions={0}, use_global_device_ids=true | all-gather | bytes 151008 | tf_op jit(solution)/shard_map/all_gather | solution.py:28
  297.2 2.1 all-gather.6
  299.3 0.3 copy.57
  299.7 0.4 reshape.129
  300.5 0.9 broadcast_in_dim.45
  301.4 9.9 %all-to-all-start.6 = ((bf16[32,66,88]{2,1,0:T(8,128)(2,1)}), bf16[32,66,88]{2,1,0:T(8,128)(2,1)S(1)}, u32[]{:S(2)}, u32[]{:S(2)}) async-start(bf16[32,66,88]{2,1,0:T(8,128)(2,1)} %broadcast_in_dim.45), calls=%async_computation.6 | async-start | bytes 1179648 | tf_op jit(solution)/shard_map/all_to_all | solution.py:20
  311.4 18.7 %all-to-all-done.6 = bf16[32,66,88]{2,1,0:T(8,128)(2,1)S(1)} async-done(((bf16[32,66,88]{2,1,0:T(8,128)(2,1)}), bf16[32,66,88]{2,1,0:T(8,128)(2,1)S(1)}, u32[]{:S(2)}, u32[]{:S(2)}) %all-to-all-start.6) | async-done | bytes 371744 | tf_op jit(solution)/shard_map/all_to_all | solution.py:20
  330.3 1.0 convolution_multiply_fusion.1
  331.4 1.0 convolution_multiply_fusion
  (25 shorter events, 2.0 us)
Async XLA Ops:
  45.3 1.0 copy-start.1
  58.9 40.5 %all-to-all-start = ((f32[32,66,88]{2,1,0:T(8,128)}), f32[32,66,88]{2,1,0:T(8,128)S(1)}, u32[]{:S(2)}, u32[]{:S(2)}) async-start(f32[32,66,88]{2,1,0:T(8,128)} %copy.48), calls=%async_computation | async-start | bytes 2359296 | tf_op jit(solution)/shard_map/all_to_all | solution.py:49
  128.8 36.4 %all-to-all-start.1 = ((f32[32,66,90]{2,1,0:T(8,128)}), f32[32,66,90]{2,1,0:T(8,128)S(1)}, u32[]{:S(2)}, u32[]{:S(2)}) async-start(f32[32,66,90]{2,1,0:T(8,128)} %broadcast_in_dim.38), calls=%async_computation.1 | async-start | bytes 2359296 | tf_op jit(solution)/shard_map/all_to_all | solution.py:20
  172.7 4.5 %copy-start = (bf16[66,2112]{1,0:T(8,128)(2,1)S(1)}, bf16[66,2112]{1,0:T(8,128)(2,1)}, u32[]{:S(2)}) copy-start(bf16[66,2112]{1,0:T(8,128)(2,1)} %convert_element_type.74) | copy-start | bytes 836356
  177.2 8.7 %copy-start.2 = (bf16[66,24,88]{2,1,0:T(8,128)(2,1)S(1)}, bf16[66,24,88]{2,1,0:T(8,128)(2,1)}, u32[]{:S(2)}) copy-start(bf16[66,24,88]{2,1,0:T(8,128)(2,1)} %get-tuple-element.10) | copy-start | bytes 836356
  179.4 24.0 %all-to-all-start.2 = ((bf16[32,66,88]{2,1,0:T(8,128)(2,1)}), bf16[32,66,88]{2,1,0:T(8,128)(2,1)S(1)}, u32[]{:S(2)}, u32[]{:S(2)}) async-start(bf16[32,66,88]{2,1,0:T(8,128)(2,1)} %broadcast_in_dim.39), calls=%async_computation.2 | async-start | bytes 1179648 | tf_op jit(solution)/shard_map/all_to_all | solution.py:20
  204.9 31.6 %all-to-all-start.3 = ((bf16[32,66,88]{2,1,0:T(8,128)(2,1)}), bf16[32,66,88]{2,1,0:T(8,128)(2,1)S(1)}, u32[]{:S(2)}, u32[]{:S(2)}) async-start(bf16[32,66,88]{2,1,0:T(8,128)(2,1)} %broadcast_in_dim.40), calls=%async_computation.3 | async-start | bytes 1179648 | tf_op jit(solution)/shard_map/all_to_all | solution.py:20
  238.9 28.6 %all-to-all-start.4 = ((bf16[32,66,88]{2,1,0:T(8,128)(2,1)}), bf16[32,66,88]{2,1,0:T(8,128)(2,1)S(1)}, u32[]{:S(2)}, u32[]{:S(2)}) async-start(bf16[32,66,88]{2,1,0:T(8,128)(2,1)} %broadcast_in_dim.43), calls=%async_computation.4 | async-start | bytes 1179648 | tf_op jit(solution)/shard_map/all_to_all | solution.py:20
  270.7 29.4 %all-to-all-start.5 = ((bf16[32,66,88]{2,1,0:T(8,128)(2,1)}), bf16[32,66,88]{2,1,0:T(8,128)(2,1)S(1)}, u32[]{:S(2)}, u32[]{:S(2)}) async-start(bf16[32,66,88]{2,1,0:T(8,128)(2,1)} %broadcast_in_dim.44), calls=%async_computation.5 | async-start | bytes 1179648 | tf_op jit(solution)/shard_map/all_to_all | solution.py:20
  301.4 28.7 %all-to-all-start.6 = ((bf16[32,66,88]{2,1,0:T(8,128)(2,1)}), bf16[32,66,88]{2,1,0:T(8,128)(2,1)S(1)}, u32[]{:S(2)}, u32[]{:S(2)}) async-start(bf16[32,66,88]{2,1,0:T(8,128)(2,1)} %broadcast_in_dim.45), calls=%async_computation.6 | async-start | bytes 1179648 | tf_op jit(solution)/shard_map/all_to_all | solution.py:20

commit v2 on v1

v2 whole, which is shorter than its diff:
```python
import functools

import jax
import jax.numpy as jnp
from jax import lax
from jax.experimental import pallas as pl
from jax.experimental.pallas import tpu as pltpu
from jax.sharding import Mesh
from jax.sharding import PartitionSpec as P

FF = 5632
FS = ("z", "core")
TP = ("y", "x")
BETA = 0.95
EPS = 1e-06
D = 2112
COLS = 88
ROWS = 72
LANES = 128
DEPTH = 12
NEAR = 6
TPS = 32
PACK = 56
SPARE = 48
KDIM = (D // COLS) * LANES
f32, bf16 = jnp.float32, jnp.bfloat16


def place(core, z):
    return ((z // NEAR) * 2 + core) * NEAR + z % NEAR


def lanes_of(rows):
    return lax.broadcasted_iota(jnp.int32, (rows, LANES), 1)


def rows_of(rows):
    return lax.broadcasted_iota(jnp.int32, (rows, LANES), 0)


def pack(block, tail=None):
    lane = lanes_of(16)
    low = block[PACK:ROWS]
    parts = [
        jnp.where(lane < COLS, block[16 * i : 16 * i + 16], pltpu.roll(low, shift, 1))
        for i, shift in enumerate((COLS, COLS - 40, COLS - 80))
    ]
    end = block[SPARE:PACK]
    if tail is not None:
        end = jnp.where(lanes_of(PACK - SPARE) < COLS, end, tail)
    return jnp.concatenate([*parts, end], axis=0)


def low_rows(packed):
    lane = lanes_of(16)
    a, b, c = (
        pltpu.roll(packed[16 * i : 16 * i + 16].astype(f32), shift, 1)
        for i, shift in enumerate((40, 80, 120))
    )
    return jnp.where(lane < 40, a, jnp.where(lane < 80, b, c))


def store_rows(target, first, value):
    at, last = first, min(first + value.shape[0], D)
    while at < last:
        block, row = divmod(at, COLS)
        count = min(COLS - row, last - at)
        start = block * LANES + row
        target[start : start + count, :] = value[at - first : at - first + count].astype(target.dtype)
        at += count


def clear_gaps(target):
    for block in range(D // COLS):
        target[block * LANES + COLS : (block + 1) * LANES, :] = jnp.zeros((LANES - COLS, LANES), target.dtype)


def unpack_columns(blocks, target, change=None):
    clear_gaps(target)
    for t in range(-(-D // ROWS)):
        packed = blocks[t]
        for first, part in ((ROWS * t, packed), (ROWS * t + PACK, low_rows(packed))):
            store_rows(target, first, change(part, first) if change else part)


def unpack_rows(blocks, targets, change):
    for core in range(2):
        for z in range(DEPTH):
            b = place(core, z)
            packed = blocks[core, z]
            for first, part in ((0, packed), (PACK, low_rows(packed))):
                for target, value in zip(targets, change(part, first, b * COLS, packed)):
                    target[first : first + part.shape[0], b * LANES : (b + 1) * LANES] = value


def poly(eye, current):
    return jnp.where(eye, 1.5 - 0.5 * current, -0.5 * current)


def dot(left, right):
    return jnp.dot(left, right, preferred_element_type=f32)


def copies(out, value):
    for i in range(out.shape[0]):
        out[i] = value


def gram_kernel(low, whole0, whole1, out, own, share):
    own[:COLS] = low[...]
    own[COLS:] = jnp.zeros((LANES - COLS, own.shape[1]), bf16)
    half = D // 2
    for h, whole in enumerate((whole0, whole1)):
        share[h * half : (h + 1) * half] = lax.dot_general(
            whole[...], own[...], (((1,), (1,)), ((), ())), preferred_element_type=f32
        )
    share[D:] = jnp.zeros((share.shape[0] - D, LANES), f32)
    filled = -(-D // ROWS)
    for t in range(filled):
        out[t] = pack(share[ROWS * t : ROWS * (t + 1)])
    for t in range(filled, TPS):
        out[t] = jnp.zeros((PACK, LANES), f32)


def total_kernel(trace, arrived, gram, out):
    total = arrived[0]
    for t in range(1, TPS):
        total += arrived[t]
    gram[...] = total
    tail = jnp.where(lanes_of(PACK) == COLS, trace[0, 0], total)
    spot = (rows_of(PACK) == SPARE) & (lanes_of(PACK) == COLS)
    copies(out, jnp.where(spot, tail, total))


def square_kernel(gram, rows, out):
    square = jnp.zeros((PACK, LANES), f32)
    trace = jnp.zeros((PACK, LANES), f32)
    free = (rows_of(PACK) >= SPARE) & (lanes_of(PACK) >= COLS)
    for core in range(2):
        for z in range(DEPTH):
            value = rows[core, z]
            square += value * value
            trace += value
    square = jnp.sum(jnp.where(free, 0.0, square), keepdims=True)
    trace = jnp.sum(jnp.where(free, trace, 0.0), keepdims=True)
    spot = rows_of(PACK) == SPARE
    value = jnp.where(spot & (lanes_of(PACK) == COLS), square, gram[...])
    copies(out, jnp.where(spot & (lanes_of(PACK) == COLS + 1), trace, value))


def first_kernel(at, rows, cols, out, poly_rows, current_rows, spectral_out, right):
    row0, col0 = at[0], at[1]
    tails = cols[0, SPARE:PACK]
    for t in range(1, TPS):
        tails += cols[t, SPARE:PACK]
    spot = rows_of(PACK - SPARE) == 0
    lane = lanes_of(PACK - SPARE)
    square = jnp.sum(jnp.where(spot & (lane == COLS), tails, 0.0), keepdims=True)
    trace = jnp.sum(jnp.where(spot & (lane == COLS + 1), tails, 0.0), keepdims=True)
    spectral = 2.0 * square / (trace + EPS)
    inverse = 1.0 / spectral
    spectral_out[...] = jnp.broadcast_to(spectral, spectral_out.shape)

    def of_cols(part, first):
        n = part.shape[0]
        eye = rows_of(n) + first == lanes_of(n) + col0
        return poly(eye, part * inverse)

    unpack_columns(cols, right, of_cols)

    def of_rows(part, first, col, packed):
        n = part.shape[0]
        eye = (rows_of(n) + (row0 + first) == lanes_of(n) + col) & (lanes_of(n) < COLS)
        current = part * inverse
        return poly(eye, current).astype(bf16), current.astype(bf16)

    unpack_rows(rows, (poly_rows, current_rows), of_rows)
    copies(out, pack(dot(poly_rows[...], right[...])).astype(bf16))


def next_poly(at, left, right):
    current = dot(left, right)
    eye = (rows_of(ROWS) + at[0] == lanes_of(ROWS) + at[1]) & (lanes_of(ROWS) < COLS)
    return poly(eye, current), jnp.sum(jnp.where(eye, current, 0.0), axis=0, keepdims=True)


def second_kernel(at, current_rows, cols, out_cols, out_rows, right):
    unpack_columns(cols, right)
    value, diag = next_poly(at, current_rows[...], right[...])
    diag = jnp.broadcast_to(diag, (PACK - SPARE, LANES))
    row = rows_of(PACK - SPARE)
    tail = jnp.where(
        row == 0,
        pltpu.roll(diag, COLS, 1),
        jnp.where(row == 1, pltpu.roll(diag, COLS - 40, 1), pltpu.roll(diag, COLS - 80, 1)),
    )
    value = pack(value, tail).astype(bf16)
    copies(out_cols, value)
    copies(out_rows, value)


def third_kernel(at, poly_rows, rows, cols, out_square, out_product, current_rows, first_rows, right):
    row0 = at[0]
    unpack_columns(cols, right)
    copies(out_product, pack(dot(poly_rows[...], right[...])).astype(bf16))

    def of_rows(part, first, col, packed):
        n = part.shape[0]
        eye = (rows_of(n) + (row0 + first) == lanes_of(n) + col) & (lanes_of(n) < COLS)
        tail = packed[SPARE:PACK].astype(f32)
        lane = lanes_of(1)
        diag = jnp.where(
            lane < 40,
            pltpu.roll(tail, 40, 1)[0:1],
            jnp.where(lane < 80, pltpu.roll(tail, 80, 1)[1:2], pltpu.roll(tail, 120, 1)[2:3]),
        )
        part = part.astype(f32)
        return part.astype(bf16), jnp.where(eye, diag, -2.0 * part).astype(bf16)

    unpack_rows(rows, (first_rows, current_rows), of_rows)
    copies(out_square, pack(dot(first_rows[...], right[...])).astype(bf16))


def fourth_kernel(at, current_rows, cols, out, right):
    unpack_columns(cols, right)
    copies(out, pack(next_poly(at, current_rows[...], right[...])[0]).astype(bf16))


def fifth_kernel(rows, cols, out, product_rows, right):
    unpack_columns(cols, right)
    unpack_rows(rows, (product_rows,), lambda part, first, col, packed: (part.astype(bf16),))
    copies(out, pack(dot(product_rows[...], right[...])).astype(bf16))


def last_kernel(cols, out):
    for t in range(-(-D // ROWS)):
        packed = cols[t]
        count = min(ROWS, D - ROWS * t)
        top = min(count, PACK)
        out[ROWS * t : ROWS * t + top, :] = packed[:top]
        if count > PACK:
            out[ROWS * t + PACK : ROWS * (t + 1), :] = low_rows(packed).astype(bf16)


def call(kernel, outs, *args, scratch=(), flops=0):
    vmem = pl.BlockSpec(memory_space=pltpu.VMEM)
    smem = pl.BlockSpec(memory_space=pltpu.SMEM)
    return pl.pallas_call(
        kernel,
        out_shape=[jax.ShapeDtypeStruct(shape, dtype) for shape, dtype in outs],
        in_specs=[smem if a.size < 8 else vmem for a in args],
        out_specs=[vmem] * len(outs),
        scratch_shapes=[pltpu.VMEM(shape, dtype) for shape, dtype in scratch],
        compiler_params=pltpu.CompilerParams(vmem_limit_bytes=24 * 2**20),
        name=kernel.__name__,
    )(*args)


def exchange(stacked, axes):
    return lax.all_to_all(stacked, axes, split_axis=0, concat_axis=0, tiled=True)


def both_cores(by_z):
    return lax.all_gather(by_z, "core")


def local(grad_gate, grad_up, moment_gate, moment_up):
    gate_next = BETA * moment_gate + grad_gate
    up_next = BETA * moment_up + grad_up
    half = gate_next.shape[1]
    low = jnp.concatenate([gate_next.astype(bf16), up_next.astype(bf16)], axis=1)
    low = jnp.pad(low, ((0, 0), (0, 3 * LANES - 2 * half)))
    trace = jnp.sum(jnp.square(low.astype(f32))).reshape(1, 1)
    by_z = lax.all_gather(low, "z")
    whole = [
        lax.all_gather(by_z[h * NEAR : (h + 1) * NEAR], "core").reshape(D // 2, -1) for h in range(2)
    ]
    z, core, t = lax.axis_index("z"), lax.axis_index("core"), lax.axis_index(TP)
    at = jnp.stack([t * ROWS, place(core, z) * COLS]).astype(jnp.int32)

    right = ((KDIM, LANES), bf16)
    left = ((ROWS, KDIM), bf16)
    to_tp, to_z = ((TPS, PACK, LANES), bf16), ((DEPTH, PACK, LANES), bf16)
    to_tp32, to_z32 = ((TPS, PACK, LANES), f32), ((DEPTH, PACK, LANES), f32)

    (shares,) = call(
        gram_kernel,
        [to_tp32],
        low,
        *whole,
        scratch=[((LANES, low.shape[1]), bf16), ((-(-D // ROWS) * ROWS, LANES), f32)],
    )
    gram, sent = call(total_kernel, [((PACK, LANES), f32), to_z32], trace, exchange(shares, TP))
    gram_rows = both_cores(exchange(sent, "z"))
    (sent,) = call(square_kernel, [to_tp32], gram, gram_rows)
    sent, poly_rows, current_rows, spectral = call(
        first_kernel,
        [to_tp, left, left, ((8, LANES), f32)],
        at,
        gram_rows,
        exchange(sent, TP),
        scratch=[right],
    )
    cols, rows = call(second_kernel, [to_tp, to_z], at, current_rows, exchange(sent, TP), scratch=[right])
    square, product, current_rows = call(
        third_kernel,
        [to_tp, to_z, left],
        at,
        poly_rows,
        both_cores(exchange(rows, "z")),
        exchange(cols, TP),
        scratch=[left, right],
    )
    (cols,) = call(fourth_kernel, [to_tp], at, current_rows, exchange(square, TP), scratch=[right])
    (cols,) = call(
        fifth_kernel,
        [to_tp],
        both_cores(exchange(product, "z")),
        exchange(cols, TP),
        scratch=[left, right],
    )
    (product,) = call(last_kernel, [((D, LANES), bf16)], exchange(cols, TP))
    over_rows = (((0,), (0,)), ((), ()))
    ortho = sum(
        lax.dot_general(
            product[h * D // 2 : (h + 1) * D // 2, :COLS], whole[h], over_rows, preferred_element_type=f32
        )
        for h in range(2)
    )
    ortho = ortho * jnp.sqrt(2.0 * FF / spectral[0, 0])
    return gate_next, up_next, ortho[:, :half], ortho[:, half : 2 * half]


def solution(mesh):
    split = Mesh(mesh.devices.reshape(DEPTH, 2, 8, 4), ("z", "core", "y", "x"))
    spec = P(FS, TP)
    return jax.shard_map(
        local, mesh=split, in_specs=(spec,) * 4, out_specs=(spec,) * 4, check_vma=False
    )
```

time: 334 us -> 275 us (0.82)
  the two profiles are of different devices: /device:TPU:8 before, /device:TPU:64 now
where the time goes in v2:
time: 275 us
  blocking collectives  158 us (57%)
  waiting for transfers between devices  75.7 us (28%)
  starting transfers between devices  23.2 us (8%)
  Pallas kernels  11.4 us (4%)
    all_to_all x5, blocking collectives, exchange(): lax.all_to_all(stacked, axes, split_axis=0, concat_axis=0, tiled=True)  113 us
    all_to_all x5, waiting for transfers between devices, exchange(): lax.all_to_all(stacked, axes, split_axis=0, concat_axis=0, tiled=True)  75.7 us
    all_gather x1, blocking collectives, local(): by_z = lax.all_gather(low, 'z')  34.1 us
    all_to_all x5, starting transfers between devices, exchange(): lax.all_to_all(stacked, axes, split_axis=0, concat_axis=0, tiled=True)  23.2 us
    pallas_call x9, Pallas kernels, call(): pl.pallas_call(kernel, out_shape=[jax.ShapeDtypeStruct(shape, dtype) for...  11.4 us
    all_gather x3, blocking collectives, both_cores(): return lax.all_gather(by_z, 'core')  6.52 us
  transfers between devices with their start and end apart: 5, of which 5 were waited for; matrix products, arithmetic and copies ran while one was open for 0% of the time, Pallas kernels for 1%

profile of v2, /device:TPU:64, one launch (start us, length us, event | category | flops | bytes accessed | tf_op | source)
XLA Modules:
  0.0 274.6 jit_solution(16106017003919367045)
XLA Ops:
  0.6 1.7 fusion.8
  2.3 0.7 multiply_reduce_fusion
  3.0 34.1 %all-gather = bf16[1056,384]{1,0:T(8,128)(2,1)S(1)} all-gather(bf16[88,384]{1,0:T(8,128)(2,1)S(1)} %get-tuple-element.27.low), channel_id=2, replica_groups=mesh['z'=12,'core'=2,'y'=8,'x'=4] {'z'}, dimensions={0}, use_global_device_ids=true | all-gather | bytes 878592 | tf_op jit(solution)/shard_map/all_gather | solution.py:274
  37.2 0.1 fusion.10
  37.3 2.4 all-gather.1
  39.7 2.4 all-gather.2
  42.0 0.7 gram_kernel.1
  42.7 35.3 %all_to_all.50.arrived = f32[32,56,128]{2,1,0:T(8,128)S(1)} all-to-all(f32[32,56,128]{2,1,0:T(8,128)S(1)} %gram_kernel.1), channel_id=1, replica_groups=mesh['z'=12,'core'=2,'y'=8,'x'=4] {'y','x'}, dimensions={0} | all-to-all | bytes 1835008 | tf_op jit(solution)/shard_map/all_to_all | solution.py:260
  78.0 0.7 total_kernel.1
  78.7 22.4 %all_to_all.51 = f32[12,56,128]{2,1,0:T(8,128)S(1)} all-to-all(f32[12,56,128]{2,1,0:T(8,128)S(1)} %get-tuple-element.15), channel_id=1, replica_groups=mesh['z'=12,'core'=2,'y'=8,'x'=4] {'z'}, dimensions={0} | all-to-all | bytes 688128 | tf_op jit(solution)/shard_map/all_to_all | solution.py:260
  101.2 2.3 all-gather.3
  103.5 1.1 square_kernel.1
  104.6 6.2 %all-to-all-start.2 = ((f32[32,56,128]{2,1,0:T(8,128)}), f32[32,56,128]{2,1,0:T(8,128)S(1)}, u32[]{:S(2)}, u32[]{:S(2)}) async-start(f32[32,56,128]{2,1,0:T(8,128)} %square_kernel.1), calls=%async_computation.2 | async-start | bytes 1835008 | tf_op jit(solution)/shard_map/all_to_all | solution.py:260
  110.8 0.1 pad_add_fusion.at
  110.9 25.5 %all-to-all-done.2.cols = f32[32,56,128]{2,1,0:T(8,128)S(1)} async-done(((f32[32,56,128]{2,1,0:T(8,128)}), f32[32,56,128]{2,1,0:T(8,128)S(1)}, u32[]{:S(2)}, u32[]{:S(2)}) %all-to-all-start.2) | async-done | bytes 917536 | tf_op jit(solution)/shard_map/all_to_all | solution.py:260
  136.4 1.7 first_kernel.1
  138.1 0.0 copy-start
  138.1 21.0 %all_to_all.52.cols = bf16[32,56,128]{2,1,0:T(8,128)(2,1)S(1)} all-to-all(bf16[32,56,128]{2,1,0:T(8,128)(2,1)S(1)} %get-tuple-element.19), channel_id=1, replica_groups=mesh['z'=12,'core'=2,'y'=8,'x'=4] {'y','x'}, dimensions={0} | all-to-all | bytes 917504 | tf_op jit(solution)/shard_map/all_to_all | solution.py:260
  159.2 0.0 copy-done
  159.2 1.9 second_kernel.1
  161.0 14.6 %all_to_all.53 = bf16[12,56,128]{2,1,0:T(8,128)(2,1)S(1)} all-to-all(bf16[12,56,128]{2,1,0:T(8,128)(2,1)S(1)} %get-tuple-element.20), channel_id=1, replica_groups=mesh['z'=12,'core'=2,'y'=8,'x'=4] {'z'}, dimensions={0} | all-to-all | bytes 344064 | tf_op jit(solution)/shard_map/all_to_all | solution.py:260
  175.6 4.6 %all-to-all-start.5 = ((bf16[32,56,128]{2,1,0:T(8,128)(2,1)}), bf16[32,56,128]{2,1,0:T(8,128)(2,1)S(1)}, u32[]{:S(2)}, u32[]{:S(2)}) async-start(bf16[32,56,128]{2,1,0:T(8,128)(2,1)} %get-tuple-element.21), calls=%async_computation.5 | async-start | bytes 917504 | tf_op jit(solution)/shard_map/all_to_all | solution.py:260
  180.2 0.0 copy-start.1
  180.2 2.2 all-gather.4
  182.4 13.3 %all-to-all-done.5.cols = bf16[32,56,128]{2,1,0:T(8,128)(2,1)S(1)} async-done(((bf16[32,56,128]{2,1,0:T(8,128)(2,1)}), bf16[32,56,128]{2,1,0:T(8,128)(2,1)S(1)}, u32[]{:S(2)}, u32[]{:S(2)}) %all-to-all-start.5) | async-done | bytes 458784 | tf_op jit(solution)/shard_map/all_to_all | solution.py:260
  195.7 0.0 copy-done.1
  195.7 1.9 third_kernel.1
  197.6 19.4 %all_to_all.54.cols = bf16[32,56,128]{2,1,0:T(8,128)(2,1)S(1)} all-to-all(bf16[32,56,128]{2,1,0:T(8,128)(2,1)S(1)} %get-tuple-element.24), channel_id=1, replica_groups=mesh['z'=12,'core'=2,'y'=8,'x'=4] {'y','x'}, dimensions={0} | all-to-all | bytes 917504 | tf_op jit(solution)/shard_map/all_to_all | solution.py:260
  217.0 3.8 %all-to-all-start.6 = ((bf16[12,56,128]{2,1,0:T(8,128)(2,1)}), bf16[12,56,128]{2,1,0:T(8,128)(2,1)S(1)}, u32[]{:S(2)}, u32[]{:S(2)}) async-start(bf16[12,56,128]{2,1,0:T(8,128)(2,1)} %get-tuple-element.22), calls=%async_computation.6 | async-start | bytes 344064 | tf_op jit(solution)/shard_map/all_to_all | solution.py:260
  220.8 1.8 fourth_kernel.1
  222.6 9.6 %all-to-all-done.6 = bf16[12,56,128]{2,1,0:T(8,128)(2,1)S(1)} async-done(((bf16[12,56,128]{2,1,0:T(8,128)(2,1)}), bf16[12,56,128]{2,1,0:T(8,128)(2,1)S(1)}, u32[]{:S(2)}, u32[]{:S(2)}) %all-to-all-start.6) | async-done | bytes 172064 | tf_op jit(solution)/shard_map/all_to_all | solution.py:260
  232.2 4.5 %all-to-all-start.8 = ((bf16[32,56,128]{2,1,0:T(8,128)(2,1)}), bf16[32,56,128]{2,1,0:T(8,128)(2,1)S(1)}, u32[]{:S(2)}, u32[]{:S(2)}) async-start(bf16[32,56,128]{2,1,0:T(8,128)(2,1)} %fourth_kernel.1), calls=%async_computation.8 | async-start | bytes 917504 | tf_op jit(solution)/shard_map/all_to_all | solution.py:260
  236.6 2.1 all-gather.5
  238.7 13.3 %all-to-all-done.8.cols = bf16[32,56,128]{2,1,0:T(8,128)(2,1)S(1)} async-done(((bf16[32,56,128]{2,1,0:T(8,128)(2,1)}), bf16[32,56,128]{2,1,0:T(8,128)(2,1)S(1)}, u32[]{:S(2)}, u32[]{:S(2)}) %all-to-all-start.8) | async-done | bytes 458784 | tf_op jit(solution)/shard_map/all_to_all | solution.py:260
  252.0 1.4 fifth_kernel.1
  253.4 4.2 %all-to-all-start.9 = ((bf16[32,56,128]{2,1,0:T(8,128)(2,1)}), bf16[32,56,128]{2,1,0:T(8,128)(2,1)S(1)}, u32[]{:S(2)}, u32[]{:S(2)}) async-start(bf16[32,56,128]{2,1,0:T(8,128)(2,1)} %fifth_kernel.1), calls=%async_computation.9 | async-start | bytes 917504 | tf_op jit(solution)/shard_map/all_to_all | solution.py:260
  257.6 0.5 slice.25
  258.8 14.1 %all-to-all-done.9.cols = bf16[32,56,128]{2,1,0:T(8,128)(2,1)S(1)} async-done(((bf16[32,56,128]{2,1,0:T(8,128)(2,1)}), bf16[32,56,128]{2,1,0:T(8,128)(2,1)S(1)}, u32[]{:S(2)}, u32[]{:S(2)}) %all-to-all-start.9) | async-done | bytes 458784 | tf_op jit(solution)/shard_map/all_to_all | solution.py:260
  273.0 0.2 last_kernel.1
  273.2 0.3 fusion.2
  273.5 0.3 fusion
  273.8 0.7 fusion.11
Async XLA Ops:
  104.6 31.8 %all-to-all-start.2 = ((f32[32,56,128]{2,1,0:T(8,128)}), f32[32,56,128]{2,1,0:T(8,128)S(1)}, u32[]{:S(2)}, u32[]{:S(2)}) async-start(f32[32,56,128]{2,1,0:T(8,128)} %square_kernel.1), calls=%async_computation.2 | async-start | bytes 1835008 | tf_op jit(solution)/shard_map/all_to_all | solution.py:260
  138.1 21.1 %copy-start = (bf16[72,3072]{1,0:T(8,128)(2,1)}, bf16[72,3072]{1,0:T(8,128)(2,1)S(1)}, u32[]{:S(2)}) copy-start(bf16[72,3072]{1,0:T(8,128)(2,1)S(1)} %get-tuple-element.17.poly_rows) | copy-start | bytes 1327108
  175.6 20.0 %all-to-all-start.5 = ((bf16[32,56,128]{2,1,0:T(8,128)(2,1)}), bf16[32,56,128]{2,1,0:T(8,128)(2,1)S(1)}, u32[]{:S(2)}, u32[]{:S(2)}) async-start(bf16[32,56,128]{2,1,0:T(8,128)(2,1)} %get-tuple-element.21), calls=%async_computation.5 | async-start | bytes 917504 | tf_op jit(solution)/shard_map/all_to_all | solution.py:260
  180.2 15.4 %copy-start.1 = (bf16[72,3072]{1,0:T(8,128)(2,1)S(1)}, bf16[72,3072]{1,0:T(8,128)(2,1)}, u32[]{:S(2)}) copy-start(bf16[72,3072]{1,0:T(8,128)(2,1)} %copy-done) | copy-start | bytes 1327108
  217.0 15.2 %all-to-all-start.6 = ((bf16[12,56,128]{2,1,0:T(8,128)(2,1)}), bf16[12,56,128]{2,1,0:T(8,128)(2,1)S(1)}, u32[]{:S(2)}, u32[]{:S(2)}) async-start(bf16[12,56,128]{2,1,0:T(8,128)(2,1)} %get-tuple-element.22), calls=%async_computation.6 | async-start | bytes 344064 | tf_op jit(solution)/shard_map/all_to_all | solution.py:260
  232.2 19.8 %all-to-all-start.8 = ((bf16[32,56,128]{2,1,0:T(8,128)(2,1)}), bf16[32,56,128]{2,1,0:T(8,128)(2,1)S(1)}, u32[]{:S(2)}, u32[]{:S(2)}) async-start(bf16[32,56,128]{2,1,0:T(8,128)(2,1)} %fourth_kernel.1), calls=%async_computation.8 | async-start | bytes 917504 | tf_op jit(solution)/shard_map/all_to_all | solution.py:260
  253.4 19.6 %all-to-all-start.9 = ((bf16[32,56,128]{2,1,0:T(8,128)(2,1)}), bf16[32,56,128]{2,1,0:T(8,128)(2,1)S(1)}, u32[]{:S(2)}, u32[]{:S(2)}) async-start(bf16[32,56,128]{2,1,0:T(8,128)(2,1)} %fifth_kernel.1), calls=%async_computation.9 | async-start | bytes 917504 | tf_op jit(solution)/shard_map/all_to_all | solution.py:260

commit v3 on v2

v3 whole, which is shorter than its diff:
```python
import jax
import jax.numpy as jnp
from jax import lax
from jax.experimental import pallas as pl
from jax.experimental.pallas import tpu as pltpu
from jax.sharding import Mesh
from jax.sharding import PartitionSpec as P

FF = 5632
FS = ("z", "core")
TP = ("y", "x")
BETA = 0.95
EPS = 1e-06
LANES = 128
D = 2112
COLS = 88
BLOCKS = D // COLS
DEPTH = 12
NEAR = 6
TPS = 32
MAIN = 64
SHARED = TPS * MAIN
ROWS = MAIN + 8
PIECE = COLS // 4
SENT = 48
WIDE = 56
FREE = 96
SPARE = 48
KDIM = BLOCKS * LANES
f32, bf16 = jnp.float32, jnp.bfloat16


def place(core, z):
    return ((z // NEAR) * 2 + core) * NEAR + z % NEAR


def lanes_of(rows):
    return lax.broadcasted_iota(jnp.int32, (rows, LANES), 1)


def rows_of(rows):
    return lax.broadcasted_iota(jnp.int32, (rows, LANES), 0)


def folded(block, low):
    lane = lanes_of(16)
    return [
        jnp.where(lane < COLS, block[16 * i : 16 * i + 16], pltpu.roll(low, shift, 1))
        for i, shift in enumerate((COLS, COLS - 40, COLS - 80))
    ]


def unfolded(packed):
    lane = lanes_of(16)
    a, b, c = (
        pltpu.roll(packed[16 * i : 16 * i + 16].astype(f32), shift, 1)
        for i, shift in enumerate((40, 80, 120))
    )
    return jnp.where(lane < 40, a, jnp.where(lane < 80, b, c))


def pack_tp(main, shared, shift, tail=None):
    a, b, c = folded(main, main[48:64])
    top = jnp.where(lanes_of(8) < FREE, c[:8], pltpu.roll(shared, shift, 1))
    end = c[8:] if tail is None else jnp.where(lanes_of(8) < FREE, c[8:], tail)
    return jnp.concatenate([a, b, top, end], axis=0)


def pack_z(block, tail=None):
    end = block[SPARE:WIDE]
    if tail is not None:
        end = jnp.where(lanes_of(WIDE - SPARE) < COLS, end, tail)
    return jnp.concatenate([*folded(block, block[WIDE:ROWS]), end], axis=0)


def spread(row):
    row = jnp.broadcast_to(row, (WIDE - SPARE, LANES))
    at = rows_of(WIDE - SPARE)
    return jnp.where(
        at == 0,
        pltpu.roll(row, COLS, 1),
        jnp.where(at == 1, pltpu.roll(row, COLS - 40, 1), pltpu.roll(row, COLS - 80, 1)),
    )


def gathered(packed):
    tail = packed[SPARE:WIDE].astype(f32)
    lane = lanes_of(1)
    return jnp.where(
        lane < 40,
        pltpu.roll(tail, 40, 1)[0:1],
        jnp.where(lane < 80, pltpu.roll(tail, 80, 1)[1:2], pltpu.roll(tail, 120, 1)[2:3]),
    )


def store_rows(target, first, value):
    at, last = first, first + value.shape[0]
    while at < last:
        block, row = divmod(at, COLS)
        count = min(COLS - row, last - at)
        start = block * LANES + row
        target[start : start + count, :] = value[at - first : at - first + count].astype(target.dtype)
        at += count


def unpack_columns(blocks, target, change=lambda part, first: part):
    for block in range(BLOCKS):
        target[block * LANES + COLS : (block + 1) * LANES, :] = jnp.zeros((LANES - COLS, LANES), target.dtype)
    for t in range(TPS):
        packed = blocks[t]
        store_rows(target, MAIN * t, change(packed, MAIN * t))
        store_rows(target, MAIN * t + 48, change(unfolded(packed), MAIN * t + 48))
    lane = lanes_of(8)
    for group in range(TPS // 4):
        parts = [
            pltpu.roll(blocks[4 * group + q, 32:40].astype(f32), PIECE * q + LANES - FREE, 1) for q in range(4)
        ]
        value = parts[3]
        for q in (2, 1, 0):
            value = jnp.where(lane < PIECE * (q + 1), parts[q], value)
        store_rows(target, SHARED + 8 * group, change(value, SHARED + 8 * group))


def unpack_rows(blocks, at, targets, change):
    for core in range(2):
        for z in range(DEPTH):
            b = place(core, z)
            packed = blocks[core, z]
            low = unfolded(packed)
            for first, part in ((0, packed), (WIDE, low[:8]), (MAIN, low[8:])):
                for target, value in zip(targets, change(part, first, b * COLS, packed)):
                    target[first : first + part.shape[0], b * LANES : (b + 1) * LANES] = value


def eye_of(at, first, count, col):
    row = at[0] if first < MAIN else at[1]
    return (rows_of(count) + (row + first) == lanes_of(count) + col) & (lanes_of(count) < COLS)


def own_eye(at):
    return jnp.concatenate([eye_of(at, 0, MAIN, at[2]), eye_of(at, MAIN, ROWS - MAIN, at[2])], axis=0)


def poly(eye, current):
    return jnp.where(eye, 1.5 - 0.5 * current, -0.5 * current)


def dot(left, right):
    return jnp.dot(left, right, preferred_element_type=f32)


def copies(out, value):
    value = value.astype(out.dtype)
    for i in range(out.shape[0]):
        out[i] = value


def send_tp(at, out, block, tail=None):
    copies(out, pack_tp(block[:MAIN], block[MAIN:ROWS], at[3], tail))


def gram_kernel(at, low, whole0, whole1, out, trace, own, share):
    mine = low[...]
    trace[...] = jnp.broadcast_to(jnp.sum(jnp.square(mine.astype(f32)), keepdims=True), trace.shape)
    own[:COLS] = mine
    own[COLS:] = jnp.zeros((LANES - COLS, own.shape[1]), bf16)
    half = D // 2
    for h, whole in enumerate((whole0, whole1)):
        share[h * half : (h + 1) * half] = lax.dot_general(
            whole[...], own[...], (((1,), (1,)), ((), ())), preferred_element_type=f32
        )
    for t in range(TPS):
        group, q = divmod(t, 4)
        shared = share[SHARED + 8 * group : SHARED + 8 * group + 8]
        out[t] = pack_tp(share[MAIN * t : MAIN * (t + 1)], shared, (FREE - PIECE * q) % LANES)


def total_kernel(trace, arrived, out):
    total = arrived[0]
    for t in range(1, TPS):
        total += arrived[t]
    spot = (rows_of(SENT) == SENT - 1) & (lanes_of(SENT) == FREE)
    copies(out, jnp.where(spot, trace[0:1], total))


def square_kernel(at, cols, out, whole):
    unpack_columns(cols, whole)
    ends = cols[0, SENT - 8 :]
    for t in range(1, TPS):
        ends += cols[t, SENT - 8 :]
    trace = jnp.sum(jnp.where((rows_of(8) == 7) & (lanes_of(8) == FREE), ends, 0.0), keepdims=True)
    square = jnp.zeros((LANES, LANES), f32)
    for block in range(BLOCKS):
        value = whole[block * LANES : (block + 1) * LANES, :]
        square += value * value
    square = jnp.sum(jnp.where(lanes_of(LANES) < COLS, square, 0.0), keepdims=True)

    def rows_at(first, count, target):
        for i in range(0, count, 8):
            block = (first + i) // COLS
            start = pl.multiple_of(block * LANES + (first + i) - block * COLS, 8)
            target.append(whole[pl.ds(start, 8), :])
        return target

    value = jnp.concatenate(rows_at(at[1] + MAIN, 8, rows_at(at[0], MAIN, [])), axis=0)
    row, lane = rows_of(WIDE - SPARE), lanes_of(WIDE - SPARE)
    tail = jnp.where((row == 0) & (lane == COLS), square, jnp.where((row == 0) & (lane == COLS + 1), trace, 0.0))
    copies(out, pack_z(value, tail))


def first_kernel(at, rows, cols, out, poly_rows, current_rows, spectral_out, right):
    tails = jnp.zeros((WIDE - SPARE, LANES), f32)
    for core in range(2):
        for z in range(DEPTH):
            tails += rows[core, z, SPARE:WIDE]
    spot = rows_of(WIDE - SPARE) == 0
    lane = lanes_of(WIDE - SPARE)
    square = jnp.sum(jnp.where(spot & (lane == COLS), tails, 0.0), keepdims=True)
    trace = jnp.sum(jnp.where(spot & (lane == COLS + 1), tails, 0.0), keepdims=True)
    spectral = 2.0 * square / (trace + EPS)
    inverse = 1.0 / spectral
    spectral_out[...] = jnp.broadcast_to(spectral, spectral_out.shape)

    def of_cols(part, first):
        n = part.shape[0]
        eye = rows_of(n) + first == lanes_of(n) + at[2]
        return poly(eye, part * inverse)

    unpack_columns(cols, right, of_cols)

    def of_rows(part, first, col, packed):
        current = part * inverse
        return (
            poly(eye_of(at, first, part.shape[0], col), current).astype(bf16),
            current.astype(bf16),
        )

    unpack_rows(rows, at, (poly_rows, current_rows), of_rows)
    send_tp(at, out, dot(poly_rows[...], right[...]))


def next_poly(at, current):
    eye = own_eye(at)
    return poly(eye, current), jnp.sum(jnp.where(eye, current, 0.0), axis=0, keepdims=True)


def second_kernel(at, current_rows, cols, out_cols, out_rows, right):
    unpack_columns(cols, right)
    value, diag = next_poly(at, dot(current_rows[...], right[...]))
    send_tp(at, out_cols, value)
    copies(out_rows, pack_z(value, spread(diag)))


def third_kernel(at, poly_rows, rows, cols, out_square, out_product, current_rows, first_rows, right):
    unpack_columns(cols, right)
    copies(out_product, pack_z(dot(poly_rows[...], right[...])))

    def of_rows(part, first, col, packed):
        eye = eye_of(at, first, part.shape[0], col)
        part = part.astype(f32)
        return part.astype(bf16), jnp.where(eye, gathered(packed), -2.0 * part).astype(bf16)

    unpack_rows(rows, at, (first_rows, current_rows), of_rows)
    send_tp(at, out_square, dot(first_rows[...], right[...]))


def fourth_kernel(at, current_rows, cols, out, right):
    unpack_columns(cols, right)
    send_tp(at, out, next_poly(at, dot(current_rows[...], right[...]))[0])


def fifth_kernel(at, rows, cols, out, product_rows, right):
    unpack_columns(cols, right)
    unpack_rows(rows, at, (product_rows,), lambda part, first, col, packed: (part.astype(bf16),))
    send_tp(at, out, dot(product_rows[...], right[...]))


def last_kernel(cols, out):
    unpack_columns(cols, out)


def call(kernel, outs, *args, scratch=()):
    vmem = pl.BlockSpec(memory_space=pltpu.VMEM)
    smem = pl.BlockSpec(memory_space=pltpu.SMEM)
    return pl.pallas_call(
        kernel,
        out_shape=[jax.ShapeDtypeStruct(shape, dtype) for shape, dtype in outs],
        in_specs=[smem if a.dtype == jnp.int32 else vmem for a in args],
        out_specs=[vmem] * len(outs),
        scratch_shapes=[pltpu.VMEM(shape, dtype) for shape, dtype in scratch],
        compiler_params=pltpu.CompilerParams(vmem_limit_bytes=24 * 2**20),
        name=kernel.__name__,
    )(*args)


def exchange(stacked, axes):
    return lax.all_to_all(stacked, axes, split_axis=0, concat_axis=0, tiled=True)


def both_cores(by_z):
    return lax.all_gather(by_z, "core")


def local(grad_gate, grad_up, moment_gate, moment_up):
    gate_next = BETA * moment_gate + grad_gate
    up_next = BETA * moment_up + grad_up
    half = gate_next.shape[1]
    low = jnp.concatenate([gate_next.astype(bf16), up_next.astype(bf16)], axis=1)
    low = jnp.pad(low, ((0, 0), (0, 3 * LANES - 2 * half)))
    z, core, t = lax.axis_index("z"), lax.axis_index("core"), lax.axis_index(TP)
    own = place(core, z)
    at = jnp.stack(
        [
            t * MAIN,
            SHARED + 8 * (t // 4) - MAIN,
            own * COLS,
            (FREE - PIECE * (t % 4)) % LANES,
            own * LANES,
        ]
    ).astype(jnp.int32)
    low, at = lax.optimization_barrier((low, at))
    by_z = lax.all_gather(low, "z")
    whole = [
        lax.all_gather(by_z[h * NEAR : (h + 1) * NEAR], "core").reshape(D // 2, -1) for h in range(2)
    ]

    right = ((KDIM, LANES), bf16)
    left = ((ROWS, KDIM), bf16)
    block = ((ROWS, LANES), f32)
    to_tp, to_z = ((TPS, SENT, LANES), bf16), ((DEPTH, WIDE, LANES), bf16)
    to_tp32, to_z32 = (to_tp[0], f32), (to_z[0], f32)

    shares, trace = call(
        gram_kernel,
        [to_tp32, ((8, LANES), f32)],
        at,
        low,
        *whole,
        scratch=[((LANES, low.shape[1]), bf16), ((D, LANES), f32)],
    )
    (cols,) = call(total_kernel, [to_tp32], trace, exchange(shares, TP))
    cols = exchange(cols, TP)
    (rows,) = call(square_kernel, [to_z32], at, cols, scratch=[(right[0], f32)])
    rows = both_cores(exchange(rows, "z"))
    sent, poly_rows, current_rows, spectral = call(
        first_kernel, [to_tp, left, left, ((8, LANES), f32)], at, rows, cols, scratch=[right]
    )
    cols, rows = call(second_kernel, [to_tp, to_z], at, current_rows, exchange(sent, TP), scratch=[right])
    cols = exchange(cols, TP)
    rows = both_cores(exchange(rows, "z"))
    square, product, current_rows = call(
        third_kernel, [to_tp, to_z, left], at, poly_rows, rows, cols, scratch=[left, right]
    )
    cols = exchange(square, TP)
    rows = both_cores(exchange(product, "z"))
    (cols,) = call(fourth_kernel, [to_tp], at, current_rows, cols, scratch=[right])
    cols = exchange(cols, TP)
    (cols,) = call(fifth_kernel, [to_tp], at, rows, cols, scratch=[left, right])
    (product,) = call(last_kernel, [right], exchange(cols, TP))

    whole_product = product.reshape(BLOCKS, LANES, LANES)[:, :COLS].reshape(2, D // 2, LANES)
    over_rows = (((0,), (0,)), ((), ()))
    ortho = sum(
        lax.dot_general(whole_product[h, :, :COLS], whole[h], over_rows, preferred_element_type=f32)
        for h in range(2)
    )
    ortho = ortho * jnp.sqrt(2.0 * FF / spectral[0, 0])
    return gate_next, up_next, ortho[:, :half], ortho[:, half : 2 * half]


def solution(mesh):
    split = Mesh(mesh.devices.reshape(DEPTH, 2, 8, 4), ("z", "core", "y", "x"))
    spec = P(FS, TP)
    return jax.shard_map(
        local, mesh=split, in_specs=(spec,) * 4, out_specs=(spec,) * 4, check_vma=False
    )
```

time: 275 us -> 267 us (0.971)
  waiting for transfers between devices: 75.7 us -> 48.8 us
  blocking collectives: 158 us -> 182 us
  starting transfers between devices: 23.2 us -> 17.1 us
    all_to_all x5 -> x4, waiting for transfers between devices: 75.7 us -> 48.8 us  [exchange(): lax.all_to_all(stacked, axes, split_axis=0, concat_axis=0, tiled=True)]
    all_to_all x5 -> x6, blocking collectives: 113 us -> 137 us  [exchange(): lax.all_to_all(stacked, axes, split_axis=0, concat_axis=0, tiled=True)]
    all_to_all x5 -> x4, starting transfers between devices: 23.2 us -> 17.1 us  [exchange(): lax.all_to_all(stacked, axes, split_axis=0, concat_axis=0, tiled=True)]
  transfers between devices with their start and end apart: 5 -> 4, of which waited for: 5 -> 4; matrix products, arithmetic and copies ran while one was open for 0% -> 0% of each run, Pallas kernels for 1% -> 1%
where the time goes in v3:
time: 267 us; the launch traced here: 266 us
  blocking collectives  182 us (68%)
  waiting for transfers between devices  48.8 us (18%)
  starting transfers between devices  17.1 us (6%)
  Pallas kernels  11.8 us (4%)
    all_to_all x6, blocking collectives, exchange(): lax.all_to_all(stacked, axes, split_axis=0, concat_axis=0, tiled=True)  137 us
    all_to_all x4, waiting for transfers between devices, exchange(): lax.all_to_all(stacked, axes, split_axis=0, concat_axis=0, tiled=True)  48.8 us
    all_gather x1, blocking collectives, local(): by_z = lax.all_gather(low, 'z')  34.1 us
    all_to_all x4, starting transfers between devices, exchange(): lax.all_to_all(stacked, axes, split_axis=0, concat_axis=0, tiled=True)  17.1 us
    pallas_call x9, Pallas kernels, call(): pl.pallas_call(kernel, out_shape=[jax.ShapeDtypeStruct(shape, dtype) for...  11.8 us
    all_gather x3, blocking collectives, both_cores(): return lax.all_gather(by_z, 'core')  6.39 us
  transfers between devices with their start and end apart: 4, of which 4 were waited for; matrix products, arithmetic and copies ran while one was open for 0% of the time, Pallas kernels for 1%

profile of v3, /device:TPU:64, one launch (start us, length us, event | category | flops | bytes accessed | tf_op | source)
XLA Modules:
  0.0 265.7 jit_solution(8958705179363176541)
XLA Ops:
  0.6 0.0 copy-start
  0.7 0.8 copy-done
  1.5 1.7 fusion.5
  3.2 0.1 fusion.4.low
  3.3 0.1 stack.23.at
  3.4 34.1 %all-gather = bf16[1056,384]{1,0:T(8,128)(2,1)S(1)} all-gather(bf16[88,384]{1,0:T(8,128)(2,1)S(1)} %fusion.4.low), channel_id=2, replica_groups=mesh['z'=12,'core'=2,'y'=8,'x'=4] {'z'}, dimensions={0}, use_global_device_ids=true | all-gather | bytes 878592 | tf_op jit(solution)/shard_map/all_gather | solution.py:322
  37.5 0.1 fusion.7
  37.6 2.4 all-gather.1
  40.0 2.4 all-gather.2
  42.4 1.2 gram_kernel.1
  43.6 33.1 %all_to_all.50.arrived = f32[32,48,128]{2,1,0:T(8,128)S(1)} all-to-all(f32[32,48,128]{2,1,0:T(8,128)S(1)} %get-tuple-element.20), channel_id=1, replica_groups=mesh['z'=12,'core'=2,'y'=8,'x'=4] {'y','x'}, dimensions={0} | all-to-all | bytes 1572864 | tf_op jit(solution)/shard_map/all_to_all | solution.py:297
  76.8 0.1 total_kernel.1
  76.8 26.5 %all_to_all.51.cols = f32[32,48,128]{2,1,0:T(8,128)S(1)} all-to-all(f32[32,48,128]{2,1,0:T(8,128)S(1)} %total_kernel.1), channel_id=1, replica_groups=mesh['z'=12,'core'=2,'y'=8,'x'=4] {'y','x'}, dimensions={0} | all-to-all | bytes 1572864 | tf_op jit(solution)/shard_map/all_to_all | solution.py:297
  103.3 1.0 square_kernel.1
  104.4 21.6 %all_to_all.52 = f32[12,56,128]{2,1,0:T(8,128)S(1)} all-to-all(f32[12,56,128]{2,1,0:T(8,128)S(1)} %square_kernel.1), channel_id=1, replica_groups=mesh['z'=12,'core'=2,'y'=8,'x'=4] {'z'}, dimensions={0} | all-to-all | bytes 688128 | tf_op jit(solution)/shard_map/all_to_all | solution.py:297
  126.0 2.3 all-gather.3
  128.3 1.8 first_kernel.1
  130.0 22.0 %all_to_all.53.cols = bf16[32,48,128]{2,1,0:T(8,128)(2,1)S(1)} all-to-all(bf16[32,48,128]{2,1,0:T(8,128)(2,1)S(1)} %get-tuple-element.23), channel_id=1, replica_groups=mesh['z'=12,'core'=2,'y'=8,'x'=4] {'y','x'}, dimensions={0} | all-to-all | bytes 786432 | tf_op jit(solution)/shard_map/all_to_all | solution.py:297
  152.0 1.8 second_kernel.1
  153.8 14.6 %all_to_all.54 = bf16[12,56,128]{2,1,0:T(8,128)(2,1)S(1)} all-to-all(bf16[12,56,128]{2,1,0:T(8,128)(2,1)S(1)} %get-tuple-element.24), channel_id=1, replica_groups=mesh['z'=12,'core'=2,'y'=8,'x'=4] {'z'}, dimensions={0} | all-to-all | bytes 344064 | tf_op jit(solution)/shard_map/all_to_all | solution.py:297
  168.4 4.9 %all-to-all-start.5 = ((bf16[32,48,128]{2,1,0:T(8,128)(2,1)}), bf16[32,48,128]{2,1,0:T(8,128)(2,1)S(1)}, u32[]{:S(2)}, u32[]{:S(2)}) async-start(bf16[32,48,128]{2,1,0:T(8,128)(2,1)} %get-tuple-element.25), calls=%async_computation.5 | async-start | bytes 786432 | tf_op jit(solution)/shard_map/all_to_all | solution.py:297
  173.4 2.1 all-gather.4
  175.4 13.0 %all-to-all-done.5.cols = bf16[32,48,128]{2,1,0:T(8,128)(2,1)S(1)} async-done(((bf16[32,48,128]{2,1,0:T(8,128)(2,1)}), bf16[32,48,128]{2,1,0:T(8,128)(2,1)S(1)}, u32[]{:S(2)}, u32[]{:S(2)}) %all-to-all-start.5) | async-done | bytes 393248 | tf_op jit(solution)/shard_map/all_to_all | solution.py:297
  188.5 1.9 third_kernel.1
  190.4 18.7 %all_to_all.55.cols = bf16[32,48,128]{2,1,0:T(8,128)(2,1)S(1)} all-to-all(bf16[32,48,128]{2,1,0:T(8,128)(2,1)S(1)} %get-tuple-element.28), channel_id=1, replica_groups=mesh['z'=12,'core'=2,'y'=8,'x'=4] {'y','x'}, dimensions={0} | all-to-all | bytes 786432 | tf_op jit(solution)/shard_map/all_to_all | solution.py:297
  209.1 3.4 %all-to-all-start.6 = ((bf16[12,56,128]{2,1,0:T(8,128)(2,1)}), bf16[12,56,128]{2,1,0:T(8,128)(2,1)S(1)}, u32[]{:S(2)}, u32[]{:S(2)}) async-start(bf16[12,56,128]{2,1,0:T(8,128)(2,1)} %get-tuple-element.26), calls=%async_computation.6 | async-start | bytes 344064 | tf_op jit(solution)/shard_map/all_to_all | solution.py:297
  212.5 1.8 fourth_kernel.1
  214.3 9.4 %all-to-all-done.6 = bf16[12,56,128]{2,1,0:T(8,128)(2,1)S(1)} async-done(((bf16[12,56,128]{2,1,0:T(8,128)(2,1)}), bf16[12,56,128]{2,1,0:T(8,128)(2,1)S(1)}, u32[]{:S(2)}, u32[]{:S(2)}) %all-to-all-start.6) | async-done | bytes 172064 | tf_op jit(solution)/shard_map/all_to_all | solution.py:297
  223.8 4.5 %all-to-all-start.8 = ((bf16[32,48,128]{2,1,0:T(8,128)(2,1)}), bf16[32,48,128]{2,1,0:T(8,128)(2,1)S(1)}, u32[]{:S(2)}, u32[]{:S(2)}) async-start(bf16[32,48,128]{2,1,0:T(8,128)(2,1)} %fourth_kernel.1), calls=%async_computation.8 | async-start | bytes 786432 | tf_op jit(solution)/shard_map/all_to_all | solution.py:297
  228.3 2.1 all-gather.5
  230.4 13.0 %all-to-all-done.8.cols = bf16[32,48,128]{2,1,0:T(8,128)(2,1)S(1)} async-done(((bf16[32,48,128]{2,1,0:T(8,128)(2,1)}), bf16[32,48,128]{2,1,0:T(8,128)(2,1)S(1)}, u32[]{:S(2)}, u32[]{:S(2)}) %all-to-all-start.8) | async-done | bytes 393248 | tf_op jit(solution)/shard_map/all_to_all | solution.py:297
  243.4 1.9 fifth_kernel.1
  245.3 4.2 %all-to-all-start.9 = ((bf16[32,48,128]{2,1,0:T(8,128)(2,1)}), bf16[32,48,128]{2,1,0:T(8,128)(2,1)S(1)}, u32[]{:S(2)}, u32[]{:S(2)}) async-start(bf16[32,48,128]{2,1,0:T(8,128)(2,1)} %fifth_kernel.1), calls=%async_computation.9 | async-start | bytes 786432 | tf_op jit(solution)/shard_map/all_to_all | solution.py:297
  249.5 0.5 slice.29
  250.7 13.3 %all-to-all-done.9.cols = bf16[32,48,128]{2,1,0:T(8,128)(2,1)S(1)} async-done(((bf16[32,48,128]{2,1,0:T(8,128)(2,1)}), bf16[32,48,128]{2,1,0:T(8,128)(2,1)S(1)}, u32[]{:S(2)}, u32[]{:S(2)}) %all-to-all-start.9) | async-done | bytes 393248 | tf_op jit(solution)/shard_map/all_to_all | solution.py:297
  264.1 0.2 last_kernel.1
  264.3 0.3 fusion.1
  264.7 0.3 fusion
  265.0 0.7 fusion.8
  (1 shorter events, 0.0 us)
Async XLA Ops:
  0.6 0.9 copy-start
  168.4 20.0 %all-to-all-start.5 = ((bf16[32,48,128]{2,1,0:T(8,128)(2,1)}), bf16[32,48,128]{2,1,0:T(8,128)(2,1)S(1)}, u32[]{:S(2)}, u32[]{:S(2)}) async-start(bf16[32,48,128]{2,1,0:T(8,128)(2,1)} %get-tuple-element.25), calls=%async_computation.5 | async-start | bytes 786432 | tf_op jit(solution)/shard_map/all_to_all | solution.py:297
  209.1 14.7 %all-to-all-start.6 = ((bf16[12,56,128]{2,1,0:T(8,128)(2,1)}), bf16[12,56,128]{2,1,0:T(8,128)(2,1)S(1)}, u32[]{:S(2)}, u32[]{:S(2)}) async-start(bf16[12,56,128]{2,1,0:T(8,128)(2,1)} %get-tuple-element.26), calls=%async_computation.6 | async-start | bytes 344064 | tf_op jit(solution)/shard_map/all_to_all | solution.py:297
  223.8 19.6 %all-to-all-start.8 = ((bf16[32,48,128]{2,1,0:T(8,128)(2,1)}), bf16[32,48,128]{2,1,0:T(8,128)(2,1)S(1)}, u32[]{:S(2)}, u32[]{:S(2)}) async-start(bf16[32,48,128]{2,1,0:T(8,128)(2,1)} %fourth_kernel.1), calls=%async_computation.8 | async-start | bytes 786432 | tf_op jit(solution)/shard_map/all_to_all | solution.py:297
  245.3 18.8 %all-to-all-start.9 = ((bf16[32,48,128]{2,1,0:T(8,128)(2,1)}), bf16[32,48,128]{2,1,0:T(8,128)(2,1)S(1)}, u32[]{:S(2)}, u32[]{:S(2)}) async-start(bf16[32,48,128]{2,1,0:T(8,128)(2,1)} %fifth_kernel.1), calls=%async_computation.9 | async-start | bytes 786432 | tf_op jit(solution)/shard_map/all_to_all | solution.py:297

commit v4 on v3

--- a/solution.py
+++ b/solution.py
@@ -251,27 +251,80 @@
     copies(out_rows, pack_z(value, spread(diag)))
 
 
-def third_kernel(at, poly_rows, rows, cols, out_square, out_product, current_rows, first_rows, right):
+def third_kernel(at, poly_rows, rows, cols, out, right, kept, rows_kept, first_rows, current_rows):
     unpack_columns(cols, right)
-    copies(out_product, pack_z(dot(poly_rows[...], right[...])))
+    diagonal = [jnp.zeros((count, LANES), f32) for count in (WIDE, 8, 8)]
 
     def of_rows(part, first, col, packed):
         eye = eye_of(at, first, part.shape[0], col)
+        i = (0, WIDE, MAIN).index(first)
         part = part.astype(f32)
-        return part.astype(bf16), jnp.where(eye, gathered(packed), -2.0 * part).astype(bf16)
+        row = gathered(packed)
+        diagonal[i] += jnp.where(eye, row, 0.0)
+        return part.astype(bf16), jnp.where(eye, row, -2.0 * part).astype(bf16)
 
     unpack_rows(rows, at, (first_rows, current_rows), of_rows)
-    send_tp(at, out_square, dot(first_rows[...], right[...]))
-
-
-def fourth_kernel(at, current_rows, cols, out, right):
+    own = pl.ds(pl.multiple_of(at[4], LANES), LANES)
+    product = dot(poly_rows[...], right[...])
+    moved = dot(current_rows[...], right[...])
+    moved_low = moved.astype(bf16).astype(f32)
+    square = dot(first_rows[...], right[...])
+    moved_off = moved - moved_low
+    kept[0] = first_rows[:, own].astype(f32)
+    kept[1] = current_rows[:, own].astype(f32)
+    kept[2] = moved_off
+    kept[3] = square.astype(bf16).astype(f32) - square
+    kept[4] = jnp.broadcast_to(
+        jnp.sum(jnp.concatenate(diagonal, axis=0), axis=1, keepdims=True), (ROWS, LANES)
+    )
+    eye = own_eye(at)
+    tail = spread(jnp.sum(jnp.where(eye, moved_off, 0.0), axis=0, keepdims=True))
+    product, moved_low = pack_z(product).astype(bf16), pack_z(moved_low, tail).astype(bf16)
+    for z in range(DEPTH):
+        out[z, :WIDE] = product
+        out[z, WIDE:] = moved_low
+    mine = right[own, :].astype(f32)
+    total = jnp.zeros((LANES, LANES), f32)
+    for block in range(BLOCKS):
+        value = right[block * LANES : (block + 1) * LANES, :].astype(f32)
+        total += value * value
+    total = jnp.sum(total, axis=0, keepdims=True)
+    on = rows_of(LANES) == lanes_of(LANES)
+    row = rows_of(8)
+    rows_kept[...] = jnp.where(
+        row == 0,
+        jnp.sum(jnp.where(on, mine, 0.0), axis=0, keepdims=True),
+        total.astype(bf16).astype(f32) - total,
+    )
+
+
+def fourth_kernel(at, rows, right, kept, rows_kept, out, product_rows, moved_rows):
+    diagonal = [jnp.zeros((count, LANES), f32) for count in (WIDE, 8, 8)]
+
+    def of_rows(part, first, col, packed):
+        eye = eye_of(at, first, part.shape[0], col)
+        diagonal[(0, WIDE, MAIN).index(first)] += jnp.where(eye, gathered(packed), 0.0)
+        return (part.astype(bf16),)
+
+    unpack_rows(rows.at[:, :, WIDE:], at, (moved_rows,), of_rows)
+    unpack_rows(rows.at[:, :, :WIDE], at, (product_rows,), lambda part, first, col, packed: (part.astype(bf16),))
+    moved_diagonal = jnp.sum(jnp.concatenate(diagonal, axis=0), axis=1, keepdims=True)
+    poly_own, current_own, moved_off, square_off, current_diagonal = (kept[i] for i in range(5))
+    poly_diagonal, square_diagonal = rows_kept[0:1], rows_kept[1:2]
+    eye = own_eye(at)
+    off = jnp.where(
+        eye,
+        moved_off * poly_own + current_own * square_off,
+        moved_diagonal * poly_own
+        + moved_off * poly_diagonal
+        + current_diagonal * square_off
+        + current_own * square_diagonal,
+    )
+    send_tp(at, out, poly(eye, dot(moved_rows[...], right[...]) + off))
+
+
+def fifth_kernel(at, product_rows, cols, out, right):
     unpack_columns(cols, right)
-    send_tp(at, out, next_poly(at, dot(current_rows[...], right[...]))[0])
-
-
-def fifth_kernel(at, rows, cols, out, product_rows, right):
-    unpack_columns(cols, right)
-    unpack_rows(rows, at, (product_rows,), lambda part, first, col, packed: (part.astype(bf16),))
     send_tp(at, out, dot(product_rows[...], right[...]))
 
 
@@ -346,16 +399,22 @@
         first_kernel, [to_tp, left, left, ((8, LANES), f32)], at, rows, cols, scratch=[right]
     )
     cols, rows = call(second_kernel, [to_tp, to_z], at, current_rows, exchange(sent, TP), scratch=[right])
+    rows = both_cores(exchange(rows, "z"))
     cols = exchange(cols, TP)
+    rows, right_poly, kept, rows_kept = call(
+        third_kernel,
+        [((DEPTH, 2 * WIDE, LANES), bf16), right, ((5, ROWS, LANES), f32), ((8, LANES), f32)],
+        at,
+        poly_rows,
+        rows,
+        cols,
+        scratch=[left, left],
+    )
     rows = both_cores(exchange(rows, "z"))
-    square, product, current_rows = call(
-        third_kernel, [to_tp, to_z, left], at, poly_rows, rows, cols, scratch=[left, right]
-    )
-    cols = exchange(square, TP)
-    rows = both_cores(exchange(product, "z"))
-    (cols,) = call(fourth_kernel, [to_tp], at, current_rows, cols, scratch=[right])
-    cols = exchange(cols, TP)
-    (cols,) = call(fifth_kernel, [to_tp], at, rows, cols, scratch=[left, right])
+    cols, product_rows = call(
+        fourth_kernel, [to_tp, left], at, rows, right_poly, kept, rows_kept, scratch=[left]
+    )
+    (cols,) = call(fifth_kernel, [to_tp], at, product_rows, exchange(cols, TP), scratch=[right])
     (product,) = call(last_kernel, [right], exchange(cols, TP))
 
     whole_product = product.reshape(BLOCKS, LANES, LANES)[:, :COLS].reshape(2, D // 2, LANES)

time: 267 us -> 257 us (0.963)
  the two profiles are of different devices: /device:TPU:64 before, /device:TPU:8 now
where the time goes in v4:
time: 257 us; the launch traced here: 256 us
  blocking collectives  205 us (80%)
  waiting for transfers between devices  23.8 us (9%)
  Pallas kernels  10.8 us (4%)
  starting transfers between devices  10.1 us (4%)
    all_to_all x7, blocking collectives, exchange(): lax.all_to_all(stacked, axes, split_axis=0, concat_axis=0, tiled=True)  157 us
    all_gather x1, blocking collectives, local(): by_z = lax.all_gather(low, 'z')  37.3 us
    all_to_all x2, waiting for transfers between devices, exchange(): lax.all_to_all(stacked, axes, split_axis=0, concat_axis=0, tiled=True)  23.8 us
    pallas_call x9, Pallas kernels, call(): pl.pallas_call(kernel, out_shape=[jax.ShapeDtypeStruct(shape, dtype) for...  10.8 us
    all_to_all x2, starting transfers between devices, exchange(): lax.all_to_all(stacked, axes, split_axis=0, concat_axis=0, tiled=True)  10.1 us
    all_gather x3, blocking collectives, both_cores(): return lax.all_gather(by_z, 'core')  6.62 us
  transfers between devices with their start and end apart: 2, of which 2 were waited for; matrix products, arithmetic and copies ran while one was open for 0% of the time, Pallas kernels for 0%

profile of v4, /device:TPU:8, one launch (start us, length us, event | category | flops | bytes accessed | tf_op | source)
XLA Modules:
  0.0 256.4 jit_solution(6159109343592572284)
XLA Ops:
  0.6 0.0 copy-start
  0.7 0.8 copy-done
  1.5 1.7 fusion.5
  3.2 0.1 fusion.4.low
  3.3 0.1 stack.23.at
  3.4 37.3 %all-gather = bf16[1056,384]{1,0:T(8,128)(2,1)S(1)} all-gather(bf16[88,384]{1,0:T(8,128)(2,1)S(1)} %fusion.4.low), channel_id=2, replica_groups=mesh['z'=12,'core'=2,'y'=8,'x'=4] {'z'}, dimensions={0}, use_global_device_ids=true | all-gather | bytes 878592 | tf_op jit(solution)/shard_map/all_gather | solution.py:375
  40.7 0.1 fusion.7
  40.8 2.4 all-gather.1
  43.2 2.4 all-gather.2
  45.6 1.2 gram_kernel.1
  46.8 32.2 %all_to_all.45.arrived = f32[32,48,128]{2,1,0:T(8,128)S(1)} all-to-all(f32[32,48,128]{2,1,0:T(8,128)S(1)} %get-tuple-element.23), channel_id=1, replica_groups=mesh['z'=12,'core'=2,'y'=8,'x'=4] {'y','x'}, dimensions={0} | all-to-all | bytes 1572864 | tf_op jit(solution)/shard_map/all_to_all | solution.py:350
  79.0 0.1 total_kernel.1
  79.1 27.4 %all_to_all.46.cols = f32[32,48,128]{2,1,0:T(8,128)S(1)} all-to-all(f32[32,48,128]{2,1,0:T(8,128)S(1)} %total_kernel.1), channel_id=1, replica_groups=mesh['z'=12,'core'=2,'y'=8,'x'=4] {'y','x'}, dimensions={0} | all-to-all | bytes 1572864 | tf_op jit(solution)/shard_map/all_to_all | solution.py:350
  106.5 1.0 square_kernel.1
  107.5 18.8 %all_to_all.47 = f32[12,56,128]{2,1,0:T(8,128)S(1)} all-to-all(f32[12,56,128]{2,1,0:T(8,128)S(1)} %square_kernel.1), channel_id=1, replica_groups=mesh['z'=12,'core'=2,'y'=8,'x'=4] {'z'}, dimensions={0} | all-to-all | bytes 688128 | tf_op jit(solution)/shard_map/all_to_all | solution.py:350
  126.3 2.3 all-gather.3
  128.6 1.8 first_kernel.1
  130.4 21.8 %all_to_all.48.cols = bf16[32,48,128]{2,1,0:T(8,128)(2,1)S(1)} all-to-all(bf16[32,48,128]{2,1,0:T(8,128)(2,1)S(1)} %get-tuple-element.26), channel_id=1, replica_groups=mesh['z'=12,'core'=2,'y'=8,'x'=4] {'y','x'}, dimensions={0} | all-to-all | bytes 786432 | tf_op jit(solution)/shard_map/all_to_all | solution.py:350
  152.2 1.8 second_kernel.1
  154.0 15.2 %all_to_all.49 = bf16[12,56,128]{2,1,0:T(8,128)(2,1)S(1)} all-to-all(bf16[12,56,128]{2,1,0:T(8,128)(2,1)S(1)} %get-tuple-element.27), channel_id=1, replica_groups=mesh['z'=12,'core'=2,'y'=8,'x'=4] {'z'}, dimensions={0} | all-to-all | bytes 344064 | tf_op jit(solution)/shard_map/all_to_all | solution.py:350
  169.2 5.2 %all-to-all-start.5 = ((bf16[32,48,128]{2,1,0:T(8,128)(2,1)}), bf16[32,48,128]{2,1,0:T(8,128)(2,1)S(1)}, u32[]{:S(2)}, u32[]{:S(2)}) async-start(bf16[32,48,128]{2,1,0:T(8,128)(2,1)} %get-tuple-element.28), calls=%async_computation.5 | async-start | bytes 786432 | tf_op jit(solution)/shard_map/all_to_all | solution.py:350
  174.5 2.1 all-gather.4
  176.5 11.1 %all-to-all-done.5.cols = bf16[32,48,128]{2,1,0:T(8,128)(2,1)S(1)} async-done(((bf16[32,48,128]{2,1,0:T(8,128)(2,1)}), bf16[32,48,128]{2,1,0:T(8,128)(2,1)S(1)}, u32[]{:S(2)}, u32[]{:S(2)}) %all-to-all-start.5) | async-done | bytes 393248 | tf_op jit(solution)/shard_map/all_to_all | solution.py:350
  187.6 1.7 third_kernel.1
  189.3 20.2 %all_to_all.50 = bf16[12,112,128]{2,1,0:T(8,128)(2,1)S(1)} all-to-all(bf16[12,112,128]{2,1,0:T(8,128)(2,1)S(1)} %get-tuple-element.29), channel_id=1, replica_groups=mesh['z'=12,'core'=2,'y'=8,'x'=4] {'z'}, dimensions={0} | all-to-all | bytes 688128 | tf_op jit(solution)/shard_map/all_to_all | solution.py:350
  209.5 2.3 all-gather.5
  211.8 1.1 fourth_kernel.1
  212.9 21.0 %all_to_all.51.cols = bf16[32,48,128]{2,1,0:T(8,128)(2,1)S(1)} all-to-all(bf16[32,48,128]{2,1,0:T(8,128)(2,1)S(1)} %get-tuple-element.34), channel_id=1, replica_groups=mesh['z'=12,'core'=2,'y'=8,'x'=4] {'y','x'}, dimensions={0} | all-to-all | bytes 786432 | tf_op jit(solution)/shard_map/all_to_all | solution.py:350
  234.0 1.8 fifth_kernel.1
  235.8 4.9 %all-to-all-start.8 = ((bf16[32,48,128]{2,1,0:T(8,128)(2,1)}), bf16[32,48,128]{2,1,0:T(8,128)(2,1)S(1)}, u32[]{:S(2)}, u32[]{:S(2)}) async-start(bf16[32,48,128]{2,1,0:T(8,128)(2,1)} %fifth_kernel.1), calls=%async_computation.8 | async-start | bytes 786432 | tf_op jit(solution)/shard_map/all_to_all | solution.py:350
  240.7 0.5 slice.29
  241.9 12.7 %all-to-all-done.8.cols = bf16[32,48,128]{2,1,0:T(8,128)(2,1)S(1)} async-done(((bf16[32,48,128]{2,1,0:T(8,128)(2,1)}), bf16[32,48,128]{2,1,0:T(8,128)(2,1)S(1)}, u32[]{:S(2)}, u32[]{:S(2)}) %all-to-all-start.8) | async-done | bytes 393248 | tf_op jit(solution)/shard_map/all_to_all | solution.py:350
  254.7 0.2 last_kernel.1
  254.9 0.3 fusion.1
  255.3 0.4 fusion
  255.6 0.7 fusion.8
  (1 shorter events, 0.0 us)
Async XLA Ops:
  0.6 0.9 copy-start
  169.2 18.4 %all-to-all-start.5 = ((bf16[32,48,128]{2,1,0:T(8,128)(2,1)}), bf16[32,48,128]{2,1,0:T(8,128)(2,1)S(1)}, u32[]{:S(2)}, u32[]{:S(2)}) async-start(bf16[32,48,128]{2,1,0:T(8,128)(2,1)} %get-tuple-element.28), calls=%async_computation.5 | async-start | bytes 786432 | tf_op jit(solution)/shard_map/all_to_all | solution.py:350
  235.8 18.9 %all-to-all-start.8 = ((bf16[32,48,128]{2,1,0:T(8,128)(2,1)}), bf16[32,48,128]{2,1,0:T(8,128)(2,1)S(1)}, u32[]{:S(2)}, u32[]{:S(2)}) async-start(bf16[32,48,128]{2,1,0:T(8,128)(2,1)} %fifth_kernel.1), calls=%async_computation.8 | async-start | bytes 786432 | tf_op jit(solution)/shard_map/all_to_all | solution.py:350

commit v5 on v4

--- a/solution.py
+++ b/solution.py
@@ -132,6 +132,18 @@
                     target[first : first + part.shape[0], b * LANES : (b + 1) * LANES] = value
 
 
+def position():
+    own = place(lax.axis_index("core"), lax.axis_index("z"))
+    t = lax.axis_index("y") * 4 + lax.axis_index("x")
+    return (
+        t * MAIN,
+        SHARED + 8 * (t // 4) - MAIN,
+        own * COLS,
+        (FREE + LANES - PIECE * (t % 4)) % LANES,
+        own * LANES,
+    )
+
+
 def eye_of(at, first, count, col):
     row = at[0] if first < MAIN else at[1]
     return (rows_of(count) + (row + first) == lanes_of(count) + col) & (lanes_of(count) < COLS)
@@ -159,7 +171,7 @@
     copies(out, pack_tp(block[:MAIN], block[MAIN:ROWS], at[3], tail))
 
 
-def gram_kernel(at, low, whole0, whole1, out, trace, own, share):
+def gram_kernel(low, whole0, whole1, out, trace, own, share):
     mine = low[...]
     trace[...] = jnp.broadcast_to(jnp.sum(jnp.square(mine.astype(f32)), keepdims=True), trace.shape)
     own[:COLS] = mine
@@ -183,7 +195,8 @@
     copies(out, jnp.where(spot, trace[0:1], total))
 
 
-def square_kernel(at, cols, out, whole):
+def square_kernel(cols, out, whole):
+    at = position()
     unpack_columns(cols, whole)
     ends = cols[0, SENT - 8 :]
     for t in range(1, TPS):
@@ -208,7 +221,8 @@
     copies(out, pack_z(value, tail))
 
 
-def first_kernel(at, rows, cols, out, poly_rows, current_rows, spectral_out, right):
+def first_kernel(rows, cols, out, poly_rows, current_rows, spectral_out, right):
+    at = position()
     tails = jnp.zeros((WIDE - SPARE, LANES), f32)
     for core in range(2):
         for z in range(DEPTH):
@@ -244,14 +258,16 @@
     return poly(eye, current), jnp.sum(jnp.where(eye, current, 0.0), axis=0, keepdims=True)
 
 
-def second_kernel(at, current_rows, cols, out_cols, out_rows, right):
+def second_kernel(current_rows, cols, out_cols, out_rows, right):
+    at = position()
     unpack_columns(cols, right)
     value, diag = next_poly(at, dot(current_rows[...], right[...]))
     send_tp(at, out_cols, value)
     copies(out_rows, pack_z(value, spread(diag)))
 
 
-def third_kernel(at, poly_rows, rows, cols, out, right, kept, rows_kept, first_rows, current_rows):
+def third_kernel(poly_rows, rows, cols, out, right, kept, rows_kept, first_rows, current_rows):
+    at = position()
     unpack_columns(cols, right)
     diagonal = [jnp.zeros((count, LANES), f32) for count in (WIDE, 8, 8)]
 
@@ -298,7 +314,8 @@
     )
 
 
-def fourth_kernel(at, rows, right, kept, rows_kept, out, product_rows, moved_rows):
+def fourth_kernel(rows, right, kept, rows_kept, out, product_rows, moved_rows):
+    at = position()
     diagonal = [jnp.zeros((count, LANES), f32) for count in (WIDE, 8, 8)]
 
     def of_rows(part, first, col, packed):
@@ -323,7 +340,8 @@
     send_tp(at, out, poly(eye, dot(moved_rows[...], right[...]) + off))
 
 
-def fifth_kernel(at, product_rows, cols, out, right):
+def fifth_kernel(product_rows, cols, out, right):
+    at = position()
     unpack_columns(cols, right)
     send_tp(at, out, dot(product_rows[...], right[...]))
 
@@ -334,11 +352,10 @@
 
 def call(kernel, outs, *args, scratch=()):
     vmem = pl.BlockSpec(memory_space=pltpu.VMEM)
-    smem = pl.BlockSpec(memory_space=pltpu.SMEM)
     return pl.pallas_call(
         kernel,
         out_shape=[jax.ShapeDtypeStruct(shape, dtype) for shape, dtype in outs],
-        in_specs=[smem if a.dtype == jnp.int32 else vmem for a in args],
+        in_specs=[vmem] * len(args),
         out_specs=[vmem] * len(outs),
         scratch_shapes=[pltpu.VMEM(shape, dtype) for shape, dtype in scratch],
         compiler_params=pltpu.CompilerParams(vmem_limit_bytes=24 * 2**20),
@@ -360,18 +377,6 @@
     half = gate_next.shape[1]
     low = jnp.concatenate([gate_next.astype(bf16), up_next.astype(bf16)], axis=1)
     low = jnp.pad(low, ((0, 0), (0, 3 * LANES - 2 * half)))
-    z, core, t = lax.axis_index("z"), lax.axis_index("core"), lax.axis_index(TP)
-    own = place(core, z)
-    at = jnp.stack(
-        [
-            t * MAIN,
-            SHARED + 8 * (t // 4) - MAIN,
-            own * COLS,
-            (FREE - PIECE * (t % 4)) % LANES,
-            own * LANES,
-        ]
-    ).astype(jnp.int32)
-    low, at = lax.optimization_barrier((low, at))
     by_z = lax.all_gather(low, "z")
     whole = [
         lax.all_gather(by_z[h * NEAR : (h + 1) * NEAR], "core").reshape(D // 2, -1) for h in range(2)
@@ -386,25 +391,23 @@
     shares, trace = call(
         gram_kernel,
         [to_tp32, ((8, LANES), f32)],
-        at,
         low,
         *whole,
         scratch=[((LANES, low.shape[1]), bf16), ((D, LANES), f32)],
     )
     (cols,) = call(total_kernel, [to_tp32], trace, exchange(shares, TP))
     cols = exchange(cols, TP)
-    (rows,) = call(square_kernel, [to_z32], at, cols, scratch=[(right[0], f32)])
+    (rows,) = call(square_kernel, [to_z32], cols, scratch=[(right[0], f32)])
     rows = both_cores(exchange(rows, "z"))
     sent, poly_rows, current_rows, spectral = call(
-        first_kernel, [to_tp, left, left, ((8, LANES), f32)], at, rows, cols, scratch=[right]
-    )
-    cols, rows = call(second_kernel, [to_tp, to_z], at, current_rows, exchange(sent, TP), scratch=[right])
+        first_kernel, [to_tp, left, left, ((8, LANES), f32)], rows, cols, scratch=[right]
+    )
+    cols, rows = call(second_kernel, [to_tp, to_z], current_rows, exchange(sent, TP), scratch=[right])
     rows = both_cores(exchange(rows, "z"))
     cols = exchange(cols, TP)
     rows, right_poly, kept, rows_kept = call(
         third_kernel,
         [((DEPTH, 2 * WIDE, LANES), bf16), right, ((5, ROWS, LANES), f32), ((8, LANES), f32)],
-        at,
         poly_rows,
         rows,
         cols,
@@ -412,9 +415,9 @@
     )
     rows = both_cores(exchange(rows, "z"))
     cols, product_rows = call(
-        fourth_kernel, [to_tp, left], at, rows, right_poly, kept, rows_kept, scratch=[left]
-    )
-    (cols,) = call(fifth_kernel, [to_tp], at, product_rows, exchange(cols, TP), scratch=[right])
+        fourth_kernel, [to_tp, left], rows, right_poly, kept, rows_kept, scratch=[left]
+    )
+    (cols,) = call(fifth_kernel, [to_tp], product_rows, exchange(cols, TP), scratch=[right])
     (product,) = call(last_kernel, [right], exchange(cols, TP))
 
     whole_product = product.reshape(BLOCKS, LANES, LANES)[:, :COLS].reshape(2, D // 2, LANES)

time: 257 us -> 252 us (0.981)
  Pallas kernels: 10.8 us -> 6.91 us
    pallas_call x9, Pallas kernels: 10.8 us -> 6.91 us  [call(): pl.pallas_call(kernel, out_shape=[jax.ShapeDtypeStruct(shape, dtype) for...]
where the time goes in v5:
time: 252 us
  blocking collectives  205 us (81%)
  waiting for transfers between devices  23.8 us (9%)
  starting transfers between devices  10.1 us (4%)
  Pallas kernels  6.91 us (3%)
    all_to_all x7, blocking collectives, exchange(): lax.all_to_all(stacked, axes, split_axis=0, concat_axis=0, tiled=True)  157 us
    all_gather x1, blocking collectives, local(): by_z = lax.all_gather(low, 'z')  37.4 us
    all_to_all x2, waiting for transfers between devices, exchange(): lax.all_to_all(stacked, axes, split_axis=0, concat_axis=0, tiled=True)  23.8 us
    all_to_all x2, starting transfers between devices, exchange(): lax.all_to_all(stacked, axes, split_axis=0, concat_axis=0, tiled=True)  10.1 us
    pallas_call x9, Pallas kernels, call(): pl.pallas_call(kernel, out_shape=[jax.ShapeDtypeStruct(shape, dtype) for...  6.91 us
    all_gather x3, blocking collectives, both_cores(): return lax.all_gather(by_z, 'core')  6.62 us
  transfers between devices with their start and end apart: 2, of which 2 were waited for; matrix products, arithmetic and copies ran while one was open for 0% of the time, Pallas kernels for 0%

profile of v5, /device:TPU:8, one launch (start us, length us, event | category | flops | bytes accessed | tf_op | source)
XLA Modules:
  0.0 251.6 jit_solution(8970954278874610007)
XLA Ops:
  0.6 1.7 fusion.5
  2.3 0.1 fusion.4.low
  2.4 37.4 %all-gather = bf16[1056,384]{1,0:T(8,128)(2,1)S(1)} all-gather(bf16[88,384]{1,0:T(8,128)(2,1)S(1)} %fusion.4.low), channel_id=2, replica_groups=mesh['z'=12,'core'=2,'y'=8,'x'=4] {'z'}, dimensions={0}, use_global_device_ids=true | all-gather | bytes 878592 | tf_op jit(solution)/shard_map/all_gather | solution.py:380
  39.8 0.1 fusion.7
  39.9 2.4 all-gather.1
  42.3 2.4 all-gather.2
  44.6 0.7 gram_kernel.1
  45.4 32.2 %all_to_all.45.arrived = f32[32,48,128]{2,1,0:T(8,128)S(1)} all-to-all(f32[32,48,128]{2,1,0:T(8,128)S(1)} %get-tuple-element.19), channel_id=1, replica_groups=mesh['z'=12,'core'=2,'y'=8,'x'=4] {'y','x'}, dimensions={0} | all-to-all | bytes 1572864 | tf_op jit(solution)/shard_map/all_to_all | solution.py:367
  77.5 0.1 total_kernel.1
  77.6 27.4 %all_to_all.46.cols = f32[32,48,128]{2,1,0:T(8,128)S(1)} all-to-all(f32[32,48,128]{2,1,0:T(8,128)S(1)} %total_kernel.1), channel_id=1, replica_groups=mesh['z'=12,'core'=2,'y'=8,'x'=4] {'y','x'}, dimensions={0} | all-to-all | bytes 1572864 | tf_op jit(solution)/shard_map/all_to_all | solution.py:367
  105.0 0.5 square_kernel.1
  105.5 18.8 %all_to_all.47 = f32[12,56,128]{2,1,0:T(8,128)S(1)} all-to-all(f32[12,56,128]{2,1,0:T(8,128)S(1)} %square_kernel.1), channel_id=1, replica_groups=mesh['z'=12,'core'=2,'y'=8,'x'=4] {'z'}, dimensions={0} | all-to-all | bytes 688128 | tf_op jit(solution)/shard_map/all_to_all | solution.py:367
  124.3 2.3 all-gather.3
  126.6 1.2 first_kernel.1
  127.8 21.8 %all_to_all.48.cols = bf16[32,48,128]{2,1,0:T(8,128)(2,1)S(1)} all-to-all(bf16[32,48,128]{2,1,0:T(8,128)(2,1)S(1)} %get-tuple-element.22), channel_id=1, replica_groups=mesh['z'=12,'core'=2,'y'=8,'x'=4] {'y','x'}, dimensions={0} | all-to-all | bytes 786432 | tf_op jit(solution)/shard_map/all_to_all | solution.py:367
  149.6 1.3 second_kernel.1
  150.9 15.2 %all_to_all.49 = bf16[12,56,128]{2,1,0:T(8,128)(2,1)S(1)} all-to-all(bf16[12,56,128]{2,1,0:T(8,128)(2,1)S(1)} %get-tuple-element.23), channel_id=1, replica_groups=mesh['z'=12,'core'=2,'y'=8,'x'=4] {'z'}, dimensions={0} | all-to-all | bytes 344064 | tf_op jit(solution)/shard_map/all_to_all | solution.py:367
  166.1 5.2 %all-to-all-start.5 = ((bf16[32,48,128]{2,1,0:T(8,128)(2,1)}), bf16[32,48,128]{2,1,0:T(8,128)(2,1)S(1)}, u32[]{:S(2)}, u32[]{:S(2)}) async-start(bf16[32,48,128]{2,1,0:T(8,128)(2,1)} %get-tuple-element.24), calls=%async_computation.5 | async-start | bytes 786432 | tf_op jit(solution)/shard_map/all_to_all | solution.py:367
  171.4 2.1 all-gather.4
  173.4 11.1 %all-to-all-done.5.cols = bf16[32,48,128]{2,1,0:T(8,128)(2,1)S(1)} async-done(((bf16[32,48,128]{2,1,0:T(8,128)(2,1)}), bf16[32,48,128]{2,1,0:T(8,128)(2,1)S(1)}, u32[]{:S(2)}, u32[]{:S(2)}) %all-to-all-start.5) | async-done | bytes 393248 | tf_op jit(solution)/shard_map/all_to_all | solution.py:367
  184.5 1.1 third_kernel.1
  185.6 20.2 %all_to_all.50 = bf16[12,112,128]{2,1,0:T(8,128)(2,1)S(1)} all-to-all(bf16[12,112,128]{2,1,0:T(8,128)(2,1)S(1)} %get-tuple-element.25), channel_id=1, replica_groups=mesh['z'=12,'core'=2,'y'=8,'x'=4] {'z'}, dimensions={0} | all-to-all | bytes 688128 | tf_op jit(solution)/shard_map/all_to_all | solution.py:367
  205.9 2.3 all-gather.5
  208.1 0.6 fourth_kernel.1
  208.7 21.0 %all_to_all.51.cols = bf16[32,48,128]{2,1,0:T(8,128)(2,1)S(1)} all-to-all(bf16[32,48,128]{2,1,0:T(8,128)(2,1)S(1)} %get-tuple-element.30), channel_id=1, replica_groups=mesh['z'=12,'core'=2,'y'=8,'x'=4] {'y','x'}, dimensions={0} | all-to-all | bytes 786432 | tf_op jit(solution)/shard_map/all_to_all | solution.py:367
  229.7 1.3 fifth_kernel.1
  231.0 4.9 %all-to-all-start.8 = ((bf16[32,48,128]{2,1,0:T(8,128)(2,1)}), bf16[32,48,128]{2,1,0:T(8,128)(2,1)S(1)}, u32[]{:S(2)}, u32[]{:S(2)}) async-start(bf16[32,48,128]{2,1,0:T(8,128)(2,1)} %fifth_kernel.1), calls=%async_computation.8 | async-start | bytes 786432 | tf_op jit(solution)/shard_map/all_to_all | solution.py:367
  235.9 0.5 slice.29
  237.2 12.7 %all-to-all-done.8.cols = bf16[32,48,128]{2,1,0:T(8,128)(2,1)S(1)} async-done(((bf16[32,48,128]{2,1,0:T(8,128)(2,1)}), bf16[32,48,128]{2,1,0:T(8,128)(2,1)S(1)}, u32[]{:S(2)}, u32[]{:S(2)}) %all-to-all-start.8) | async-done | bytes 393248 | tf_op jit(solution)/shard_map/all_to_all | solution.py:367
  249.9 0.2 last_kernel.1
  250.2 0.3 fusion.1
  250.5 0.3 fusion
  250.9 0.7 fusion.8
  (1 shorter events, 0.0 us)
Async XLA Ops:
  166.1 18.4 %all-to-all-start.5 = ((bf16[32,48,128]{2,1,0:T(8,128)(2,1)}), bf16[32,48,128]{2,1,0:T(8,128)(2,1)S(1)}, u32[]{:S(2)}, u32[]{:S(2)}) async-start(bf16[32,48,128]{2,1,0:T(8,128)(2,1)} %get-tuple-element.24), calls=%async_computation.5 | async-start | bytes 786432 | tf_op jit(solution)/shard_map/all_to_all | solution.py:367
  231.0 18.9 %all-to-all-start.8 = ((bf16[32,48,128]{2,1,0:T(8,128)(2,1)}), bf16[32,48,128]{2,1,0:T(8,128)(2,1)S(1)}, u32[]{:S(2)}, u32[]{:S(2)}) async-start(bf16[32,48,128]{2,1,0:T(8,128)(2,1)} %fifth_kernel.1), calls=%async_computation.8 | async-start | bytes 786432 | tf_op jit(solution)/shard_map/all_to_all | solution.py:367

commit v6 on v5

--- a/solution.py
+++ b/solution.py
@@ -103,22 +103,28 @@
         at += count
 
 
-def unpack_columns(blocks, target, change=lambda part, first: part):
+def unpack_columns(blocks, target, scales=None):
+    def scaled(part, t):
+        return part if scales is None else part * scales[t]
+
     for block in range(BLOCKS):
         target[block * LANES + COLS : (block + 1) * LANES, :] = jnp.zeros((LANES - COLS, LANES), target.dtype)
     for t in range(TPS):
         packed = blocks[t]
-        store_rows(target, MAIN * t, change(packed, MAIN * t))
-        store_rows(target, MAIN * t + 48, change(unfolded(packed), MAIN * t + 48))
+        store_rows(target, MAIN * t, scaled(packed, t))
+        store_rows(target, MAIN * t + 48, scaled(unfolded(packed), t))
     lane = lanes_of(8)
     for group in range(TPS // 4):
         parts = [
-            pltpu.roll(blocks[4 * group + q, 32:40].astype(f32), PIECE * q + LANES - FREE, 1) for q in range(4)
+            scaled(
+                pltpu.roll(blocks[4 * group + q, 32:40].astype(f32), PIECE * q + LANES - FREE, 1), 4 * group + q
+            )
+            for q in range(4)
         ]
         value = parts[3]
         for q in (2, 1, 0):
             value = jnp.where(lane < PIECE * (q + 1), parts[q], value)
-        store_rows(target, SHARED + 8 * group, change(value, SHARED + 8 * group))
+        store_rows(target, SHARED + 8 * group, value)
 
 
 def unpack_rows(blocks, at, targets, change):
@@ -141,6 +147,7 @@
         own * COLS,
         (FREE + LANES - PIECE * (t % 4)) % LANES,
         own * LANES,
+        t % 4,
     )
 
 
@@ -171,10 +178,8 @@
     copies(out, pack_tp(block[:MAIN], block[MAIN:ROWS], at[3], tail))
 
 
-def gram_kernel(low, whole0, whole1, out, trace, own, share):
-    mine = low[...]
-    trace[...] = jnp.broadcast_to(jnp.sum(jnp.square(mine.astype(f32)), keepdims=True), trace.shape)
-    own[:COLS] = mine
+def gram_kernel(low, whole0, whole1, out, own, share):
+    own[:COLS] = low[...]
     own[COLS:] = jnp.zeros((LANES - COLS, own.shape[1]), bf16)
     half = D // 2
     for h, whole in enumerate((whole0, whole1)):
@@ -187,41 +192,84 @@
         out[t] = pack_tp(share[MAIN * t : MAIN * (t + 1)], shared, (FREE - PIECE * q) % LANES)
 
 
-def total_kernel(trace, arrived, out):
+def eleven_bits(value):
+    moved = value * 8193.0
+    return moved - (moved - value)
+
+
+def total_kernel(arrived, gram, out):
+    at = position()
     total = arrived[0]
     for t in range(1, TPS):
         total += arrived[t]
-    spot = (rows_of(SENT) == SENT - 1) & (lanes_of(SENT) == FREE)
-    copies(out, jnp.where(spot, trace[0:1], total))
-
-
-def square_kernel(cols, out, whole):
-    at = position()
-    unpack_columns(cols, whole)
-    ends = cols[0, SENT - 8 :]
-    for t in range(1, TPS):
-        ends += cols[t, SENT - 8 :]
-    trace = jnp.sum(jnp.where((rows_of(8) == 7) & (lanes_of(8) == FREE), ends, 0.0), keepdims=True)
+    gram[...] = total
+    most = jnp.max(jnp.abs(total), keepdims=True)
+    scale, factors = jnp.ones((1, 1), f32), []
+    for power in (-12, *(14,) * 8, 7, 4, 2, 1):
+        up = 2.0**power
+        take = most >= 2.0**15 if power < 0 else most < 2.0 ** (15 - power)
+        most = jnp.where(take, most * up, most)
+        scale = jnp.where(take, scale * up, scale)
+        factors.append(jnp.where(take, 1.0 / up, 1.0))
+    total = total * scale
+    high = eleven_bits(total)
+    rest = total - high
+    piece = pltpu.roll(rest[32:40], LANES - at[3], 1)
+    parts = (rest[:48], unfolded(rest), jnp.where(lanes_of(8) // PIECE == at[5], piece, 0.0))
+    left = sum(
+        jnp.sum(jnp.where(eye_of(at, first, p.shape[0], at[2]), p, 0.0), axis=0, keepdims=True)
+        for first, p in zip((0, 48, MAIN), parts)
+    )
+    left = jnp.broadcast_to(eleven_bits(left), (8, LANES))
+    row, lane = rows_of(8), lanes_of(8)
+    tail = jnp.where(
+        row == 0, pltpu.roll(left, FREE, 1), jnp.where(row == 1, pltpu.roll(left, FREE - 32, 1), pltpu.roll(left, FREE - 64, 1))
+    )
+    for i, factor in enumerate(factors):
+        tail = jnp.where((row == 7) & (lane == FREE + i), factor, tail)
+    tail = jnp.where((row == 7) & (lane >= FREE + len(factors)), 1.0, tail)
+    out[:40] = high[:40]
+    out[40:] = jnp.where(lane < FREE, high[40:], tail)
+
+
+def square_kernel(gram, cols, out, whole):
+    at = position()
+    lane = lanes_of(8)
+    left = jnp.zeros((8, LANES), f32)
+    inverses = []
+    for t in range(TPS):
+        tail = cols[t, 40:48]
+        product = tail
+        for shift in (1, 2, 4, 8):
+            product = product * pltpu.roll(product, LANES - shift, 1)
+        inverses.append(product[7:8, FREE : FREE + 1])
+        left += tail * inverses[t]
+    unpack_columns(cols, whole, scales=inverses)
+    left = jnp.where(
+        lane[:1] < 32,
+        pltpu.roll(left, 32, 1)[0:1],
+        jnp.where(lane[:1] < 64, pltpu.roll(left, 64, 1)[1:2], pltpu.roll(left, 96, 1)[2:3]),
+    )
+    own = pl.ds(pl.multiple_of(at[4], LANES), LANES)
+    eye = (rows_of(LANES) == lanes_of(LANES)) & (rows_of(LANES) < COLS)
+    mine = whole[own, :] + jnp.where(eye, left, 0.0)
+    whole[own, :] = mine
+    trace = jnp.sum(jnp.where(eye, mine, 0.0), keepdims=True)
     square = jnp.zeros((LANES, LANES), f32)
     for block in range(BLOCKS):
         value = whole[block * LANES : (block + 1) * LANES, :]
         square += value * value
     square = jnp.sum(jnp.where(lanes_of(LANES) < COLS, square, 0.0), keepdims=True)
-
-    def rows_at(first, count, target):
-        for i in range(0, count, 8):
-            block = (first + i) // COLS
-            start = pl.multiple_of(block * LANES + (first + i) - block * COLS, 8)
-            target.append(whole[pl.ds(start, 8), :])
-        return target
-
-    value = jnp.concatenate(rows_at(at[1] + MAIN, 8, rows_at(at[0], MAIN, [])), axis=0)
-    row, lane = rows_of(WIDE - SPARE), lanes_of(WIDE - SPARE)
+    shared = at[1] + MAIN
+    start = (shared // COLS) * LANES + shared % COLS
+    shared = whole[pl.ds(pl.multiple_of(start, 8), 8), :]
+    value = jnp.concatenate([gram[:48], unfolded(gram), shared], axis=0)
+    row = rows_of(8)
     tail = jnp.where((row == 0) & (lane == COLS), square, jnp.where((row == 0) & (lane == COLS + 1), trace, 0.0))
     copies(out, pack_z(value, tail))
 
 
-def first_kernel(rows, cols, out, poly_rows, current_rows, spectral_out, right):
+def first_kernel(rows, whole, out, poly_rows, current_rows, spectral_out, right):
     at = position()
     tails = jnp.zeros((WIDE - SPARE, LANES), f32)
     for core in range(2):
@@ -234,13 +282,12 @@
     spectral = 2.0 * square / (trace + EPS)
     inverse = 1.0 / spectral
     spectral_out[...] = jnp.broadcast_to(spectral, spectral_out.shape)
-
-    def of_cols(part, first):
-        n = part.shape[0]
-        eye = rows_of(n) + first == lanes_of(n) + at[2]
-        return poly(eye, part * inverse)
-
-    unpack_columns(cols, right, of_cols)
+    for block in range(BLOCKS):
+        part = pl.ds(block * LANES, LANES)
+        right[part, :] = (-0.5 * (whole[part, :] * inverse)).astype(bf16)
+    own = pl.ds(pl.multiple_of(at[4], LANES), LANES)
+    eye = (rows_of(LANES) == lanes_of(LANES)) & (rows_of(LANES) < COLS)
+    right[own, :] = poly(eye, whole[own, :] * inverse).astype(bf16)
 
     def of_rows(part, first, col, packed):
         current = part * inverse
@@ -346,8 +393,32 @@
     send_tp(at, out, dot(product_rows[...], right[...]))
 
 
-def last_kernel(cols, out):
-    unpack_columns(cols, out)
+def last_kernel(cols, whole0, whole1, spectral, out_gate, out_up, product):
+    for t in range(TPS):
+        packed = cols[t]
+        product[MAIN * t : MAIN * t + 48, :] = packed
+        product[MAIN * t + 48 : MAIN * (t + 1), :] = unfolded(packed).astype(bf16)
+    lane = lanes_of(8)
+    for group in range(TPS // 4):
+        value = pltpu.roll(cols[4 * group + 3, 32:40].astype(f32), PIECE * 3 + LANES - FREE, 1)
+        for q in (2, 1, 0):
+            part = pltpu.roll(cols[4 * group + q, 32:40].astype(f32), PIECE * q + LANES - FREE, 1)
+            value = jnp.where(lane < PIECE * (q + 1), part, value)
+        product[SHARED + 8 * group : SHARED + 8 * (group + 1), :] = value.astype(bf16)
+    half = D // 2
+    ortho = sum(
+        lax.dot_general(
+            product[h * half : (h + 1) * half, :],
+            whole[...],
+            (((0,), (0,)), ((), ())),
+            preferred_element_type=f32,
+        )
+        for h, whole in enumerate((whole0, whole1))
+    )
+    ortho = ortho[:COLS] * jnp.sqrt(2.0 * FF / spectral[0:1, 0:1])
+    width = out_gate.shape[1]
+    out_gate[...] = ortho[:, :width]
+    out_up[...] = ortho[:, width : 2 * width]
 
 
 def call(kernel, outs, *args, scratch=()):
@@ -388,19 +459,16 @@
     to_tp, to_z = ((TPS, SENT, LANES), bf16), ((DEPTH, WIDE, LANES), bf16)
     to_tp32, to_z32 = (to_tp[0], f32), (to_z[0], f32)
 
-    shares, trace = call(
-        gram_kernel,
-        [to_tp32, ((8, LANES), f32)],
-        low,
-        *whole,
-        scratch=[((LANES, low.shape[1]), bf16), ((D, LANES), f32)],
-    )
-    (cols,) = call(total_kernel, [to_tp32], trace, exchange(shares, TP))
-    cols = exchange(cols, TP)
-    (rows,) = call(square_kernel, [to_z32], cols, scratch=[(right[0], f32)])
+    (shares,) = call(
+        gram_kernel, [to_tp32], low, *whole, scratch=[((LANES, low.shape[1]), bf16), ((D, LANES), f32)]
+    )
+    gram, sent = call(total_kernel, [((SENT, LANES), f32)] * 2, exchange(shares, TP))
+    sent = jnp.broadcast_to(sent.astype(jnp.float16), to_tp[0])
+    cols = exchange(sent, TP).astype(f32)
+    rows, gram_cols = call(square_kernel, [to_z32, (right[0], f32)], gram, cols)
     rows = both_cores(exchange(rows, "z"))
     sent, poly_rows, current_rows, spectral = call(
-        first_kernel, [to_tp, left, left, ((8, LANES), f32)], rows, cols, scratch=[right]
+        first_kernel, [to_tp, left, left, ((8, LANES), f32)], rows, gram_cols, scratch=[right]
     )
     cols, rows = call(second_kernel, [to_tp, to_z], current_rows, exchange(sent, TP), scratch=[right])
     rows = both_cores(exchange(rows, "z"))
@@ -418,16 +486,15 @@
         fourth_kernel, [to_tp, left], rows, right_poly, kept, rows_kept, scratch=[left]
     )
     (cols,) = call(fifth_kernel, [to_tp], product_rows, exchange(cols, TP), scratch=[right])
-    (product,) = call(last_kernel, [right], exchange(cols, TP))
-
-    whole_product = product.reshape(BLOCKS, LANES, LANES)[:, :COLS].reshape(2, D // 2, LANES)
-    over_rows = (((0,), (0,)), ((), ()))
-    ortho = sum(
-        lax.dot_general(whole_product[h, :, :COLS], whole[h], over_rows, preferred_element_type=f32)
-        for h in range(2)
-    )
-    ortho = ortho * jnp.sqrt(2.0 * FF / spectral[0, 0])
-    return gate_next, up_next, ortho[:, :half], ortho[:, half : 2 * half]
+    ortho_gate, ortho_up = call(
+        last_kernel,
+        [((COLS, half), f32)] * 2,
+        exchange(cols, TP),
+        *whole,
+        spectral,
+        scratch=[((D, LANES), bf16)],
+    )
+    return gate_next, up_next, ortho_gate, ortho_up
 
 
 def solution(mesh):

time: 252 us -> 243 us (0.964)
  waiting for transfers between devices: 23.8 us -> 11.1 us
  blocking collectives: 205 us -> 216 us
  starting transfers between devices: 10.1 us -> 5.22 us
    all_to_all x2 -> x1, waiting for transfers between devices: 23.8 us -> 11.1 us  [exchange(): lax.all_to_all(stacked, axes, split_axis=0, concat_axis=0, tiled=True)]
    all_to_all x7 -> x8, blocking collectives: 157 us -> 167 us  [exchange(): lax.all_to_all(stacked, axes, split_axis=0, concat_axis=0, tiled=True)]
    all_to_all x2 -> x1, starting transfers between devices: 10.1 us -> 5.22 us  [exchange(): lax.all_to_all(stacked, axes, split_axis=0, concat_axis=0, tiled=True)]
  transfers between devices with their start and end apart: 2 -> 1, of which waited for: 2 -> 1; matrix products, arithmetic and copies ran while one was open for 0% -> 0% of each run, Pallas kernels for 0% -> 0%
where the time goes in v6:
time: 243 us
  blocking collectives  216 us (89%)
  waiting for transfers between devices  11.1 us (5%)
  Pallas kernels  7.98 us (3%)
  starting transfers between devices  5.22 us (2%)
    all_to_all x8, blocking collectives, exchange(): lax.all_to_all(stacked, axes, split_axis=0, concat_axis=0, tiled=True)  167 us
    all_gather x1, blocking collectives, local(): by_z = lax.all_gather(low, 'z')  37.4 us
    all_to_all x1, waiting for transfers between devices, exchange(): lax.all_to_all(stacked, axes, split_axis=0, concat_axis=0, tiled=True)  11.1 us
    pallas_call x9, Pallas kernels, call(): pl.pallas_call(kernel, out_shape=[jax.ShapeDtypeStruct(shape, dtype) for...  7.98 us
    all_gather x3, blocking collectives, both_cores(): return lax.all_gather(by_z, 'core')  6.62 us
    all_to_all x1, starting transfers between devices, exchange(): lax.all_to_all(stacked, axes, split_axis=0, concat_axis=0, tiled=True)  5.22 us
  transfers between devices with their start and end apart: 1, of which 1 were waited for; matrix products, arithmetic and copies ran while one was open for 0% of the time, Pallas kernels for 0%

profile of v6, /device:TPU:8, one launch (start us, length us, event | category | flops | bytes accessed | tf_op | source)
XLA Modules:
  0.0 242.7 jit_solution(10032575773766934504)
XLA Ops:
  0.6 1.7 fusion.3
  2.3 0.1 fusion.2.low
  2.4 37.4 %all-gather = bf16[1056,384]{1,0:T(8,128)(2,1)S(1)} all-gather(bf16[88,384]{1,0:T(8,128)(2,1)S(1)} %fusion.2.low), channel_id=2, replica_groups=mesh['z'=12,'core'=2,'y'=8,'x'=4] {'z'}, dimensions={0}, use_global_device_ids=true | all-gather | bytes 878592 | tf_op jit(solution)/shard_map/all_gather | solution.py:451
  39.8 0.1 fusion.5
  39.9 2.4 all-gather.1
  42.3 2.4 all-gather.2
  44.6 0.7 gram_kernel.1
  45.3 32.1 %all_to_all.45.arrived = f32[32,48,128]{2,1,0:T(8,128)S(1)} all-to-all(f32[32,48,128]{2,1,0:T(8,128)S(1)} %gram_kernel.1), channel_id=1, replica_groups=mesh['z'=12,'core'=2,'y'=8,'x'=4] {'y','x'}, dimensions={0} | all-to-all | bytes 1572864 | tf_op jit(solution)/shard_map/all_to_all | solution.py:438
  77.5 0.4 total_kernel.1
  77.9 0.1 broadcast_in_dim.3
  77.9 19.8 %all_to_all.46 = f16[32,48,128]{2,1,0:T(8,128)(2,1)S(1)} all-to-all(f16[32,48,128]{2,1,0:T(8,128)(2,1)S(1)} %broadcast_in_dim.3), channel_id=1, replica_groups=mesh['z'=12,'core'=2,'y'=8,'x'=4] {'y','x'}, dimensions={0} | all-to-all | bytes 786432 | tf_op jit(solution)/shard_map/all_to_all | solution.py:438
  97.7 0.1 convert_element_type.17.cols
  97.7 0.9 square_kernel.1
  98.6 18.6 %all_to_all.47 = f32[12,56,128]{2,1,0:T(8,128)S(1)} all-to-all(f32[12,56,128]{2,1,0:T(8,128)S(1)} %get-tuple-element.24), channel_id=1, replica_groups=mesh['z'=12,'core'=2,'y'=8,'x'=4] {'z'}, dimensions={0} | all-to-all | bytes 688128 | tf_op jit(solution)/shard_map/all_to_all | solution.py:438
  117.2 2.3 all-gather.3
  119.5 1.0 first_kernel.1
  120.5 21.3 %all_to_all.48.cols = bf16[32,48,128]{2,1,0:T(8,128)(2,1)S(1)} all-to-all(bf16[32,48,128]{2,1,0:T(8,128)(2,1)S(1)} %get-tuple-element.28), channel_id=1, replica_groups=mesh['z'=12,'core'=2,'y'=8,'x'=4] {'y','x'}, dimensions={0} | all-to-all | bytes 786432 | tf_op jit(solution)/shard_map/all_to_all | solution.py:438
  141.9 1.3 second_kernel.1
  143.1 15.2 %all_to_all.49 = bf16[12,56,128]{2,1,0:T(8,128)(2,1)S(1)} all-to-all(bf16[12,56,128]{2,1,0:T(8,128)(2,1)S(1)} %get-tuple-element.29), channel_id=1, replica_groups=mesh['z'=12,'core'=2,'y'=8,'x'=4] {'z'}, dimensions={0} | all-to-all | bytes 344064 | tf_op jit(solution)/shard_map/all_to_all | solution.py:438
  158.4 5.2 %all-to-all-start.5 = ((bf16[32,48,128]{2,1,0:T(8,128)(2,1)}), bf16[32,48,128]{2,1,0:T(8,128)(2,1)S(1)}, u32[]{:S(2)}, u32[]{:S(2)}) async-start(bf16[32,48,128]{2,1,0:T(8,128)(2,1)} %get-tuple-element.30), calls=%async_computation.5 | async-start | bytes 786432 | tf_op jit(solution)/shard_map/all_to_all | solution.py:438
  163.6 2.1 all-gather.4
  165.6 11.1 %all-to-all-done.5.cols = bf16[32,48,128]{2,1,0:T(8,128)(2,1)S(1)} async-done(((bf16[32,48,128]{2,1,0:T(8,128)(2,1)}), bf16[32,48,128]{2,1,0:T(8,128)(2,1)S(1)}, u32[]{:S(2)}, u32[]{:S(2)}) %all-to-all-start.5) | async-done | bytes 393248 | tf_op jit(solution)/shard_map/all_to_all | solution.py:438
  176.7 1.1 third_kernel.1
  177.9 20.2 %all_to_all.50 = bf16[12,112,128]{2,1,0:T(8,128)(2,1)S(1)} all-to-all(bf16[12,112,128]{2,1,0:T(8,128)(2,1)S(1)} %get-tuple-element.31), channel_id=1, replica_groups=mesh['z'=12,'core'=2,'y'=8,'x'=4] {'z'}, dimensions={0} | all-to-all | bytes 688128 | tf_op jit(solution)/shard_map/all_to_all | solution.py:438
  198.1 2.3 all-gather.5
  200.4 0.6 fourth_kernel.1
  201.0 21.0 %all_to_all.51.cols = bf16[32,48,128]{2,1,0:T(8,128)(2,1)S(1)} all-to-all(bf16[32,48,128]{2,1,0:T(8,128)(2,1)S(1)} %get-tuple-element.36), channel_id=1, replica_groups=mesh['z'=12,'core'=2,'y'=8,'x'=4] {'y','x'}, dimensions={0} | all-to-all | bytes 786432 | tf_op jit(solution)/shard_map/all_to_all | solution.py:438
  222.0 0.5 fifth_kernel.1
  222.5 18.7 %all_to_all.52.cols = bf16[32,48,128]{2,1,0:T(8,128)(2,1)S(1)} all-to-all(bf16[32,48,128]{2,1,0:T(8,128)(2,1)S(1)} %fifth_kernel.1), channel_id=1, replica_groups=mesh['z'=12,'core'=2,'y'=8,'x'=4] {'y','x'}, dimensions={0} | all-to-all | bytes 786432 | tf_op jit(solution)/shard_map/all_to_all | solution.py:438
  241.2 1.5 last_kernel.1
  (1 shorter events, 0.0 us)
Async XLA Ops:
  158.4 18.4 %all-to-all-start.5 = ((bf16[32,48,128]{2,1,0:T(8,128)(2,1)}), bf16[32,48,128]{2,1,0:T(8,128)(2,1)S(1)}, u32[]{:S(2)}, u32[]{:S(2)}) async-start(bf16[32,48,128]{2,1,0:T(8,128)(2,1)} %get-tuple-element.30), calls=%async_computation.5 | async-start | bytes 786432 | tf_op jit(solution)/shard_map/all_to_all | solution.py:438

commit v7 on v6

--- a/solution.py
+++ b/solution.py
@@ -27,7 +27,7 @@
 FREE = 96
 SPARE = 48
 KDIM = BLOCKS * LANES
-f32, bf16 = jnp.float32, jnp.bfloat16
+f32, bf16, f16 = jnp.float32, jnp.bfloat16, jnp.float16
 
 
 def place(core, z):
@@ -178,83 +178,127 @@
     copies(out, pack_tp(block[:MAIN], block[MAIN:ROWS], at[3], tail))
 
 
-def gram_kernel(low, whole0, whole1, out, own, share):
-    own[:COLS] = low[...]
-    own[COLS:] = jnp.zeros((LANES - COLS, own.shape[1]), bf16)
-    half = D // 2
-    for h, whole in enumerate((whole0, whole1)):
-        share[h * half : (h + 1) * half] = lax.dot_general(
-            whole[...], own[...], (((1,), (1,)), ((), ())), preferred_element_type=f32
-        )
-    for t in range(TPS):
-        group, q = divmod(t, 4)
-        shared = share[SHARED + 8 * group : SHARED + 8 * group + 8]
-        out[t] = pack_tp(share[MAIN * t : MAIN * (t + 1)], shared, (FREE - PIECE * q) % LANES)
-
-
 def eleven_bits(value):
     moved = value * 8193.0
     return moved - (moved - value)
 
 
-def total_kernel(arrived, gram, out):
-    at = position()
-    total = arrived[0]
-    for t in range(1, TPS):
-        total += arrived[t]
-    gram[...] = total
-    most = jnp.max(jnp.abs(total), keepdims=True)
+def float16_scale(most):
     scale, factors = jnp.ones((1, 1), f32), []
-    for power in (-12, *(14,) * 8, 7, 4, 2, 1):
+    for power in (*(-14,) * 5, *(14,) * 8, 7, 4, 2, 1):
         up = 2.0**power
         take = most >= 2.0**15 if power < 0 else most < 2.0 ** (15 - power)
         most = jnp.where(take, most * up, most)
         scale = jnp.where(take, scale * up, scale)
         factors.append(jnp.where(take, 1.0 / up, 1.0))
+    return scale, factors
+
+
+FACTORS = 17
+WORDS = 32
+
+
+def with_row(tail, at, lane, values):
+    row, lanes = rows_of(8), lanes_of(8)
+    for i, value in enumerate(values):
+        tail = jnp.where((row == at) & (lanes == lane + i), value, tail)
+    return tail
+
+
+def with_factors(tail, at, lane, factors):
+    row, lanes = rows_of(8), lanes_of(8)
+    tail = jnp.where((row == at) & (lanes >= lane) & (lanes < lane + WORDS), 1.0, tail)
+    return with_row(tail, at, lane, factors)
+
+
+def products(tail):
+    for shift in (1, 2, 4, 8, 16):
+        tail = tail * pltpu.roll(tail, LANES - shift, 1)
+    return tail
+
+
+def tail_tp(left, factors):
+    left, row = jnp.broadcast_to(left, (8, LANES)), rows_of(8)
+    tail = jnp.where(
+        row == 0,
+        pltpu.roll(left, FREE, 1),
+        jnp.where(row == 1, pltpu.roll(left, FREE - 32, 1), pltpu.roll(left, FREE - 64, 1)),
+    )
+    return with_factors(tail, 7, FREE, factors)
+
+
+def left_tp(tail):
+    lane = lanes_of(1)
+    return jnp.where(
+        lane < 32,
+        pltpu.roll(tail, 32, 1)[0:1],
+        jnp.where(lane < 64, pltpu.roll(tail, 64, 1)[1:2], pltpu.roll(tail, 96, 1)[2:3]),
+    )
+
+
+def own_square():
+    return (rows_of(LANES) == lanes_of(LANES)) & (rows_of(LANES) < COLS)
+
+
+def gram_kernel(low, whole0, whole1, out, own, share):
+    at = position()
+    own[:COLS] = low[...]
+    own[COLS:] = jnp.zeros((LANES - COLS, own.shape[1]), bf16)
+    half = D // 2
+    most = jnp.zeros((1, 1), f32)
+    for h, whole in enumerate((whole0, whole1)):
+        part = lax.dot_general(
+            whole[...], own[...], (((1,), (1,)), ((), ())), preferred_element_type=f32
+        )
+        share[h * half : (h + 1) * half] = part
+        most = jnp.maximum(most, jnp.max(jnp.abs(part), keepdims=True))
+    scale, factors = float16_scale(most)
+    mine = share[pl.ds(pl.multiple_of(at[2], 8), COLS), :] * scale
+    eye = rows_of(COLS) == lanes_of(COLS)
+    left = jnp.sum(jnp.where(eye, mine - eleven_bits(mine), 0.0), axis=0, keepdims=True)
+    tail = tail_tp(eleven_bits(left), factors)
+    for t in range(TPS):
+        group, q = divmod(t, 4)
+        main = eleven_bits(share[MAIN * t : MAIN * (t + 1)] * scale)
+        shared = eleven_bits(share[SHARED + 8 * group : SHARED + 8 * group + 8] * scale)
+        out[t] = pack_tp(main, shared, (FREE - PIECE * q) % LANES, tail)
+
+
+def total_kernel(arrived, gram, out):
+    at = position()
+    total, left = jnp.zeros((SENT, LANES), f32), jnp.zeros((8, LANES), f32)
+    for t in range(TPS):
+        tail = arrived[t, 40:]
+        inverse = products(tail)[7:8, FREE : FREE + 1]
+        total += arrived[t] * inverse
+        left += tail * inverse
+    piece = pltpu.roll(total[32:40], LANES - at[3], 1)
+    piece = jnp.where(lanes_of(8) // PIECE == at[5], piece, 0.0)
+    total = jnp.concatenate([total[:48], unfolded(total), piece], axis=0)
+    total = jnp.where(lanes_of(ROWS) < COLS, total, 0.0)
+    eye = own_eye(at) & ((rows_of(ROWS) < MAIN) | (lanes_of(ROWS) // PIECE == at[5]))
+    total += jnp.where(eye, left_tp(left), 0.0)
+    gram[...] = total
+    scale, factors = float16_scale(jnp.max(jnp.abs(total), keepdims=True))
     total = total * scale
     high = eleven_bits(total)
-    rest = total - high
-    piece = pltpu.roll(rest[32:40], LANES - at[3], 1)
-    parts = (rest[:48], unfolded(rest), jnp.where(lanes_of(8) // PIECE == at[5], piece, 0.0))
-    left = sum(
-        jnp.sum(jnp.where(eye_of(at, first, p.shape[0], at[2]), p, 0.0), axis=0, keepdims=True)
-        for first, p in zip((0, 48, MAIN), parts)
-    )
-    left = jnp.broadcast_to(eleven_bits(left), (8, LANES))
-    row, lane = rows_of(8), lanes_of(8)
-    tail = jnp.where(
-        row == 0, pltpu.roll(left, FREE, 1), jnp.where(row == 1, pltpu.roll(left, FREE - 32, 1), pltpu.roll(left, FREE - 64, 1))
-    )
-    for i, factor in enumerate(factors):
-        tail = jnp.where((row == 7) & (lane == FREE + i), factor, tail)
-    tail = jnp.where((row == 7) & (lane >= FREE + len(factors)), 1.0, tail)
-    out[:40] = high[:40]
-    out[40:] = jnp.where(lane < FREE, high[40:], tail)
+    left = jnp.sum(jnp.where(eye, total - high, 0.0), axis=0, keepdims=True)
+    out[...] = pack_tp(high[:MAIN], high[MAIN:], at[3], tail_tp(eleven_bits(left), factors))
 
 
 def square_kernel(gram, cols, out, whole):
     at = position()
-    lane = lanes_of(8)
     left = jnp.zeros((8, LANES), f32)
     inverses = []
     for t in range(TPS):
-        tail = cols[t, 40:48]
-        product = tail
-        for shift in (1, 2, 4, 8):
-            product = product * pltpu.roll(product, LANES - shift, 1)
-        inverses.append(product[7:8, FREE : FREE + 1])
+        tail = cols[t, 40:]
+        inverses.append(products(tail)[7:8, FREE : FREE + 1])
         left += tail * inverses[t]
     unpack_columns(cols, whole, scales=inverses)
-    left = jnp.where(
-        lane[:1] < 32,
-        pltpu.roll(left, 32, 1)[0:1],
-        jnp.where(lane[:1] < 64, pltpu.roll(left, 64, 1)[1:2], pltpu.roll(left, 96, 1)[2:3]),
-    )
     own = pl.ds(pl.multiple_of(at[4], LANES), LANES)
-    eye = (rows_of(LANES) == lanes_of(LANES)) & (rows_of(LANES) < COLS)
-    mine = whole[own, :] + jnp.where(eye, left, 0.0)
+    mine = whole[own, :] + jnp.where(own_square(), left_tp(left), 0.0)
     whole[own, :] = mine
-    trace = jnp.sum(jnp.where(eye, mine, 0.0), keepdims=True)
+    trace = jnp.sum(jnp.where(own_square(), mine, 0.0), keepdims=True)
     square = jnp.zeros((LANES, LANES), f32)
     for block in range(BLOCKS):
         value = whole[block * LANES : (block + 1) * LANES, :]
@@ -263,22 +307,36 @@
     shared = at[1] + MAIN
     start = (shared // COLS) * LANES + shared % COLS
     shared = whole[pl.ds(pl.multiple_of(start, 8), 8), :]
-    value = jnp.concatenate([gram[:48], unfolded(gram), shared], axis=0)
-    row = rows_of(8)
-    tail = jnp.where((row == 0) & (lane == COLS), square, jnp.where((row == 0) & (lane == COLS + 1), trace, 0.0))
-    copies(out, pack_z(value, tail))
+    value = jnp.concatenate([gram[:MAIN], jnp.where(lanes_of(8) < COLS, shared, 0.0)], axis=0)
+    scale, factors = float16_scale(jnp.max(jnp.abs(value), keepdims=True))
+    value = value * scale
+    high = eleven_bits(value)
+    left = jnp.sum(jnp.where(own_eye(at), value - high, 0.0), axis=0, keepdims=True)
+    tail = with_factors(spread(eleven_bits(left)), 3, COLS, factors)
+    for i, number in enumerate((square, trace)):
+        scale, factors = float16_scale(number)
+        rest, words = number * scale, []
+        for _ in range(3):
+            words.append(eleven_bits(rest))
+            rest = rest - words[-1]
+        tail = with_row(with_factors(tail, 4 + i, COLS, factors), 4 + i, COLS + WORDS, words)
+    out[...] = pack_z(high, tail)
 
 
 def first_kernel(rows, whole, out, poly_rows, current_rows, spectral_out, right):
     at = position()
-    tails = jnp.zeros((WIDE - SPARE, LANES), f32)
+    inverses = {}
+    square, trace = jnp.zeros((1, 1), f32), jnp.zeros((1, 1), f32)
     for core in range(2):
         for z in range(DEPTH):
-            tails += rows[core, z, SPARE:WIDE]
-    spot = rows_of(WIDE - SPARE) == 0
-    lane = lanes_of(WIDE - SPARE)
-    square = jnp.sum(jnp.where(spot & (lane == COLS), tails, 0.0), keepdims=True)
-    trace = jnp.sum(jnp.where(spot & (lane == COLS + 1), tails, 0.0), keepdims=True)
+            tail = rows[core, z, SPARE:WIDE]
+            factor = products(tail)[:, COLS : COLS + 1]
+            word = (tail[:, COLS + WORDS + 2 : COLS + WORDS + 3] + tail[:, COLS + WORDS + 1 : COLS + WORDS + 2]) + tail[
+                :, COLS + WORDS : COLS + WORDS + 1
+            ]
+            inverses[place(core, z)] = factor[3:4]
+            square += word[4:5] * factor[4:5]
+            trace += word[5:6] * factor[5:6]
     spectral = 2.0 * square / (trace + EPS)
     inverse = 1.0 / spectral
     spectral_out[...] = jnp.broadcast_to(spectral, spectral_out.shape)
@@ -286,15 +344,13 @@
         part = pl.ds(block * LANES, LANES)
         right[part, :] = (-0.5 * (whole[part, :] * inverse)).astype(bf16)
     own = pl.ds(pl.multiple_of(at[4], LANES), LANES)
-    eye = (rows_of(LANES) == lanes_of(LANES)) & (rows_of(LANES) < COLS)
-    right[own, :] = poly(eye, whole[own, :] * inverse).astype(bf16)
+    right[own, :] = poly(own_square(), whole[own, :] * inverse).astype(bf16)
 
     def of_rows(part, first, col, packed):
-        current = part * inverse
-        return (
-            poly(eye_of(at, first, part.shape[0], col), current).astype(bf16),
-            current.astype(bf16),
-        )
+        eye = eye_of(at, first, part.shape[0], col)
+        whole_part = jnp.where(eye, part + gathered(packed), part) * inverses[col // COLS]
+        current = whole_part * inverse
+        return poly(eye, current).astype(bf16), current.astype(bf16)
 
     unpack_rows(rows, at, (poly_rows, current_rows), of_rows)
     send_tp(at, out, dot(poly_rows[...], right[...]))
@@ -457,16 +513,17 @@
     left = ((ROWS, KDIM), bf16)
     block = ((ROWS, LANES), f32)
     to_tp, to_z = ((TPS, SENT, LANES), bf16), ((DEPTH, WIDE, LANES), bf16)
-    to_tp32, to_z32 = (to_tp[0], f32), (to_z[0], f32)
+    to_tp32 = (to_tp[0], f32)
 
     (shares,) = call(
         gram_kernel, [to_tp32], low, *whole, scratch=[((LANES, low.shape[1]), bf16), ((D, LANES), f32)]
     )
-    gram, sent = call(total_kernel, [((SENT, LANES), f32)] * 2, exchange(shares, TP))
-    sent = jnp.broadcast_to(sent.astype(jnp.float16), to_tp[0])
-    cols = exchange(sent, TP).astype(f32)
-    rows, gram_cols = call(square_kernel, [to_z32, (right[0], f32)], gram, cols)
-    rows = both_cores(exchange(rows, "z"))
+    shares = exchange(shares.astype(f16), TP).astype(f32)
+    gram, sent = call(total_kernel, [((ROWS, LANES), f32), ((SENT, LANES), f32)], shares)
+    cols = exchange(jnp.broadcast_to(sent.astype(f16), to_tp[0]), TP).astype(f32)
+    sent, gram_cols = call(square_kernel, [((WIDE, LANES), f32), (right[0], f32)], gram, cols)
+    rows = exchange(jnp.broadcast_to(sent.astype(f16), to_z[0]), "z")
+    rows = both_cores(rows).astype(f32)
     sent, poly_rows, current_rows, spectral = call(
         first_kernel, [to_tp, left, left, ((8, LANES), f32)], rows, gram_cols, scratch=[right]
     )

time: 243 us -> 231 us (0.951)
  blocking collectives: 216 us -> 202 us
    all_to_all x8, blocking collectives: 167 us -> 154 us  [exchange(): lax.all_to_all(stacked, axes, split_axis=0, concat_axis=0, tiled=True)]
where the time goes in v7:
time: 231 us
  blocking collectives  202 us (87%)
  waiting for transfers between devices  11.1 us (5%)
  Pallas kernels  9.39 us (4%)
  starting transfers between devices  5.23 us (2%)
    all_to_all x8, blocking collectives, exchange(): lax.all_to_all(stacked, axes, split_axis=0, concat_axis=0, tiled=True)  154 us
    all_gather x1, blocking collectives, local(): by_z = lax.all_gather(low, 'z')  37.4 us
    all_to_all x1, waiting for transfers between devices, exchange(): lax.all_to_all(stacked, axes, split_axis=0, concat_axis=0, tiled=True)  11.1 us
    pallas_call x9, Pallas kernels, call(): pl.pallas_call(kernel, out_shape=[jax.ShapeDtypeStruct(shape, dtype) for...  9.39 us
    all_gather x3, blocking collectives, both_cores(): return lax.all_gather(by_z, 'core')  6.38 us
    all_to_all x1, starting transfers between devices, exchange(): lax.all_to_all(stacked, axes, split_axis=0, concat_axis=0, tiled=True)  5.23 us
    all_gather x2, blocking collectives, local(): lax.all_gather(by_z[h * NEAR:(h + 1) * NEAR], 'core').reshape(D // 2, -1)  4.76 us
  transfers between devices with their start and end apart: 1, of which 1 were waited for; matrix products, arithmetic and copies ran while one was open for 0% of the time, Pallas kernels for 0%

profile of v7, /device:TPU:8, one launch (start us, length us, event | category | flops | bytes accessed | tf_op | source)
XLA Modules:
  0.0 230.8 jit_solution(17834262840295885074)
XLA Ops:
  0.6 1.7 fusion.3
  2.3 0.1 fusion.2.low
  2.4 37.4 %all-gather = bf16[1056,384]{1,0:T(8,128)(2,1)S(1)} all-gather(bf16[88,384]{1,0:T(8,128)(2,1)S(1)} %fusion.2.low), channel_id=2, replica_groups=mesh['z'=12,'core'=2,'y'=8,'x'=4] {'z'}, dimensions={0}, use_global_device_ids=true | all-gather | bytes 878592 | tf_op jit(solution)/shard_map/all_gather | solution.py:507
  39.8 0.1 fusion.5
  39.9 2.4 %all-gather.1 = bf16[12,88,384]{2,1,0:T(8,128)(2,1)S(1)} all-gather(bf16[6,88,384]{2,1,0:T(8,128)(2,1)S(1)} %bitcast.15), channel_id=3, replica_groups=mesh['z'=12,'core'=2,'y'=8,'x'=4] {'core'}, dimensions={0}, use_global_device_ids=true | all-gather | bytes 1216512 | tf_op jit(solution)/shard_map/all_gather | solution.py:509
  42.3 2.4 %all-gather.2 = bf16[12,88,384]{2,1,0:T(8,128)(2,1)S(1)} all-gather(bf16[6,88,384]{2,1,0:T(8,128)(2,1)S(1)} %bitcast.14), channel_id=4, replica_groups=mesh['z'=12,'core'=2,'y'=8,'x'=4] {'core'}, dimensions={0}, use_global_device_ids=true | all-gather | bytes 1216512 | tf_op jit(solution)/shard_map/all_gather | solution.py:509
  44.6 1.1 gram_kernel.1
  45.7 0.1 convert_element_type.28
  45.8 25.0 %all_to_all.45 = f16[32,48,128]{2,1,0:T(8,128)(2,1)S(1)} all-to-all(f16[32,48,128]{2,1,0:T(8,128)(2,1)S(1)} %convert_element_type.28), channel_id=1, replica_groups=mesh['z'=12,'core'=2,'y'=8,'x'=4] {'y','x'}, dimensions={0} | all-to-all | bytes 786432 | tf_op jit(solution)/shard_map/all_to_all | solution.py:494
  70.7 0.1 convert_element_type.29.arrived
  70.8 0.8 total_kernel.1
  71.6 0.1 broadcast_in_dim.6
  71.7 18.7 %all_to_all.46 = f16[32,48,128]{2,1,0:T(8,128)(2,1)S(1)} all-to-all(f16[32,48,128]{2,1,0:T(8,128)(2,1)S(1)} %broadcast_in_dim.6), channel_id=1, replica_groups=mesh['z'=12,'core'=2,'y'=8,'x'=4] {'y','x'}, dimensions={0} | all-to-all | bytes 786432 | tf_op jit(solution)/shard_map/all_to_all | solution.py:494
  90.4 0.1 convert_element_type.31.cols
  90.4 1.0 square_kernel.1
  91.5 15.1 %all_to_all.47 = f16[12,56,128]{2,1,0:T(8,128)(2,1)S(1)} all-to-all(f16[12,56,128]{2,1,0:T(8,128)(2,1)S(1)} %broadcast_in_dim.7), channel_id=1, replica_groups=mesh['z'=12,'core'=2,'y'=8,'x'=4] {'z'}, dimensions={0} | all-to-all | bytes 344064 | tf_op jit(solution)/shard_map/all_to_all | solution.py:494
  106.7 2.0 all-gather.3
  108.7 1.4 first_kernel.1
  110.2 19.7 %all_to_all.48.cols = bf16[32,48,128]{2,1,0:T(8,128)(2,1)S(1)} all-to-all(bf16[32,48,128]{2,1,0:T(8,128)(2,1)S(1)} %get-tuple-element.28), channel_id=1, replica_groups=mesh['z'=12,'core'=2,'y'=8,'x'=4] {'y','x'}, dimensions={0} | all-to-all | bytes 786432 | tf_op jit(solution)/shard_map/all_to_all | solution.py:494
  129.9 1.3 second_kernel.1
  131.2 15.2 %all_to_all.49 = bf16[12,56,128]{2,1,0:T(8,128)(2,1)S(1)} all-to-all(bf16[12,56,128]{2,1,0:T(8,128)(2,1)S(1)} %get-tuple-element.29), channel_id=1, replica_groups=mesh['z'=12,'core'=2,'y'=8,'x'=4] {'z'}, dimensions={0} | all-to-all | bytes 344064 | tf_op jit(solution)/shard_map/all_to_all | solution.py:494
  146.4 5.2 %all-to-all-start.5 = ((bf16[32,48,128]{2,1,0:T(8,128)(2,1)}), bf16[32,48,128]{2,1,0:T(8,128)(2,1)S(1)}, u32[]{:S(2)}, u32[]{:S(2)}) async-start(bf16[32,48,128]{2,1,0:T(8,128)(2,1)} %get-tuple-element.30), calls=%async_computation.5 | async-start | bytes 786432 | tf_op jit(solution)/shard_map/all_to_all | solution.py:494
  151.7 2.1 all-gather.4
  153.7 11.1 %all-to-all-done.5.cols = bf16[32,48,128]{2,1,0:T(8,128)(2,1)S(1)} async-done(((bf16[32,48,128]{2,1,0:T(8,128)(2,1)}), bf16[32,48,128]{2,1,0:T(8,128)(2,1)S(1)}, u32[]{:S(2)}, u32[]{:S(2)}) %all-to-all-start.5) | async-done | bytes 393248 | tf_op jit(solution)/shard_map/all_to_all | solution.py:494
  164.8 1.1 third_kernel.1
  166.0 20.2 %all_to_all.50 = bf16[12,112,128]{2,1,0:T(8,128)(2,1)S(1)} all-to-all(bf16[12,112,128]{2,1,0:T(8,128)(2,1)S(1)} %get-tuple-element.31), channel_id=1, replica_groups=mesh['z'=12,'core'=2,'y'=8,'x'=4] {'z'}, dimensions={0} | all-to-all | bytes 688128 | tf_op jit(solution)/shard_map/all_to_all | solution.py:494
  186.2 2.3 all-gather.5
  188.5 0.6 fourth_kernel.1
  189.0 21.0 %all_to_all.51.cols = bf16[32,48,128]{2,1,0:T(8,128)(2,1)S(1)} all-to-all(bf16[32,48,128]{2,1,0:T(8,128)(2,1)S(1)} %get-tuple-element.36), channel_id=1, replica_groups=mesh['z'=12,'core'=2,'y'=8,'x'=4] {'y','x'}, dimensions={0} | all-to-all | bytes 786432 | tf_op jit(solution)/shard_map/all_to_all | solution.py:494
  210.1 0.5 fifth_kernel.1
  210.6 18.7 %all_to_all.52.cols = bf16[32,48,128]{2,1,0:T(8,128)(2,1)S(1)} all-to-all(bf16[32,48,128]{2,1,0:T(8,128)(2,1)S(1)} %fifth_kernel.1), channel_id=1, replica_groups=mesh['z'=12,'core'=2,'y'=8,'x'=4] {'y','x'}, dimensions={0} | all-to-all | bytes 786432 | tf_op jit(solution)/shard_map/all_to_all | solution.py:494
  229.3 1.5 last_kernel.1
  (4 shorter events, 0.1 us)
Async XLA Ops:
  146.4 18.4 %all-to-all-start.5 = ((bf16[32,48,128]{2,1,0:T(8,128)(2,1)}), bf16[32,48,128]{2,1,0:T(8,128)(2,1)S(1)}, u32[]{:S(2)}, u32[]{:S(2)}) async-start(bf16[32,48,128]{2,1,0:T(8,128)(2,1)} %get-tuple-element.30), calls=%async_computation.5 | async-start | bytes 786432 | tf_op jit(solution)/shard_map/all_to_all | solution.py:494

commit v8 on v5

v8 whole, which is shorter than its diff:
```python
import jax
import jax.numpy as jnp
from jax import lax
from jax.experimental import pallas as pl
from jax.experimental.pallas import tpu as pltpu
from jax.sharding import Mesh
from jax.sharding import PartitionSpec as P

FF = 5632
FS = ("z", "core")
TP = ("y", "x")
BETA = 0.95
EPS = 1e-06
LANES = 128
D = 2112
COLS = 88
BLOCKS = D // COLS
DEPTH = 12
NEAR = 6
TPS = 32
MAIN = 64
LAST = TPS * MAIN
PAIR = 2
ROWS = MAIN + 8
SENT = 48
FREE = 96
KDIM = BLOCKS * LANES
WORDS = 32
f32, bf16, f16 = jnp.float32, jnp.bfloat16, jnp.float16


def place(core, z):
    return ((z // NEAR) * 2 + core) * NEAR + z % NEAR


def lanes_of(rows):
    return lax.broadcasted_iota(jnp.int32, (rows, LANES), 1)


def rows_of(rows):
    return lax.broadcasted_iota(jnp.int32, (rows, LANES), 0)


def position():
    own = place(lax.axis_index("core"), lax.axis_index("z"))
    t = lax.axis_index("y") * 4 + lax.axis_index("x")
    return t * MAIN, LAST + PAIR * t - MAIN, own * COLS, own * LANES


def pack(block, tail=None):
    lane, low = lanes_of(16), block[48:MAIN]
    a, b, c = (
        jnp.where(lane < COLS, block[16 * i : 16 * i + 16], pltpu.roll(low, shift, 1))
        for i, shift in enumerate((COLS, COLS - 40, COLS - 80))
    )
    last, row = block[MAIN:ROWS], rows_of(8)
    pair = jnp.where(
        row < 2,
        pltpu.roll(last, FREE, 1),
        jnp.where(
            row < 4,
            pltpu.roll(pltpu.roll(last, FREE - 32, 1), 2, 0),
            pltpu.roll(pltpu.roll(last, FREE - 64, 1), 4, 0),
        ),
    )
    used = lanes_of(8) < FREE
    end = c[8:] if tail is None else jnp.where(used, c[8:], tail)
    return jnp.concatenate([a, b, jnp.where(used, c[:8], pair), end], axis=0)


def low_rows(packed):
    lane = lanes_of(16)
    a, b, c = (
        pltpu.roll(packed[16 * i : 16 * i + 16].astype(f32), shift, 1)
        for i, shift in enumerate((40, 80, 120))
    )
    return jnp.where(lane < 40, a, jnp.where(lane < 80, b, c))


def last_rows(packed):
    part, lane = packed[32:40].astype(f32), lanes_of(8)
    a = pltpu.roll(part, 32, 1)
    b = pltpu.roll(pltpu.roll(part, 64, 1), 6, 0)
    c = pltpu.roll(pltpu.roll(part, 96, 1), 4, 0)
    return jnp.where(lane < 32, a, jnp.where(lane < 64, b, c))


def parts_of(packed):
    return (0, packed), (48, low_rows(packed)), (MAIN, last_rows(packed))


def last_eight(blocks, group):
    row = rows_of(8)
    value = last_rows(blocks[4 * group])
    for q in (1, 2, 3):
        value = jnp.where(row < PAIR * q, value, pltpu.roll(last_rows(blocks[4 * group + q]), PAIR * q, 0))
    return value


def with_row(tail, at, lane, values):
    row, lanes = rows_of(8), lanes_of(8)
    for i, value in enumerate(values):
        tail = jnp.where((row == at) & (lanes == lane + i), value, tail)
    return tail


def with_factors(tail, at, factors):
    tail = jnp.where((rows_of(8) == at) & (lanes_of(8) >= FREE), 1.0, tail)
    return with_row(tail, at, FREE, factors)


def products(tail):
    for shift in (1, 2, 4, 8, 16):
        tail = tail * pltpu.roll(tail, LANES - shift, 1)
    return tail


def tail_of(row):
    row, at = jnp.broadcast_to(row, (8, LANES)), rows_of(8)
    return jnp.where(
        at == 0,
        pltpu.roll(row, FREE, 1),
        jnp.where(at == 1, pltpu.roll(row, FREE - 32, 1), pltpu.roll(row, FREE - 64, 1)),
    )


def row_in(tail):
    lane = lanes_of(1)
    return jnp.where(
        lane < 32,
        pltpu.roll(tail, 32, 1)[0:1],
        jnp.where(lane < 64, pltpu.roll(tail, 64, 1)[1:2], pltpu.roll(tail, 96, 1)[2:3]),
    )


def eleven_bits(value):
    moved = value * 8193.0
    return moved - (moved - value)


def float16_scale(most):
    scale, factors = jnp.ones((1, 1), f32), []
    for power in (*(-14,) * 5, *(14,) * 8, 7, 4, 2, 1):
        up = 2.0**power
        take = most >= 2.0**15 if power < 0 else most < 2.0 ** (15 - power)
        most = jnp.where(take, most * up, most)
        scale = jnp.where(take, scale * up, scale)
        factors.append(jnp.where(take, 1.0 / up, 1.0))
    return scale, factors


def store_rows(target, first, value):
    at, last = first, first + value.shape[0]
    while at < last:
        block, row = divmod(at, COLS)
        count = min(COLS - row, last - at)
        start = block * LANES + row
        target[start : start + count, :] = value[at - first : at - first + count].astype(target.dtype)
        at += count


def unpack_columns(blocks, target):
    for block in range(BLOCKS):
        target[block * LANES + COLS : (block + 1) * LANES, :] = jnp.zeros((LANES - COLS, LANES), target.dtype)
    for t in range(TPS):
        packed = blocks[t]
        store_rows(target, MAIN * t, packed)
        store_rows(target, MAIN * t + 48, low_rows(packed))
    for group in range(TPS // 4):
        store_rows(target, LAST + 8 * group, last_eight(blocks, group))


def eye_of(at, first, count, col):
    row = rows_of(count)
    use = lanes_of(count) < COLS
    if first >= MAIN:
        use &= row < PAIR
    return (row + ((at[0] if first < MAIN else at[1]) + first) == lanes_of(count) + col) & use


def own_eye(at):
    return jnp.concatenate([eye_of(at, 0, MAIN, at[2]), eye_of(at, MAIN, ROWS - MAIN, at[2])], axis=0)


def own_square():
    return (rows_of(LANES) == lanes_of(LANES)) & (rows_of(LANES) < COLS)


def poly(eye, current):
    return jnp.where(eye, 1.5 - 0.5 * current, -0.5 * current)


def dot(left, right):
    return jnp.dot(left, right, preferred_element_type=f32)


def copies(out, value):
    value = value.astype(out.dtype)
    for i in range(out.shape[0]):
        out[i] = value


def each_row_block(rows):
    for core in range(2):
        for z in range(DEPTH):
            b = place(core, z)
            yield b, slice(b * LANES, (b + 1) * LANES), rows[core, z]


def gram_kernel(low, whole0, whole1, out, own, share):
    at = position()
    own[:COLS] = low[...]
    own[COLS:] = jnp.zeros((LANES - COLS, own.shape[1]), bf16)
    half = D // 2
    most = jnp.zeros((1, 1), f32)
    for h, whole in enumerate((whole0, whole1)):
        part = lax.dot_general(
            whole[...], own[...], (((1,), (1,)), ((), ())), preferred_element_type=f32
        )
        share[h * half : (h + 1) * half] = part
        most = jnp.maximum(most, jnp.max(jnp.abs(part), keepdims=True))
    scale, factors = float16_scale(most)
    mine = share[pl.ds(pl.multiple_of(at[2], 8), COLS), :] * scale
    eye = rows_of(COLS) == lanes_of(COLS)
    left = jnp.sum(jnp.where(eye, mine - eleven_bits(mine), 0.0), axis=0, keepdims=True)
    tail = with_factors(tail_of(eleven_bits(left)), 7, factors)
    for group in range(TPS // 4):
        last = eleven_bits(share[LAST + 8 * group : LAST + 8 * group + 8] * scale)
        for q in range(4):
            t = 4 * group + q
            main = eleven_bits(share[MAIN * t : MAIN * (t + 1)] * scale)
            pair = pltpu.roll(last, 8 - PAIR * q, 0) if q else last
            out[t] = pack(jnp.concatenate([main, pair], axis=0), tail)


def total_kernel(arrived, out):
    at = position()
    total, left = jnp.zeros((SENT, LANES), f32), jnp.zeros((8, LANES), f32)
    for t in range(TPS):
        tail = arrived[t, 40:]
        inverse = products(tail)[7:8, FREE : FREE + 1]
        total += arrived[t] * inverse
        left += tail * inverse
    eye = own_eye(at)
    total = jnp.concatenate([part for _, part in parts_of(total)], axis=0)
    total = jnp.where((lanes_of(ROWS) < COLS) & (rows_of(ROWS) < MAIN + PAIR), total, 0.0)
    total += jnp.where(eye, row_in(left), 0.0)
    scale, factors = float16_scale(jnp.max(jnp.abs(total), keepdims=True))
    scaled = total * scale
    high = eleven_bits(scaled)
    left = eleven_bits(jnp.sum(jnp.where(eye, scaled - high, 0.0), axis=0, keepdims=True))
    out[...] = pack(high, with_factors(tail_of(left), 7, factors))


def square_kernel(own, cols, out, whole):
    at = position()
    left = jnp.zeros((8, LANES), f32)
    for t in range(TPS):
        tail = cols[t, 40:]
        inverse = products(tail)[7:8, FREE : FREE + 1]
        left += tail * inverse
        packed = cols[t] * inverse
        store_rows(whole, MAIN * t, packed)
        store_rows(whole, MAIN * t + 48, low_rows(packed))
        if t % 4 == 0:
            last = last_rows(packed)
        else:
            last = jnp.where(rows_of(8) < PAIR * (t % 4), last, pltpu.roll(last_rows(packed), PAIR * (t % 4), 0))
        if t % 4 == 3:
            store_rows(whole, LAST + 2 * (t - 3), last)
    for block in range(BLOCKS):
        whole[block * LANES + COLS : (block + 1) * LANES, :] = jnp.zeros((LANES - COLS, LANES), f32)
    mine = pl.ds(pl.multiple_of(at[3], LANES), LANES)
    value = whole[mine, :] + jnp.where(own_square(), row_in(left), 0.0)
    whole[mine, :] = value
    trace = jnp.sum(jnp.where(own_square(), value, 0.0), keepdims=True)
    square = jnp.zeros((LANES, LANES), f32)
    for block in range(BLOCKS):
        value = whole[block * LANES : (block + 1) * LANES, :]
        square += value * value
    square = jnp.sum(jnp.where(lanes_of(LANES) < COLS, square, 0.0), keepdims=True)
    out[:40] = own[:40]
    tail = own[40:]
    for i, number in enumerate((square, trace)):
        scale, factors = float16_scale(number)
        rest, words = number * scale, []
        for _ in range(3):
            words.append(eleven_bits(rest))
            rest = rest - words[-1]
        tail = with_row(with_factors(tail, 3 + 2 * i, factors), 4 + 2 * i, FREE, words)
    out[40:] = tail


def first_kernel(rows, whole, out, poly_rows, current_rows, spectral_out, right):
    at = position()
    inverses = {}
    square, trace = jnp.zeros((1, 1), f32), jnp.zeros((1, 1), f32)
    for b, _, packed in each_row_block(rows):
        tail = packed[40:]
        factor = products(tail)[:, FREE : FREE + 1]
        word = (tail[:, FREE + 2 : FREE + 3] + tail[:, FREE + 1 : FREE + 2]) + tail[:, FREE : FREE + 1]
        inverses[b] = factor[7:8]
        square += word[4:5] * factor[3:4]
        trace += word[6:7] * factor[5:6]
    spectral = 2.0 * square / (trace + EPS)
    inverse = 1.0 / spectral
    spectral_out[...] = jnp.broadcast_to(spectral, spectral_out.shape)
    for block in range(BLOCKS):
        part = pl.ds(block * LANES, LANES)
        right[part, :] = (-0.5 * (whole[part, :] * inverse)).astype(bf16)
    mine = pl.ds(pl.multiple_of(at[3], LANES), LANES)
    right[mine, :] = poly(own_square(), whole[mine, :] * inverse).astype(bf16)
    for b, lanes, packed in each_row_block(rows):
        left = row_in(packed[40:])
        for first, part in parts_of(packed):
            eye = eye_of(at, first, part.shape[0], b * COLS)
            current = (jnp.where(eye, part + left, part) * inverses[b]) * inverse
            poly_rows[first : first + part.shape[0], lanes] = poly(eye, current).astype(bf16)
            current_rows[first : first + part.shape[0], lanes] = current.astype(bf16)
    copies(out, pack(dot(poly_rows[...], right[...])))


def second_kernel(current_rows, cols, out_cols, out_rows, right):
    at = position()
    unpack_columns(cols, right)
    current, eye = dot(current_rows[...], right[...]), own_eye(at)
    value = poly(eye, current)
    copies(out_cols, pack(value))
    diagonal = jnp.sum(jnp.where(eye, current, 0.0), axis=0, keepdims=True)
    copies(out_rows, pack(value, tail_of(diagonal)))


def third_kernel(poly_rows, rows, cols, out, right, kept, rows_kept, first_rows, current_rows):
    at = position()
    unpack_columns(cols, right)
    diagonal = [jnp.zeros((count, LANES), f32) for count in (48, 16, 8)]
    for b, lanes, packed in each_row_block(rows):
        row = row_in(packed[40:].astype(f32))
        for i, (first, part) in enumerate(parts_of(packed)):
            count = part.shape[0]
            eye, part = eye_of(at, first, count, b * COLS), part.astype(f32)
            diagonal[i] += jnp.where(eye, row, 0.0)
            first_rows[first : first + count, lanes] = part.astype(bf16)
            current_rows[first : first + count, lanes] = jnp.where(eye, row, -2.0 * part).astype(bf16)
    own = pl.ds(pl.multiple_of(at[3], LANES), LANES)
    product = dot(poly_rows[...], right[...])
    moved = dot(current_rows[...], right[...])
    moved_low = moved.astype(bf16).astype(f32)
    square = dot(first_rows[...], right[...])
    moved_off = moved - moved_low
    kept[0] = first_rows[:, own].astype(f32)
    kept[1] = current_rows[:, own].astype(f32)
    kept[2] = moved_off
    kept[3] = square.astype(bf16).astype(f32) - square
    kept[4] = jnp.broadcast_to(
        jnp.sum(jnp.concatenate(diagonal, axis=0), axis=1, keepdims=True), (ROWS, LANES)
    )
    tail = tail_of(jnp.sum(jnp.where(own_eye(at), moved_off, 0.0), axis=0, keepdims=True))
    product, moved_low = pack(product).astype(bf16), pack(moved_low, tail).astype(bf16)
    for z in range(DEPTH):
        out[z, :SENT] = product
        out[z, SENT:] = moved_low
    mine = right[own, :].astype(f32)
    total = jnp.zeros((LANES, LANES), f32)
    for block in range(BLOCKS):
        value = right[block * LANES : (block + 1) * LANES, :].astype(f32)
        total += value * value
    total = jnp.sum(total, axis=0, keepdims=True)
    on = rows_of(LANES) == lanes_of(LANES)
    rows_kept[...] = jnp.where(
        rows_of(8) == 0,
        jnp.sum(jnp.where(on, mine, 0.0), axis=0, keepdims=True),
        total.astype(bf16).astype(f32) - total,
    )


def fourth_kernel(rows, right, kept, rows_kept, out, product_rows, moved_rows):
    at = position()
    diagonal = [jnp.zeros((count, LANES), f32) for count in (48, 16, 8)]
    for b, lanes, packed in each_row_block(rows):
        moved = packed[SENT:]
        row = row_in(moved[40:].astype(f32))
        for i, (first, part) in enumerate(parts_of(moved)):
            count = part.shape[0]
            diagonal[i] += jnp.where(eye_of(at, first, count, b * COLS), row, 0.0)
            moved_rows[first : first + count, lanes] = part.astype(bf16)
        for first, part in parts_of(packed[:SENT]):
            product_rows[first : first + part.shape[0], lanes] = part.astype(bf16)
    moved_diagonal = jnp.sum(jnp.concatenate(diagonal, axis=0), axis=1, keepdims=True)
    poly_own, current_own, moved_off, square_off, current_diagonal = (kept[i] for i in range(5))
    poly_diagonal, square_diagonal = rows_kept[0:1], rows_kept[1:2]
    eye = own_eye(at)
    off = jnp.where(
        eye,
        moved_off * poly_own + current_own * square_off,
        moved_diagonal * poly_own
        + moved_off * poly_diagonal
        + current_diagonal * square_off
        + current_own * square_diagonal,
    )
    copies(out, pack(poly(eye, dot(moved_rows[...], right[...]) + off)))


def fifth_kernel(product_rows, cols, out, right):
    unpack_columns(cols, right)
    copies(out, pack(dot(product_rows[...], right[...])))


def last_kernel(cols, whole0, whole1, spectral, out_gate, out_up, product):
    for t in range(TPS):
        packed = cols[t]
        product[MAIN * t : MAIN * t + 48, :] = packed
        product[MAIN * t + 48 : MAIN * (t + 1), :] = low_rows(packed).astype(bf16)
    for group in range(TPS // 4):
        product[LAST + 8 * group : LAST + 8 * (group + 1), :] = last_eight(cols, group).astype(bf16)
    half = D // 2
    ortho = sum(
        lax.dot_general(
            product[h * half : (h + 1) * half, :],
            whole[...],
            (((0,), (0,)), ((), ())),
            preferred_element_type=f32,
        )
        for h, whole in enumerate((whole0, whole1))
    )
    ortho = ortho[:COLS] * jnp.sqrt(2.0 * FF / spectral[0:1, 0:1])
    width = out_gate.shape[1]
    out_gate[...] = ortho[:, :width]
    out_up[...] = ortho[:, width : 2 * width]


def call(kernel, outs, *args, scratch=()):
    vmem = pl.BlockSpec(memory_space=pltpu.VMEM)
    return pl.pallas_call(
        kernel,
        out_shape=[jax.ShapeDtypeStruct(shape, dtype) for shape, dtype in outs],
        in_specs=[vmem] * len(args),
        out_specs=[vmem] * len(outs),
        scratch_shapes=[pltpu.VMEM(shape, dtype) for shape, dtype in scratch],
        compiler_params=pltpu.CompilerParams(vmem_limit_bytes=24 * 2**20),
        name=kernel.__name__,
    )(*args)


def exchange(stacked, axes):
    return lax.all_to_all(stacked, axes, split_axis=0, concat_axis=0, tiled=True)


def both_cores(by_z):
    return lax.all_gather(by_z, "core")


def local(grad_gate, grad_up, moment_gate, moment_up):
    gate_next = BETA * moment_gate + grad_gate
    up_next = BETA * moment_up + grad_up
    half = gate_next.shape[1]
    low = jnp.concatenate([gate_next.astype(bf16), up_next.astype(bf16)], axis=1)
    low = jnp.pad(low, ((0, 0), (0, 3 * LANES - 2 * half)))
    by_z = lax.all_gather(low, "z")
    whole = [
        both_cores(by_z[h * NEAR : (h + 1) * NEAR]).reshape(D // 2, -1) for h in range(2)
    ]

    right, left = ((KDIM, LANES), bf16), ((ROWS, KDIM), bf16)
    to_tp, to_z = ((TPS, SENT, LANES), bf16), ((DEPTH, SENT, LANES), bf16)
    packed = ((SENT, LANES), f32)

    (shares,) = call(
        gram_kernel,
        [(to_tp[0], f32)],
        low,
        *whole,
        scratch=[((LANES, low.shape[1]), bf16), ((D, LANES), f32)],
    )
    shares = exchange(shares.astype(f16), TP).astype(f32)
    (sent,) = call(total_kernel, [packed], shares)
    cols = exchange(jnp.broadcast_to(sent.astype(f16), to_tp[0]), TP).astype(f32)
    sent, gram_cols = call(square_kernel, [packed, (right[0], f32)], sent, cols)
    rows = exchange(jnp.broadcast_to(sent.astype(f16), to_z[0]), "z")
    rows = both_cores(rows).astype(f32)
    sent, poly_rows, current_rows, spectral = call(
        first_kernel, [to_tp, left, left, ((8, LANES), f32)], rows, gram_cols, scratch=[right]
    )
    cols, rows = call(
        second_kernel, [to_tp, to_z], current_rows, exchange(sent, TP), scratch=[right]
    )
    rows = both_cores(exchange(rows, "z"))
    cols = exchange(cols, TP)
    rows, right_poly, kept, rows_kept = call(
        third_kernel,
        [((DEPTH, 2 * SENT, LANES), bf16), right, ((5, ROWS, LANES), f32), ((8, LANES), f32)],
        poly_rows,
        rows,
        cols,
        scratch=[left, left],
    )
    rows = both_cores(exchange(rows, "z"))
    cols, product_rows = call(
        fourth_kernel, [to_tp, left], rows, right_poly, kept, rows_kept, scratch=[left]
    )
    (cols,) = call(fifth_kernel, [to_tp], product_rows, exchange(cols, TP), scratch=[right])
    ortho_gate, ortho_up = call(
        last_kernel,
        [((COLS, half), f32)] * 2,
        exchange(cols, TP),
        *whole,
        spectral,
        scratch=[((D, LANES), bf16)],
    )
    return gate_next, up_next, ortho_gate, ortho_up


def solution(mesh):
    split = Mesh(mesh.devices.reshape(DEPTH, 2, 8, 4), ("z", "core", "y", "x"))
    spec = P(FS, TP)
    return jax.shard_map(
        local, mesh=split, in_specs=(spec,) * 4, out_specs=(spec,) * 4, check_vma=False
    )
```

time: 252 us -> 229 us (0.909)
  waiting for transfers between devices: 23.8 us -> 10.7 us
  starting transfers between devices: 10.1 us -> 5.09 us
  blocking collectives: 205 us -> 200 us
  Pallas kernels: 6.91 us -> 9.98 us
    all_to_all x2 -> x1, waiting for transfers between devices: 23.8 us -> 10.7 us  [exchange(): lax.all_to_all(stacked, axes, split_axis=0, concat_axis=0, tiled=True)]
    all_to_all x7 -> x8, blocking collectives: 157 us -> 151 us  [exchange(): lax.all_to_all(stacked, axes, split_axis=0, concat_axis=0, tiled=True)]
    all_to_all x2 -> x1, starting transfers between devices: 10.1 us -> 5.09 us  [exchange(): lax.all_to_all(stacked, axes, split_axis=0, concat_axis=0, tiled=True)]
    all_gather x2 -> x0, blocking collectives: 4.76 us -> none  [local(): lax.all_gather(by_z[h * NEAR:(h + 1) * NEAR], 'core').reshape(D // 2, -1)]
    all_gather x3 -> x5, blocking collectives: 6.62 us -> 11 us  [both_cores(): return lax.all_gather(by_z, 'core')]
    pallas_call x9, Pallas kernels: 6.91 us -> 9.98 us  [call(): pl.pallas_call(kernel, out_shape=[jax.ShapeDtypeStruct(shape, dtype) for...]
  transfers between devices with their start and end apart: 2 -> 1, of which waited for: 2 -> 1; matrix products, arithmetic and copies ran while one was open for 0% -> 0% of each run, Pallas kernels for 0% -> 0%
where the time goes in v8:
time: 229 us; the launch traced here: 228 us
  blocking collectives  200 us (87%)
  waiting for transfers between devices  10.7 us (5%)
  Pallas kernels  9.98 us (4%)
  starting transfers between devices  5.09 us (2%)
    all_to_all x8, blocking collectives, exchange(): lax.all_to_all(stacked, axes, split_axis=0, concat_axis=0, tiled=True)  151 us
    all_gather x1, blocking collectives, local(): by_z = lax.all_gather(low, 'z')  37.4 us
    all_gather x5, blocking collectives, both_cores(): return lax.all_gather(by_z, 'core')  11 us
    all_to_all x1, waiting for transfers between devices, exchange(): lax.all_to_all(stacked, axes, split_axis=0, concat_axis=0, tiled=True)  10.7 us
    pallas_call x9, Pallas kernels, call(): pl.pallas_call(kernel, out_shape=[jax.ShapeDtypeStruct(shape, dtype) for...  9.98 us
    all_to_all x1, starting transfers between devices, exchange(): lax.all_to_all(stacked, axes, split_axis=0, concat_axis=0, tiled=True)  5.09 us
  transfers between devices with their start and end apart: 1, of which 1 were waited for; matrix products, arithmetic and copies ran while one was open for 0% of the time, Pallas kernels for 0%

profile of v8, /device:TPU:8, one launch (start us, length us, event | category | flops | bytes accessed | tf_op | source)
XLA Modules:
  0.0 228.2 jit_solution(16129275502393457683)
XLA Ops:
  0.6 1.7 fusion.3
  2.3 0.1 fusion.2.low
  2.4 37.4 %all-gather = bf16[1056,384]{1,0:T(8,128)(2,1)S(1)} all-gather(bf16[88,384]{1,0:T(8,128)(2,1)S(1)} %fusion.2.low), channel_id=2, replica_groups=mesh['z'=12,'core'=2,'y'=8,'x'=4] {'z'}, dimensions={0}, use_global_device_ids=true | all-gather | bytes 878592 | tf_op jit(solution)/shard_map/all_gather | solution.py:459
  39.8 0.1 fusion.5
  39.9 2.4 %all-gather.1 = bf16[12,88,384]{2,1,0:T(8,128)(2,1)S(1)} all-gather(bf16[6,88,384]{2,1,0:T(8,128)(2,1)S(1)} %bitcast.15), channel_id=3, replica_groups=mesh['z'=12,'core'=2,'y'=8,'x'=4] {'core'}, dimensions={0}, use_global_device_ids=true | all-gather | bytes 1216512 | tf_op jit(solution)/shard_map/all_gather | solution.py:450
  42.3 2.4 %all-gather.2 = bf16[12,88,384]{2,1,0:T(8,128)(2,1)S(1)} all-gather(bf16[6,88,384]{2,1,0:T(8,128)(2,1)S(1)} %bitcast.14), channel_id=4, replica_groups=mesh['z'=12,'core'=2,'y'=8,'x'=4] {'core'}, dimensions={0}, use_global_device_ids=true | all-gather | bytes 1216512 | tf_op jit(solution)/shard_map/all_gather | solution.py:450
  44.6 1.1 gram_kernel.1
  45.8 0.1 convert_element_type.28
  45.8 25.0 %all_to_all.45 = f16[32,48,128]{2,1,0:T(8,128)(2,1)S(1)} all-to-all(f16[32,48,128]{2,1,0:T(8,128)(2,1)S(1)} %convert_element_type.28), channel_id=1, replica_groups=mesh['z'=12,'core'=2,'y'=8,'x'=4] {'y','x'}, dimensions={0} | all-to-all | bytes 786432 | tf_op jit(solution)/shard_map/all_to_all | solution.py:446
  70.8 0.1 convert_element_type.29.arrived
  70.8 0.8 total_kernel.1.own
  71.7 0.1 broadcast_in_dim.6
  71.8 18.7 %all_to_all.46 = f16[32,48,128]{2,1,0:T(8,128)(2,1)S(1)} all-to-all(f16[32,48,128]{2,1,0:T(8,128)(2,1)S(1)} %broadcast_in_dim.6), channel_id=1, replica_groups=mesh['z'=12,'core'=2,'y'=8,'x'=4] {'y','x'}, dimensions={0} | all-to-all | bytes 786432 | tf_op jit(solution)/shard_map/all_to_all | solution.py:446
  90.4 0.1 convert_element_type.31.cols
  90.5 1.2 square_kernel.1
  91.7 14.7 %all_to_all.47 = f16[12,48,128]{2,1,0:T(8,128)(2,1)S(1)} all-to-all(f16[12,48,128]{2,1,0:T(8,128)(2,1)S(1)} %broadcast_in_dim.7), channel_id=1, replica_groups=mesh['z'=12,'core'=2,'y'=8,'x'=4] {'z'}, dimensions={0} | all-to-all | bytes 294912 | tf_op jit(solution)/shard_map/all_to_all | solution.py:446
  106.4 2.0 all-gather.3
  108.5 1.5 first_kernel.1
  110.0 19.6 %all_to_all.48.cols = bf16[32,48,128]{2,1,0:T(8,128)(2,1)S(1)} all-to-all(bf16[32,48,128]{2,1,0:T(8,128)(2,1)S(1)} %get-tuple-element.24), channel_id=1, replica_groups=mesh['z'=12,'core'=2,'y'=8,'x'=4] {'y','x'}, dimensions={0} | all-to-all | bytes 786432 | tf_op jit(solution)/shard_map/all_to_all | solution.py:446
  129.6 1.3 second_kernel.1
  130.9 14.6 %all_to_all.49 = bf16[12,48,128]{2,1,0:T(8,128)(2,1)S(1)} all-to-all(bf16[12,48,128]{2,1,0:T(8,128)(2,1)S(1)} %get-tuple-element.25), channel_id=1, replica_groups=mesh['z'=12,'core'=2,'y'=8,'x'=4] {'z'}, dimensions={0} | all-to-all | bytes 294912 | tf_op jit(solution)/shard_map/all_to_all | solution.py:446
  145.5 5.1 %all-to-all-start.5 = ((bf16[32,48,128]{2,1,0:T(8,128)(2,1)}), bf16[32,48,128]{2,1,0:T(8,128)(2,1)S(1)}, u32[]{:S(2)}, u32[]{:S(2)}) async-start(bf16[32,48,128]{2,1,0:T(8,128)(2,1)} %get-tuple-element.26), calls=%async_computation.5 | async-start | bytes 786432 | tf_op jit(solution)/shard_map/all_to_all | solution.py:446
  150.6 2.0 all-gather.4
  152.6 10.7 %all-to-all-done.5.cols = bf16[32,48,128]{2,1,0:T(8,128)(2,1)S(1)} async-done(((bf16[32,48,128]{2,1,0:T(8,128)(2,1)}), bf16[32,48,128]{2,1,0:T(8,128)(2,1)S(1)}, u32[]{:S(2)}, u32[]{:S(2)}) %all-to-all-start.5) | async-done | bytes 393248 | tf_op jit(solution)/shard_map/all_to_all | solution.py:446
  163.3 1.2 third_kernel.1
  164.5 19.1 %all_to_all.50 = bf16[12,96,128]{2,1,0:T(8,128)(2,1)S(1)} all-to-all(bf16[12,96,128]{2,1,0:T(8,128)(2,1)S(1)} %get-tuple-element.27), channel_id=1, replica_groups=mesh['z'=12,'core'=2,'y'=8,'x'=4] {'z'}, dimensions={0} | all-to-all | bytes 589824 | tf_op jit(solution)/shard_map/all_to_all | solution.py:446
  183.5 2.2 all-gather.5
  185.7 0.6 fourth_kernel.1
  186.4 20.8 %all_to_all.51.cols = bf16[32,48,128]{2,1,0:T(8,128)(2,1)S(1)} all-to-all(bf16[32,48,128]{2,1,0:T(8,128)(2,1)S(1)} %get-tuple-element.32), channel_id=1, replica_groups=mesh['z'=12,'core'=2,'y'=8,'x'=4] {'y','x'}, dimensions={0} | all-to-all | bytes 786432 | tf_op jit(solution)/shard_map/all_to_all | solution.py:446
  207.2 0.6 fifth_kernel.1
  207.8 18.7 %all_to_all.52.cols = bf16[32,48,128]{2,1,0:T(8,128)(2,1)S(1)} all-to-all(bf16[32,48,128]{2,1,0:T(8,128)(2,1)S(1)} %fifth_kernel.1), channel_id=1, replica_groups=mesh['z'=12,'core'=2,'y'=8,'x'=4] {'y','x'}, dimensions={0} | all-to-all | bytes 786432 | tf_op jit(solution)/shard_map/all_to_all | solution.py:446
  226.5 1.7 last_kernel.1
  (4 shorter events, 0.1 us)
Async XLA Ops:
  145.5 17.8 %all-to-all-start.5 = ((bf16[32,48,128]{2,1,0:T(8,128)(2,1)}), bf16[32,48,128]{2,1,0:T(8,128)(2,1)S(1)}, u32[]{:S(2)}, u32[]{:S(2)}) async-start(bf16[32,48,128]{2,1,0:T(8,128)(2,1)} %get-tuple-element.26), calls=%async_computation.5 | async-start | bytes 786432 | tf_op jit(solution)/shard_map/all_to_all | solution.py:446

commit v9 on v8

--- a/solution.py
+++ b/solution.py
@@ -16,7 +16,7 @@
 COLS = 88
 BLOCKS = D // COLS
 DEPTH = 12
-NEAR = 6
+SIDE = DEPTH * 88
 TPS = 32
 MAIN = 64
 LAST = TPS * MAIN
@@ -30,7 +30,12 @@
 
 
 def place(core, z):
-    return ((z // NEAR) * 2 + core) * NEAR + z % NEAR
+    return core * DEPTH + z
+
+
+def sides():
+    core = lax.axis_index("core")
+    return tuple(pl.ds(pl.multiple_of(c * SIDE, 8), SIDE) for c in (core, 1 - core))
 
 
 def lanes_of(rows):
@@ -207,18 +212,27 @@
             yield b, slice(b * LANES, (b + 1) * LANES), rows[core, z]
 
 
-def gram_kernel(low, whole0, whole1, out, own, share):
-    at = position()
+def side_kernel(low, whole, out, own):
     own[:COLS] = low[...]
     own[COLS:] = jnp.zeros((LANES - COLS, own.shape[1]), bf16)
-    half = D // 2
-    most = jnp.zeros((1, 1), f32)
-    for h, whole in enumerate((whole0, whole1)):
-        part = lax.dot_general(
-            whole[...], own[...], (((1,), (1,)), ((), ())), preferred_element_type=f32
-        )
-        share[h * half : (h + 1) * half] = part
-        most = jnp.maximum(most, jnp.max(jnp.abs(part), keepdims=True))
+    out[...] = lax.dot_general(
+        whole[...], own[...], (((1,), (1,)), ((), ())), preferred_element_type=f32
+    )
+
+
+def gram_kernel(low, whole, side, out, own, share):
+    at = position()
+    own[:COLS] = low[...]
+    own[COLS:] = jnp.zeros((LANES - COLS, own.shape[1]), bf16)
+    here, there = sides()
+    part = side[...]
+    most = jnp.max(jnp.abs(part), keepdims=True)
+    share[here] = part
+    part = lax.dot_general(
+        whole[...], own[...], (((1,), (1,)), ((), ())), preferred_element_type=f32
+    )
+    most = jnp.maximum(most, jnp.max(jnp.abs(part), keepdims=True))
+    share[there] = part
     scale, factors = float16_scale(most)
     mine = share[pl.ds(pl.multiple_of(at[2], 8), COLS), :] * scale
     eye = rows_of(COLS) == lanes_of(COLS)
@@ -413,15 +427,11 @@
         product[MAIN * t + 48 : MAIN * (t + 1), :] = low_rows(packed).astype(bf16)
     for group in range(TPS // 4):
         product[LAST + 8 * group : LAST + 8 * (group + 1), :] = last_eight(cols, group).astype(bf16)
-    half = D // 2
     ortho = sum(
         lax.dot_general(
-            product[h * half : (h + 1) * half, :],
-            whole[...],
-            (((0,), (0,)), ((), ())),
-            preferred_element_type=f32,
+            product[side, :], whole[...], (((0,), (0,)), ((), ())), preferred_element_type=f32
         )
-        for h, whole in enumerate((whole0, whole1))
+        for side, whole in zip(sides(), (whole0, whole1))
     )
     ortho = ortho[:COLS] * jnp.sqrt(2.0 * FF / spectral[0:1, 0:1])
     width = out_gate.shape[1]
@@ -457,20 +467,18 @@
     low = jnp.concatenate([gate_next.astype(bf16), up_next.astype(bf16)], axis=1)
     low = jnp.pad(low, ((0, 0), (0, 3 * LANES - 2 * half)))
     by_z = lax.all_gather(low, "z")
-    whole = [
-        both_cores(by_z[h * NEAR : (h + 1) * NEAR]).reshape(D // 2, -1) for h in range(2)
-    ]
+    here = by_z.reshape(SIDE, -1)
+    there = lax.ppermute(here, "core", [(0, 1), (1, 0)])
+    whole = (here, there)
 
     right, left = ((KDIM, LANES), bf16), ((ROWS, KDIM), bf16)
     to_tp, to_z = ((TPS, SENT, LANES), bf16), ((DEPTH, SENT, LANES), bf16)
     packed = ((SENT, LANES), f32)
 
+    own = ((LANES, low.shape[1]), bf16)
+    (side,) = call(side_kernel, [((SIDE, LANES), f32)], low, here, scratch=[own])
     (shares,) = call(
-        gram_kernel,
-        [(to_tp[0], f32)],
-        low,
-        *whole,
-        scratch=[((LANES, low.shape[1]), bf16), ((D, LANES), f32)],
+        gram_kernel, [(to_tp[0], f32)], low, there, side, scratch=[own, ((D, LANES), f32)]
     )
     shares = exchange(shares.astype(f16), TP).astype(f32)
     (sent,) = call(total_kernel, [packed], shares)

time: 229 us -> 228 us (level)
  blocking collectives: 200 us -> 195 us
    all_gather x5 -> x3, blocking collectives: 11 us -> 6.24 us  [both_cores(): return lax.all_gather(by_z, 'core')]
    pallas_call x9 -> x10, Pallas kernels: 9.98 us -> 9.95 us  [call(): pl.pallas_call(kernel, out_shape=[jax.ShapeDtypeStruct(shape, dtype) for...]
  transfers between devices with their start and end apart: 1 -> 2, of which waited for: 1 -> 2; matrix products, arithmetic and copies ran while one was open for 0% -> 0% of each run, Pallas kernels for 0% -> 0%
where the time goes in v9:
time: 228 us; the launch traced here: 227 us
  blocking collectives  195 us (86%)
  waiting for transfers between devices  12.6 us (6%)
  Pallas kernels  9.95 us (4%)
  starting transfers between devices  7.01 us (3%)
    all_to_all x8, blocking collectives, exchange(): lax.all_to_all(stacked, axes, split_axis=0, concat_axis=0, tiled=True)  151 us
    all_gather x1, blocking collectives, local(): by_z = lax.all_gather(low, 'z')  37.4 us
    all_to_all x1, waiting for transfers between devices, exchange(): lax.all_to_all(stacked, axes, split_axis=0, concat_axis=0, tiled=True)  10.7 us
    pallas_call x10, Pallas kernels, call(): pl.pallas_call(kernel, out_shape=[jax.ShapeDtypeStruct(shape, dtype) for...  9.95 us
    all_gather x3, blocking collectives, both_cores(): return lax.all_gather(by_z, 'core')  6.24 us
    all_to_all x1, starting transfers between devices, exchange(): lax.all_to_all(stacked, axes, split_axis=0, concat_axis=0, tiled=True)  5.1 us
  transfers between devices with their start and end apart: 2, of which 2 were waited for; matrix products, arithmetic and copies ran while one was open for 0% of the time, Pallas kernels for 0%

profile of v9, /device:TPU:8, one launch (start us, length us, event | category | flops | bytes accessed | tf_op | source)
XLA Modules:
  0.0 227.1 jit_solution(8667919763325490111)
XLA Ops:
  0.6 1.7 fusion.3
  2.3 0.1 fusion.2.low
  2.4 37.4 %all-gather.whole.whole0 = bf16[1056,384]{1,0:T(8,128)(2,1)S(1)} all-gather(bf16[88,384]{1,0:T(8,128)(2,1)S(1)} %fusion.2.low), channel_id=2, replica_groups=mesh['z'=12,'core'=2,'y'=8,'x'=4] {'z'}, dimensions={0}, use_global_device_ids=true | all-gather | bytes 878592 | tf_op jit(solution)/shard_map/all_gather | solution.py:469
  39.8 1.9 collective-permute-start
  41.7 0.4 side_kernel.1.side
  42.1 1.9 collective-permute-done.whole.whole1
  44.0 0.9 gram_kernel.1
  44.9 0.1 convert_element_type.28
  45.0 24.9 %all_to_all.45 = f16[32,48,128]{2,1,0:T(8,128)(2,1)S(1)} all-to-all(f16[32,48,128]{2,1,0:T(8,128)(2,1)S(1)} %convert_element_type.28), channel_id=1, replica_groups=mesh['z'=12,'core'=2,'y'=8,'x'=4] {'y','x'}, dimensions={0} | all-to-all | bytes 786432 | tf_op jit(solution)/shard_map/all_to_all | solution.py:456
  69.9 0.1 convert_element_type.29.arrived
  70.0 0.8 total_kernel.1.own
  70.9 0.1 broadcast_in_dim.6
  70.9 18.7 %all_to_all.46 = f16[32,48,128]{2,1,0:T(8,128)(2,1)S(1)} all-to-all(f16[32,48,128]{2,1,0:T(8,128)(2,1)S(1)} %broadcast_in_dim.6), channel_id=1, replica_groups=mesh['z'=12,'core'=2,'y'=8,'x'=4] {'y','x'}, dimensions={0} | all-to-all | bytes 786432 | tf_op jit(solution)/shard_map/all_to_all | solution.py:456
  89.6 0.1 convert_element_type.31.cols
  89.7 1.2 square_kernel.1
  90.9 14.7 %all_to_all.47 = f16[12,48,128]{2,1,0:T(8,128)(2,1)S(1)} all-to-all(f16[12,48,128]{2,1,0:T(8,128)(2,1)S(1)} %broadcast_in_dim.7), channel_id=1, replica_groups=mesh['z'=12,'core'=2,'y'=8,'x'=4] {'z'}, dimensions={0} | all-to-all | bytes 294912 | tf_op jit(solution)/shard_map/all_to_all | solution.py:456
  105.6 2.0 all-gather.1
  107.6 1.5 first_kernel.1
  109.1 19.6 %all_to_all.48.cols = bf16[32,48,128]{2,1,0:T(8,128)(2,1)S(1)} all-to-all(bf16[32,48,128]{2,1,0:T(8,128)(2,1)S(1)} %get-tuple-element.24), channel_id=1, replica_groups=mesh['z'=12,'core'=2,'y'=8,'x'=4] {'y','x'}, dimensions={0} | all-to-all | bytes 786432 | tf_op jit(solution)/shard_map/all_to_all | solution.py:456
  128.7 1.3 second_kernel.1
  130.0 14.6 %all_to_all.49 = bf16[12,48,128]{2,1,0:T(8,128)(2,1)S(1)} all-to-all(bf16[12,48,128]{2,1,0:T(8,128)(2,1)S(1)} %get-tuple-element.25), channel_id=1, replica_groups=mesh['z'=12,'core'=2,'y'=8,'x'=4] {'z'}, dimensions={0} | all-to-all | bytes 294912 | tf_op jit(solution)/shard_map/all_to_all | solution.py:456
  144.7 5.1 %all-to-all-start.5 = ((bf16[32,48,128]{2,1,0:T(8,128)(2,1)}), bf16[32,48,128]{2,1,0:T(8,128)(2,1)S(1)}, u32[]{:S(2)}, u32[]{:S(2)}) async-start(bf16[32,48,128]{2,1,0:T(8,128)(2,1)} %get-tuple-element.26), calls=%async_computation.5 | async-start | bytes 786432 | tf_op jit(solution)/shard_map/all_to_all | solution.py:456
  149.8 2.0 all-gather.2
  151.8 10.7 %all-to-all-done.5.cols = bf16[32,48,128]{2,1,0:T(8,128)(2,1)S(1)} async-done(((bf16[32,48,128]{2,1,0:T(8,128)(2,1)}), bf16[32,48,128]{2,1,0:T(8,128)(2,1)S(1)}, u32[]{:S(2)}, u32[]{:S(2)}) %all-to-all-start.5) | async-done | bytes 393248 | tf_op jit(solution)/shard_map/all_to_all | solution.py:456
  162.5 1.2 third_kernel.1
  163.6 19.0 %all_to_all.50 = bf16[12,96,128]{2,1,0:T(8,128)(2,1)S(1)} all-to-all(bf16[12,96,128]{2,1,0:T(8,128)(2,1)S(1)} %get-tuple-element.27), channel_id=1, replica_groups=mesh['z'=12,'core'=2,'y'=8,'x'=4] {'z'}, dimensions={0} | all-to-all | bytes 589824 | tf_op jit(solution)/shard_map/all_to_all | solution.py:456
  182.7 2.2 all-gather.3
  184.9 0.6 fourth_kernel.1
  185.5 20.8 %all_to_all.51.cols = bf16[32,48,128]{2,1,0:T(8,128)(2,1)S(1)} all-to-all(bf16[32,48,128]{2,1,0:T(8,128)(2,1)S(1)} %get-tuple-element.32), channel_id=1, replica_groups=mesh['z'=12,'core'=2,'y'=8,'x'=4] {'y','x'}, dimensions={0} | all-to-all | bytes 786432 | tf_op jit(solution)/shard_map/all_to_all | solution.py:456
  206.4 0.6 fifth_kernel.1
  207.0 18.7 %all_to_all.52.cols = bf16[32,48,128]{2,1,0:T(8,128)(2,1)S(1)} all-to-all(bf16[32,48,128]{2,1,0:T(8,128)(2,1)S(1)} %fifth_kernel.1), channel_id=1, replica_groups=mesh['z'=12,'core'=2,'y'=8,'x'=4] {'y','x'}, dimensions={0} | all-to-all | bytes 786432 | tf_op jit(solution)/shard_map/all_to_all | solution.py:456
  225.6 1.5 last_kernel.1
  (4 shorter events, 0.1 us)
Async XLA Ops:
  39.8 4.2 %collective-permute-start = (bf16[1056,384]{1,0:T(8,128)(2,1)S(1)}, bf16[1056,384]{1,0:T(8,128)(2,1)S(1)}, u32[]{:S(2)}, u32[]{:S(2)}) collective-permute-start(bf16[1056,384]{1,0:T(8,128)(2,1)S(1)} %all-gather.whole.whole0), channel_id=1, source_target_pairs={{0,32},{32,0},{1,33},{33,1},{2,34},{34,2},{3,35},{35,3},{4,36},{36... | collective-permute-start | bytes 2433032 | tf_op jit(solution)/shard_map/ppermute | solution.py:471
  144.7 17.8 %all-to-all-start.5 = ((bf16[32,48,128]{2,1,0:T(8,128)(2,1)}), bf16[32,48,128]{2,1,0:T(8,128)(2,1)S(1)}, u32[]{:S(2)}, u32[]{:S(2)}) async-start(bf16[32,48,128]{2,1,0:T(8,128)(2,1)} %get-tuple-element.26), calls=%async_computation.5 | async-start | bytes 786432 | tf_op jit(solution)/shard_map/all_to_all | solution.py:456
